TPU v7x, 256 devices: a whole 4x4x8 slice. The times are simulated.
256 devices in a mesh: rep: 2 (over z_hi), fs: 16 (over z_lo, x), tp: 8 (over y, core).
Axes of the slice: x: 4, y: 4, z: 8 (z_hi: 2, z_lo: 4; z = z_hi * 4 + z_lo), core: 2. Of those that a mesh axis runs over, the one named last changes fastest.
Arguments:
- tokens: bfloat16 [4096, 4096], P(('rep', 'fs'), 'tp'), may hold values from -6 to 6
- mixer_gain: float32 [4096], replicated, may hold values from 0.75 to 1.25
- gate_proj: bfloat16 [4096, 2048], P('fs', 'tp'), may hold values from -0.09375 to 0.09375
- value_proj: bfloat16 [4096, 2048], P('fs', 'tp'), may hold values from -0.09375 to 0.09375
- value_gain: float32 [16, 128], P('tp'), may hold values from 0.75 to 1.25
- spatial_mix: bfloat16 [16, 128, 128], P('tp', 'fs'), may hold values from -0.5 to 0.5
- spatial_bias: float32 [16, 128], P('tp'), may hold values from 0.5 to 1.5
- head_gain: float32 [16, 128], P('tp'), may hold values from 0.75 to 1.25
- merge_proj: bfloat16 [2048, 4096], P('tp', 'fs'), may hold values from -0.125 to 0.125
- ffn_gain: float32 [4096], replicated, may hold values from 0.25 to 1.75
- gate_up: bfloat16 [4096, 11008], P('fs', 'tp'), may hold values from -0.09375 to 0.09375
- value_up: bfloat16 [4096, 11008], P('fs', 'tp'), may hold values from -0.09375 to 0.09375
- gate_kernel: float32 [3, 11008], P(None, 'tp'), may hold values from -3.5 to 3.5
- value_kernel: float32 [3, 11008], P(None, 'tp'), may hold values from -3.5 to 3.5
- gate_offset: float32 [11008], P('tp'), may hold values from -0.6 to 0.6
- value_offset: float32 [11008], P('tp'), may hold values from -1.8 to 1.8
- down_proj: bfloat16 [11008, 4096], P('tp', 'fs'), may hold values from -0.0546875 to 0.0546875
Outputs:
- layer_out: bfloat16 [4096, 4096], P(('rep', 'fs'), 'tp')
All inputs are finite; a program needn't handle non-finite values.
Results may differ from a plain program's by a relative error of at most 0.02.
Values may be sent and summed in bfloat16 or wider, within the bound.
A program may use at most 128 MiB of HBM per device.

v0:
```python
import jax
import jax.numpy as jnp
from jax import lax
from jax.sharding import Mesh
from jax.sharding import PartitionSpec as P

TP = ("tp_0", "tp_1")
FS = ("fs_0", "fs_1")
REP_FS = ("rep", "fs_0", "fs_1")


epsilon = 1e-06


def cut_rows(length, count):
    hop = length // count
    if hop >= 8:
        hop -= hop % 8
    return [hop * k for k in range(1, count)]


def stacked_from(value, axes, sequence):
    blocks = value[None]
    for k in sequence:
        blocks = lax.all_gather(blocks, axes[k], axis=0, tiled=True)
    block = [lax.axis_size(axes[k]) for k in reversed(sequence)]
    blocks = blocks.reshape(*block, *value.shape)
    turned = sorted(range(len(sequence)), key=lambda place: sequence[len(sequence) - 1 - place])
    return blocks.transpose(*turned, *range(len(sequence), blocks.ndim)).reshape(-1, *value.shape)


def laid_out(blocks, dim):
    dims = list(blocks.shape[1:])
    dims[dim] *= blocks.shape[0]
    return jnp.moveaxis(blocks, 0, dim).reshape(dims)


def gather_at_once(value, axes, dim):
    numbers = list(range(len(axes)))[::-1]
    widest = value.shape.index(max(value.shape[:-1] or value.shape))
    edges = [0, *cut_rows(value.shape[widest], len(axes)), value.shape[widest]]
    gathered = []
    for k, (start, end) in enumerate(zip(edges, edges[1:])):
        if end > start:
            slab = lax.slice_in_dim(value, start, end, axis=widest)
            gathered.append(stacked_from(slab, axes, numbers[k:] + numbers[:k]))
    return laid_out(jnp.concatenate(gathered, axis=widest + 1), dim)


def whole_of(value, axes, sequence, dim):
    return laid_out(stacked_from(value, axes, sequence), dim)


def taken_in(value, axes, sequence, dim, take_in, carry):
    everything = jax.tree.map(lambda part: whole_of(part, axes, sequence, dim), value)
    return take_in(carry, everything, jnp.int32(0))


def on_whole(value, axes, sequence, dim, apply):
    return apply(whole_of(value, axes, sequence, dim), jnp.int32(0))


def folded(value, axis, dim, take_in, carry):
    whole = jax.tree.map(lambda part: lax.all_gather(part, axis, axis=dim, tiled=True), value)
    return take_in(carry, whole, jnp.int32(0))


def gathered_then(shard, axis, dim, work):
    return work(lax.all_gather(shard, axis, axis=dim, tiled=True), jnp.int32(0))


def normalize(values, gain):
    values = values.astype(jnp.float32)
    scaled = values * lax.rsqrt(jnp.mean(values * values, axis=-1, keepdims=True) + epsilon)
    return scaled * gain


def rounded(values):
    return lax.optimization_barrier(values.astype(jnp.bfloat16)).astype(jnp.float32)


def gelu_exact(values):
    return jax.nn.gelu(values, approximate=False)


def convolve(values, kernel, offset, length):
    total_rows, width = values.shape
    blocks = values.reshape(total_rows // length, length, width)
    padded = jnp.pad(blocks, ((0, 0), (1, 1), (0, 0)))
    result = (
        offset
        + padded[:, 0:length] * kernel[0]
        + padded[:, 1 : length + 1] * kernel[1]
        + padded[:, 2:] * kernel[2]
    )
    return result.reshape(total_rows, width)


def add_block(total, whole, piece, start):
    columns = lax.dynamic_slice_in_dim(whole, start, piece.shape[0], 1)
    return total + jnp.dot(columns, piece, preferred_element_type=jnp.float32)


def body(
    tokens,
    mixer_gain,
    gate_proj,
    value_proj,
    value_gain,
    spatial_mix,
    spatial_bias,
    head_gain,
    merge_proj,
    ffn_gain,
    gate_up,
    value_up,
    gate_kernel,
    value_kernel,
    gate_offset,
    value_offset,
    down_proj,
):
    heads_here = spatial_mix.shape[0]
    length = spatial_mix.shape[2]
    whole = gather_at_once(tokens, TP, 1)
    normed = normalize(whole, mixer_gain).astype(jnp.bfloat16)
    total_rows = normed.shape[0]
    width = gate_proj.shape[1]
    empty = jnp.zeros((total_rows, width), jnp.float32)

    def add_mixer(total, piece, start):
        return add_block(total, normed, piece, start)

    first = taken_in(gate_proj, FS, (0, 1), 0, add_mixer, empty)
    second = taken_in(value_proj, FS, (0, 1), 0, add_mixer, empty)
    gated = gelu_exact(rounded(first))
    spread = gelu_exact(rounded(second))
    head_width = width // heads_here
    seqs = total_rows // length
    spread = normalize(spread.reshape(seqs, length, heads_here, head_width), value_gain).astype(
        jnp.bfloat16
    )
    matrix = whole_of(spatial_mix, FS, (0, 1), 1)
    mixed = jnp.einsum("hij,njhd->nihd", matrix, spread, preferred_element_type=jnp.float32)
    mixed = mixed + spatial_bias.T[None, :, :, None]
    joined = gated.reshape(seqs, length, heads_here, head_width) * mixed
    merged = normalize(joined, head_gain).astype(jnp.bfloat16).reshape(total_rows, width)

    def project_merge(piece, start):
        return jnp.dot(merged, piece, preferred_element_type=jnp.float32)

    merge_terms = on_whole(merge_proj, FS, (0, 1), 1, project_merge)
    branch = lax.psum_scatter(
        merge_terms.astype(jnp.bfloat16), TP, scatter_dimension=1, tiled=True
    ).astype(jnp.float32)
    hidden = (tokens.astype(jnp.float32) + branch).astype(jnp.bfloat16)
    full_rows = gather_at_once(hidden, TP, 1)
    normed_ffn = normalize(full_rows, ffn_gain).astype(jnp.bfloat16)
    inner = gate_up.shape[1]
    blank = jnp.zeros((total_rows, inner), jnp.float32)

    def add_ffn(total, piece, start):
        return add_block(total, normed_ffn, piece, start)

    upper_gate = folded(gate_up, FS, 0, add_ffn, blank)
    upper_value = folded(value_up, FS, 0, add_ffn, blank)
    conv_gate = convolve(rounded(upper_gate), gate_kernel, gate_offset, length)
    conv_value = convolve(rounded(upper_value), value_kernel, value_offset, length)
    active = (gelu_exact(conv_gate) * conv_value).astype(jnp.bfloat16)

    def project_down(piece, start):
        return jnp.dot(active, piece, preferred_element_type=jnp.float32)

    down_terms = gathered_then(down_proj, FS, 1, project_down)
    change = lax.psum_scatter(
        down_terms.astype(jnp.bfloat16), TP, scatter_dimension=1, tiled=True
    ).astype(jnp.float32)
    return (hidden.astype(jnp.float32) + change).astype(jnp.bfloat16)


def solution(mesh):
    finer = Mesh(
        mesh.devices.reshape(mesh.shape["rep"], 4, 4, 4, 2), ("rep", "fs_0", "fs_1", "tp_0", "tp_1")
    )
    return jax.shard_map(
        body,
        mesh=finer,
        in_specs=(
            P(REP_FS, TP),
            P(),
            P(FS, TP),
            P(FS, TP),
            P(TP, None),
            P(TP, FS, None),
            P(TP, None),
            P(TP, None),
            P(TP, FS),
            P(),
            P(FS, TP),
            P(FS, TP),
            P(None, TP),
            P(None, TP),
            P(TP),
            P(TP),
            P(TP, FS),
        ),
        out_specs=P(REP_FS, TP),
        check_vma=False,
    )
```

profile of v0, /device:TPU:57, one launch (start us, length us, event | category | flops | bytes accessed | tf_op | source)
XLA Modules:
  0.0 657.7 jit_solution(1269820380555032049)
XLA Ops:
  7.4 14.3 %all-gather.3 = bf16[1024,256]{1,0:T(8,128)(2,1)} all-gather(bf16[256,256]{1,0:T(8,128)(2,1)} %param.20), channel_id=5, replica_groups=mesh['rep'=2,'fs_0'=4,'fs_1'=4,'tp_0'=4,'tp_1'=2] {'fs_0'}, dimensions={0}, use_global_device_ids=true | all-gather | bytes 655360 | tf_op jit(solution)/shard_map/all_gather | solution.py:25
  21.8 14.0 %all-gather.2 = bf16[1024,256]{1,0:T(8,128)(2,1)} all-gather(bf16[256,256]{1,0:T(8,128)(2,1)} %param.19), channel_id=4, replica_groups=mesh['rep'=2,'fs_0'=4,'fs_1'=4,'tp_0'=4,'tp_1'=2] {'fs_0'}, dimensions={0}, use_global_device_ids=true | all-gather | bytes 655360 | tf_op jit(solution)/shard_map/all_gather | solution.py:25
  35.8 14.4 %all-gather.5 = bf16[1024,256]{1,0:T(8,128)(2,1)} all-gather(bf16[256,256]{1,0:T(8,128)(2,1)S(1)} %copy-done.1), channel_id=7, replica_groups=mesh['rep'=2,'fs_0'=4,'fs_1'=4,'tp_0'=4,'tp_1'=2] {'fs_0'}, dimensions={0}, use_global_device_ids=true | all-gather | bytes 655360 | tf_op jit(solution)/shard_map/all_gather | solution.py:25
  50.3 10.2 %all-gather.1 = bf16[256,512]{1,0:T(8,128)(2,1)S(1)} all-gather(bf16[64,512]{1,0:T(8,128)(2,1)S(1)} %get-tuple-element.16), channel_id=3, replica_groups=mesh['rep'=2,'fs_0'=4,'fs_1'=4,'tp_0'=4,'tp_1'=2] {'tp_0'}, dimensions={0}, use_global_device_ids=true | all-gather | bytes 327680 | tf_op jit(solution)/shard_map/all_gather | solution.py:25
  60.4 12.4 %all_gather.60 = bf16[8,64,512]{2,1,0:T(8,128)(2,1)S(1)} all-gather(bf16[4,64,512]{2,1,0:T(8,128)(2,1)S(1)} %bitcast.190), channel_id=1, replica_groups=mesh['rep'=2,'fs_0'=4,'fs_1'=4,'tp_0'=4,'tp_1'=2] {'tp_1'}, dimensions={0}, use_global_device_ids=true | all-gather | bytes 786432 | tf_op jit(solution)/shard_map/all_gather | solution.py:25
  72.9 1.9 all-gather
  74.8 11.1 %all_gather.58 = bf16[8,64,512]{2,1,0:T(8,128)(2,1)S(1)} all-gather(bf16[2,64,512]{2,1,0:T(8,128)(2,1)S(1)} %bitcast.194), channel_id=1, replica_groups=mesh['rep'=2,'fs_0'=4,'fs_1'=4,'tp_0'=4,'tp_1'=2] {'tp_0'}, dimensions={0}, use_global_device_ids=true | all-gather | bytes 655360 | tf_op jit(solution)/shard_map/all_gather | solution.py:25
  86.5 0.7 copy.80
  87.2 10.4 %all-gather.4 = bf16[8,8,128]{2,1,0:T(8,128)(2,1)S(1)} all-gather(bf16[2,8,128]{2,1,0:T(8,128)(2,1)S(1)} %copy-done.6), channel_id=6, replica_groups=mesh['rep'=2,'fs_0'=4,'fs_1'=4,'tp_0'=4,'tp_1'=2] {'fs_0'}, dimensions={0}, use_global_device_ids=true | all-gather | bytes 20480 | tf_op jit(solution)/shard_map/all_gather | solution.py:25
  97.6 9.0 %all_gather.66 = bf16[16,2,8,128]{3,2,1,0:T(8,128)(2,1)S(1)} all-gather(bf16[4,2,8,128]{3,2,1,0:T(8,128)(2,1)S(1)} %bitcast.199), channel_id=1, replica_groups=mesh['rep'=2,'fs_0'=4,'fs_1'=4,'tp_0'=4,'tp_1'=2] {'fs_1'}, dimensions={0}, use_global_device_ids=true | all-gather | bytes 81920 | tf_op jit(solution)/shard_map/all_gather | solution.py:25
  106.7 1.7 copy.82
  108.4 0.7 convolution_convert_fusion.4
  109.9 1.7 copy.81
  112.9 16.6 %all-gather.19.cloned.1.call-done = bf16[16,256,256]{2,1,0:T(8,128)(2,1)} async-done(((bf16[4,256,256]{2,1,0:T(8,128)(2,1)}), bf16[16,256,256]{2,1,0:T(8,128)(2,1)}) %all-gather.19.cloned.1.call-update) | async-done | bytes 2097168 | tf_op jit(solution)/shard_map/all_gather | solution.py:25
  129.5 3.1 copy.87
  132.6 2.9 copy.88
  135.6 1.8 convolution_convert_fusion.1
  139.4 32.1 %reduce-scatter.3.cloned.1.call-done = bf16[128,512]{1,0:T(8,128)(2,1)} async-done(((bf16[128,4096]{1,0:T(8,128)(2,1)}), bf16[128,512]{1,0:T(8,128)(2,1)}) %reduce-scatter.3.cloned.1.call-update) | async-done | bytes 131088 | tf_op jit(solution)/shard_map/reduce_scatter | solution.py:153
  171.5 0.9 add_convert_fusion.1
  172.4 10.7 %all-gather.7 = bf16[256,512]{1,0:T(8,128)(2,1)S(1)} all-gather(bf16[64,512]{1,0:T(8,128)(2,1)S(1)} %get-tuple-element.14), channel_id=9, replica_groups=mesh['rep'=2,'fs_0'=4,'fs_1'=4,'tp_0'=4,'tp_1'=2] {'tp_0'}, dimensions={0}, use_global_device_ids=true | all-gather | bytes 327680 | tf_op jit(solution)/shard_map/all_gather | solution.py:25
  183.1 3.4 all_gather.72
  187.0 1.9 all-gather.6
  188.9 12.1 %all_gather.70 = bf16[8,64,512]{2,1,0:T(8,128)(2,1)S(1)} all-gather(bf16[2,64,512]{2,1,0:T(8,128)(2,1)S(1)} %bitcast.195), channel_id=1, replica_groups=mesh['rep'=2,'fs_0'=4,'fs_1'=4,'tp_0'=4,'tp_1'=2] {'tp_0'}, dimensions={0}, use_global_device_ids=true | all-gather | bytes 655360 | tf_op jit(solution)/shard_map/all_gather | solution.py:25
  202.8 0.8 fusion.4
  203.7 78.2 %all-gather.21.cloned.1.call-done = bf16[4096,1376]{0,1:T(8,128)(2,1)} async-done(((bf16[256,1376]{0,1:T(8,128)(2,1)}), bf16[4096,1376]{0,1:T(8,128)(2,1)}) %all-gather.21.cloned.1.call-update) | async-done | bytes 11272208 | tf_op jit(solution)/shard_map/all_gather | solution.py:64
  281.9 5.9 convolution_convert_fusion.3
  287.9 149.1 %all-gather.23.cloned.1.call-done = bf16[4096,1376]{0,1:T(8,128)(2,1)} async-done(((bf16[256,1376]{0,1:T(8,128)(2,1)}), bf16[4096,1376]{0,1:T(8,128)(2,1)}) %all-gather.23.cloned.1.call-update) | async-done | bytes 11272208 | tf_op jit(solution)/shard_map/all_gather | solution.py:64
  437.0 5.9 convolution_convert_fusion.2
  443.1 149.6 %all-gather.25.cloned.1.call-done = bf16[1376,4096]{1,0:T(8,128)(2,1)} async-done(((bf16[1376,256]{1,0:T(8,128)(2,1)}), bf16[1376,4096]{1,0:T(8,128)(2,1)}) %all-gather.25.cloned.1.call-update) | async-done | bytes 11272208 | tf_op jit(solution)/shard_map/all_gather | solution.py:69
  592.7 10.3 %convolution_convert_fusion = bf16[128,4096]{1,0:T(8,128)(2,1)} fusion(bf16[1376,4096]{1,0:T(8,128)(2,1)} %all-gather.25.cloned.1.call-done, bf16[128,1376]{0,1:T(8,128)(2,1)S(1)} %convolution_convert_fusion.2, f32[1,128,1376]{1,2,0:T(8,128)S(1)} %convert_bitcast_fusion, f32[1,128,1376]{1,2,0:T(8,128)S(1)} %convert_bitcast_fusion.1, ...), kind=kOutput, calls=%fused_computation | convolution fusion | flops 1457455104 | bytes 14478336 | tf_op jit(solution)/shard_map/dot_general | solution.py:172
  603.0 45.8 %reduce-scatter.5.cloned.1.call-done = bf16[128,512]{1,0:T(8,128)(2,1)} async-done(((bf16[128,4096]{1,0:T(8,128)(2,1)}), bf16[128,512]{1,0:T(8,128)(2,1)}) %reduce-scatter.5.cloned.1.call-update) | async-done | bytes 131088 | tf_op jit(solution)/shard_map/reduce_scatter | solution.py:175
  648.8 1.6 add_convert_fusion
  (70 shorter events, 7.3 us)
Async XLA Ops:
  7.4 28.4 %copy-start.1 = (bf16[256,256]{1,0:T(8,128)(2,1)S(1)}, bf16[256,256]{1,0:T(8,128)(2,1)}, u32[]{:S(2)}) copy-start(bf16[256,256]{1,0:T(8,128)(2,1)} %param.25) | copy-start | bytes 393220
  7.4 42.9 %copy-start = (bf16[128,512]{1,0:T(8,128)(2,1)S(1)}, bf16[128,512]{1,0:T(8,128)(2,1)}, u32[]{:S(2)}) copy-start(bf16[128,512]{1,0:T(8,128)(2,1)} %param.17) | copy-start | bytes 393220
  7.4 99.3 %all-gather.17.cloned.1.call-start = ((), (), s32[]{:S(2)}) async-start(), calls=%async_computation.3 | async-start | bytes 2621440 | tf_op jit(solution)/shard_map/all_gather | solution.py:25
  21.7 88.1 %all-gather.15.cloned.1.call-start = ((), (), s32[]{:S(2)}) async-start(), calls=%async_computation.2 | async-start | bytes 2621440 | tf_op jit(solution)/shard_map/all_gather | solution.py:25
  35.7 37.1 %copy-start.3 = (f32[4096]{0:T(1024)S(1)}, f32[4096]{0:T(1024)}, u32[]{:S(2)}) copy-start(f32[4096]{0:T(1024)} %param.18) | copy-start | bytes 49156
  35.8 93.8 %all-gather.19.cloned.1.call-start = ((), (), s32[]{:S(2)}) async-start(), calls=%async_computation.4 | async-start | bytes 2621440 | tf_op jit(solution)/shard_map/all_gather | solution.py:25
  50.2 121.3 %reduce-scatter.3.cloned.1.call-start = ((), (), s32[]{:S(2)}) async-start(), calls=%async_computation.5 | async-start | bytes 1179648 | tf_op jit(solution)/shard_map/reduce_scatter | solution.py:153
  86.2 1.0 copy-start.6
  111.6 1.1 copy-start.7
  111.6 1.1 copy-start.8
  132.6 2.9 copy-start.9
  137.4 1.8 copy-start.4
  137.4 1.8 copy-start.5
  137.5 144.5 %all-gather.21.cloned.1.call-start = ((), (), s32[]{:S(2)}) async-start(), calls=%async_computation.6 | async-start | bytes 11976704 | tf_op jit(solution)/shard_map/all_gather | solution.py:64
  138.0 298.9 %all-gather.23.cloned.1.call-start = ((), (), s32[]{:S(2)}) async-start(), calls=%async_computation.7 | async-start | bytes 11976704 | tf_op jit(solution)/shard_map/all_gather | solution.py:64
  138.6 454.0 %all-gather.25.cloned.1.call-start = ((), (), s32[]{:S(2)}) async-start(), calls=%async_computation.8 | async-start | bytes 11976704 | tf_op jit(solution)/shard_map/all_gather | solution.py:69
  139.2 509.6 %reduce-scatter.5.cloned.1.call-start = ((), (), s32[]{:S(2)}) async-start(), calls=%async_computation.9 | async-start | bytes 1179648 | tf_op jit(solution)/shard_map/reduce_scatter | solution.py:175
  202.1 0.7 copy-start.2
  442.9 149.7 %copy-start.10 = (f32[1376]{0:T(1024)S(1)}, f32[1376]{0:T(1024)}, u32[]{:S(2)}) copy-start(f32[1376]{0:T(1024)} %param.32) | copy-start | bytes 16516
  442.9 149.7 %copy-start.11 = (f32[1376]{0:T(1024)S(1)}, f32[1376]{0:T(1024)}, u32[]{:S(2)}) copy-start(f32[1376]{0:T(1024)} %param.31) | copy-start | bytes 16516
Sparse Core Ops, SparseCore 0:
  21.8 37.3 all-gather.16
  61.1 33.2 all-gather.14
  96.2 33.3 all-gather.18
  137.6 33.8 reduce-scatter.2
  603.1 45.6 reduce-scatter.4
Sparse Core Ops, SparseCore 1:
  139.7 142.2 all-gather.20
  283.5 153.4 all-gather.22
  438.6 154.0 all-gather.24
where the time goes:
time: 661 us; the launch traced here: 658 us
  waiting for transfers between devices  473 us (72%)
  blocking collectives  126 us (19%)
  matrix products  25.5 us (4%)
  between operations  15.2 us (2%)
  local copies, waits for them, and re-layouts  11.7 us (2%)
    all_gather x2, waiting for transfers between devices, folded(): lax.all_gather(part, axis, axis=dim, tiled=True)  227 us
    all_gather x1, waiting for transfers between devices, gathered_then(): return work(lax.all_gather(shard, axis, axis=dim, tiled=True), jnp.int32(0))  150 us
    all_gather x13, blocking collectives, stacked_from(): blocks = lax.all_gather(blocks, axes[k], axis=0, tiled=True)  126 us
    reduce_scatter x1, waiting for transfers between devices, body(): lax.psum_scatter(down_terms.astype(jnp.bfloat16), TP, scatter_dimension=1...  45.8 us
    reduce_scatter x1, waiting for transfers between devices, body(): lax.psum_scatter(merge_terms.astype(jnp.bfloat16), TP, scatter_dimension=...  32.1 us
    all_gather x3, waiting for transfers between devices, stacked_from(): blocks = lax.all_gather(blocks, axes[k], axis=0, tiled=True)  16.6 us
  transfers between devices with their start and end apart: 8, of which 6 were waited for; matrix products, arithmetic and copies ran while one was open for 4% of the time, Pallas kernels for 0%

commit v1 on v0

v1 whole, which is shorter than its diff:
```python
import jax
import jax.numpy as jnp
from jax import lax
from jax.experimental import pallas as pl
from jax.experimental.pallas import tpu as pltpu
from jax.sharding import Mesh
from jax.sharding import PartitionSpec as P

TP = ("tp_0", "tp_1")
FS = ("fs_0", "fs_1")
REP_FS = ("rep", "fs_0", "fs_1")
MESH = pl.DeviceIdType.MESH
EPS = 1e-06
F32 = jnp.float32
BF16 = jnp.bfloat16
SEMS = 160


def gelu(v):
    return 0.5 * v * (1.0 + lax.erf(v * 0.7071067811865476))


def lanes_of(n):
    return lax.broadcasted_iota(jnp.int32, (n, 128), 1)


def kernel(
    tok, gains, gp, vp, vgain, smix, sbias, hgain, mp, gu, vu, cv, dn,
    out,
    XG, HG, XS, WGP, WVP, WMP, WGU, WVU, WDN, SM, SQ, MG, ACT, OP,
    P1, A1, B1, C1, HL1, HR1, FL1, FR1,
    P2, A2, B2, C2, HL2, HR2, FL2, FR2,
    P3, A3, B3, C3, HL3, HR3, FL3, FR3,
    T, CS4, CR4, YA4, YB4, YC4, YHL4, YHR4, YFL4, YFR4,
    CS5, CR5, YA5, YB5, YC5, YHL5, YHR5, YFL5, YFR5,
    ssem, rsem, lsem,
):
    r, z, x, y, c = (lax.axis_index(a) for a in ("rep", "fs_0", "fs_1", "tp_0", "tp_1"))
    other = 1 - c
    f = 4 * z + x
    inner = gu.shape[1]
    depth = gains.shape[1] * gains.shape[2]

    def at(z_=None, x_=None, y_=None, c_=None, r_=None):
        pick = lambda new, old: old if new is None else new
        return (pick(r_, r), pick(z_, z), pick(x_, x), pick(y_, y), pick(c_, c))

    up = lambda v: lax.rem(v + 1, 4)
    down = lambda v: lax.rem(v + 3, 4)
    far = lambda v: lax.rem(v + 2, 4)

    zr = 4 * r + z
    zu, zd = lax.rem(zr + 1, 8), lax.rem(zr + 7, 8)
    z_up = at(r_=zu // 4, z_=lax.rem(zu, 4))
    z_dn = at(r_=zd // 4, z_=lax.rem(zd, 4))
    x_up, x_dn = at(x_=up(x)), at(x_=down(x))
    y_up, y_dn = at(y_=up(y)), at(y_=down(y))
    mate = at(c_=other)
    fs_peers = []
    for i in range(1, 16):
        g = lax.rem(f + i, 16)
        fs_peers.append(at(z_=g // 4, x_=lax.rem(g, 4)))

    barrier = pltpu.get_barrier_semaphore()
    greet = fs_peers + [at(x_=jnp.int32(k), c_=other) for k in range(4)]
    greet += [y_up, y_dn, z_up, z_dn]
    for peer in greet:
        pl.semaphore_signal(barrier, inc=1, device_id=peer, device_id_type=MESH)
    pl.semaphore_wait(barrier, len(greet))

    started = []
    count = [0]

    def take(n=1):
        first = count[0]
        count[0] += n
        return first

    def remote(src, dst, s, k, peer):
        return pltpu.make_async_remote_copy(
            src_ref=src, dst_ref=dst, send_sem=ssem.at[s], recv_sem=rsem.at[k],
            device_id=peer, device_id_type=MESH,
        )

    def send(src, dst, k, peer):
        copy = remote(src, dst, k, k, peer)
        copy.start()
        started.append(copy)

    def recv(dst, k):
        remote(dst, dst, 0, k, mate).wait_recv()

    half = dn.shape[0] // 2
    chunks = [
        (gp, WGP, 0, 256, 128), (vp, WVP, 0, 256, 128), (mp, WMP, 0, 256, 128),
        (gu, WGU, 0, 128, 64), (gu, WGU, 128, 128, 64),
        (vu, WVU, 0, 128, 64), (vu, WVU, 128, 128, 64),
        (dn, WDN, 0, half, 352), (dn, WDN, half, half, 352),
    ]
    zk = [take(4) for _ in chunks]

    def z_own(i):
        src, buf, at0, n, _ = chunks[i]
        rows = pl.ds(at0, n)
        send(src.at[rows], buf.at[z, rows], zk[i], z_up)
        send(src.at[rows], buf.at[z, rows], zk[i] + 1, z_dn)
        pltpu.make_async_copy(src.at[rows], buf.at[z, rows], lsem.at[i]).start()

    def z_fwd(i):
        _, buf, at0, n, cut = chunks[i]
        lo, hi = down(z), up(z)
        recv(buf.at[lo, pl.ds(at0, n)], zk[i])
        a = pl.ds(at0, cut)
        send(buf.at[lo, a], buf.at[lo, a], zk[i] + 2, z_up)
        recv(buf.at[hi, pl.ds(at0, n)], zk[i] + 1)
        b = pl.ds(at0 + cut, n - cut)
        send(buf.at[hi, b], buf.at[hi, b], zk[i] + 3, z_dn)

    def z_fin(i):
        src, buf, at0, n, cut = chunks[i]
        rows = pl.ds(at0, n)
        recv(buf.at[far(z), pl.ds(at0, cut)], zk[i] + 2)
        recv(buf.at[far(z), pl.ds(at0 + cut, n - cut)], zk[i] + 3)
        pltpu.make_async_copy(src.at[rows], buf.at[z, rows], lsem.at[i]).wait()

    for k in range(4):
        WDN[k, dn.shape[0] :, :] = jnp.zeros((inner - dn.shape[0], 256), BF16)

    swaps = []
    kx = take(4)
    me = 2 * y + c
    to_me = x // 2 == c
    for j in range(2):
        for h in range(2):
            xt = 2 * c + j
            mine = jnp.logical_and(xt == x, c == h)
            cols = slice(j * 256 + h * 128, j * 256 + h * 128 + 128)
            copy = remote(
                tok.at[:, cols], XG.at[2 * y + h, x], kx + 2 * j + h, kx + x,
                at(x_=xt, c_=jnp.int32(h)),
            )

            swaps.append((mine, copy))

            @pl.when(jnp.logical_not(mine))
            def _():
                copy.start()

            @pl.when(mine)
            def _():
                XG[2 * y + h, x] = tok[:, cols]

    z_own(0)
    z_own(1)
    z_own(2)
    km = take(15)
    for i in range(15):
        send(smix, SM.at[f], km + i, fs_peers[i])
    SM[f] = smix[...]

    for j in range(4):

        @pl.when(jnp.logical_not(jnp.logical_and(x == j, to_me)))
        def _():
            recv(XG.at[me, j], kx + j)

    def y_start(buf, k):
        send(buf.at[me], buf.at[me], k, y_up)
        send(buf.at[me], buf.at[me], k + 1, y_dn)
        send(buf.at[me], buf.at[me], k + 2, mate)

    lo_y, hi_y, far_y = 2 * down(y) + c, 2 * up(y) + c, 2 * far(y) + c
    a2, b2 = pl.ds(0, 2), pl.ds(2, 2)

    def y_mid(buf, k):
        recv(buf.at[lo_y], k)
        send(buf.at[lo_y, a2], buf.at[lo_y, a2], k + 3, y_up)
        recv(buf.at[hi_y], k + 1)
        send(buf.at[hi_y, b2], buf.at[hi_y, b2], k + 4, y_dn)
        send(buf.at[lo_y], buf.at[lo_y], k + 5, mate)
        send(buf.at[hi_y], buf.at[hi_y], k + 6, mate)

    def y_end(buf, k):
        recv(buf.at[far_y, a2], k + 3)
        send(buf.at[far_y, a2], buf.at[far_y, a2], k + 7, mate)
        recv(buf.at[far_y, b2], k + 4)
        send(buf.at[far_y, b2], buf.at[far_y, b2], k + 8, mate)

    def y_last(buf, k):
        recv(buf.at[2 * y + other], k + 2)
        recv(buf.at[2 * down(y) + other], k + 5)
        recv(buf.at[2 * up(y) + other], k + 6)
        recv(buf.at[2 * far(y) + other, a2], k + 7)
        recv(buf.at[2 * far(y) + other, b2], k + 8)

    def scaled(buf, which):
        gain = jnp.concatenate([gains[which, pl.ds(4 * k + x, 1), :] for k in range(4)], axis=1)

        def block(b, _):
            rows = jnp.concatenate([buf[i, b] for i in range(8)], axis=1).astype(F32)
            SQ[b] = jnp.broadcast_to(jnp.sum(rows * rows, axis=-1, keepdims=True), (128, 128))
            XS[pl.ds(pl.multiple_of(b * 128, 128), 128), :] = (rows * gain).astype(BF16)
            return 0

        lax.fori_loop(0, 4, block, 0)

    ky = take(9)
    y_start(XG, ky)
    z_fwd(0)
    y_mid(XG, ky)
    z_fwd(1)
    y_end(XG, ky)
    z_fwd(2)
    z_own(3)
    z_own(4)
    y_last(XG, ky)

    scaled(XG, 0)
    z_fin(0)
    z_fin(1)
    for w, W in ((0, WGP), (1, WVP)):
        prod = jnp.dot(XS[...], W[...].reshape(1024, 256), preferred_element_type=F32)
        P1[:, :, w * 256 : w * 256 + 256] = prod.reshape(4, 128, 256)
    P1[:, :, 512:640] = SQ[...]

    def enc(v, edge):
        if edge is None:
            return v.astype(BF16)
        m = v.shape[1] - 128
        last = v[:, m:]
        low = last - last.astype(BF16).astype(F32)
        last = jnp.where(lanes_of(v.shape[0]) >= (edge + 128) // 2, low, last)
        return jnp.concatenate([v[:, :m].astype(BF16), last.astype(BF16)], axis=1)

    def dec(v, edge):
        v = v.astype(F32)
        if edge is None:
            return v
        m = v.shape[1] - 128
        last, lane = v[:, m:], lanes_of(v.shape[0])
        keep = jnp.logical_or(lane == edge, lane == (edge + 128) // 2)
        total = jnp.sum(jnp.where(keep, last, 0.0), axis=-1, keepdims=True)
        last = jnp.where(lane < edge, last, total)
        return jnp.concatenate([v[:, :m], last], axis=1) if m else last

    def row_loop(n, fn):
        def step(i, _):
            fn(pl.ds(pl.multiple_of(i * 16, 16), 16))
            return 0

        lax.fori_loop(0, n // 16, step, 0)

    def shifted(rows, by):
        return pl.ds(pl.multiple_of(rows.start + by, 16), 16)

    def rs_first(p, A, HL, HR, k, edge):
        def conv(rows):
            A[rows, :] = enc(p[far(x), rows, :], edge)

        row_loop(128, conv)
        send(A.at[pl.ds(0, 64)], HL, k, x_up)
        send(A.at[pl.ds(64, 64)], HR, k + 1, x_dn)

    def rs_second(p, B, C, HL, HR, FL, FR, k, edge):
        u, d = up(x), down(x)
        recv(HL, k)

        def left(rows):
            low = shifted(rows, 64)
            B[rows, :] = enc(p[u, rows, :] + dec(HL[rows, :], edge), edge)
            B[low, :] = enc(p[u, low, :], edge)

        row_loop(64, left)
        send(B, FL, k + 2, x_up)
        recv(HR, k + 1)

        def right(rows):
            low = shifted(rows, 64)
            C[low, :] = enc(p[d, low, :] + dec(HR[rows, :], edge), edge)
            C[rows, :] = enc(p[d, rows, :], edge)

        row_loop(64, right)
        send(C, FR, k + 3, x_dn)

    def rs_wait(FL, FR, k):
        recv(FL, k + 2)
        recv(FR, k + 3)

    k1 = take(4)
    rs_first(P1, A1, HL1, HR1, k1, 0)
    z_fwd(3)
    z_own(5)
    rs_second(P1, B1, C1, HL1, HR1, FL1, FR1, k1, 0)
    for i in range(15):
        recv(SM.at[lax.rem(f + 15 - i, 16)], km + i)
    rs_wait(FL1, FR1, k1)

    total = P1[x] + dec(FL1[...], 0) + dec(FR1[...], 0)
    rs = lax.rsqrt(total[:, 512:513] / depth + EPS)
    eye = lax.broadcasted_iota(jnp.int32, (128, 128), 0) == lanes_of(128)
    for h in range(2):
        cols = slice(h * 128, h * 128 + 128)
        gated = gelu((rs * total[:, cols]).astype(BF16).astype(F32))
        spread = gelu((rs * total[:, 256 + h * 128 : 384 + h * 128]).astype(BF16).astype(F32))
        spread = spread * lax.rsqrt(jnp.mean(spread * spread, axis=-1, keepdims=True) + EPS)
        spread = (spread * vgain[h : h + 1, :]).astype(BF16)
        matrix = SM[:, h].astype(F32).reshape(128, 128).astype(BF16)
        mixed = jnp.dot(matrix, spread, preferred_element_type=F32)
        bias = jnp.broadcast_to(sbias[h : h + 1, :], (128, 128))
        mixed = mixed + jnp.sum(jnp.where(eye, bias, 0.0), axis=-1, keepdims=True)
        joined = gated * mixed
        joined = joined * lax.rsqrt(jnp.mean(joined * joined, axis=-1, keepdims=True) + EPS)
        MG[x, :, cols] = (joined * hgain[h : h + 1, :]).astype(BF16)

    ra, rb = pl.ds(0, 64), pl.ds(64, 64)

    def x_start(buf, k):
        send(buf.at[x], buf.at[x], k, x_up)
        send(buf.at[x], buf.at[x], k + 1, x_dn)

    def x_mid(buf, k):
        recv(buf.at[down(x)], k)
        send(buf.at[down(x), ra], buf.at[down(x), ra], k + 2, x_up)
        recv(buf.at[up(x)], k + 1)
        send(buf.at[up(x), rb], buf.at[up(x), rb], k + 3, x_dn)

    def x_last(buf, k):
        recv(buf.at[far(x), ra], k + 2)
        recv(buf.at[far(x), rb], k + 3)

    k2 = take(4)
    x_start(MG, k2)
    x_mid(MG, k2)
    z_fwd(4)
    z_own(6)
    z_fin(2)
    x_last(MG, k2)

    def cy_first(lhs, W, CS, CR, k):
        for n, yt in enumerate((far(y), up(y), down(y), y)):
            prod = jnp.dot(lhs(), W[yt], preferred_element_type=F32)
            T[n] = jnp.where(c == 0, prod[:, :128], prod[:, 128:])
            CS[n] = jnp.where(c == 0, prod[:, 128:], prod[:, :128]).astype(BF16)
            send(CS.at[n], CR.at[n], k + n, mate)

    def cy_second(CR, YA, YHL, YHR, k):
        recv(CR.at[0], k)
        YA[...] = (T[0] + CR[0].astype(F32)).astype(BF16)
        send(YA.at[pl.ds(0, 256)], YHL, k + 4, y_up)
        send(YA.at[pl.ds(256, 256)], YHR, k + 5, y_dn)
        for n in (1, 2, 3):
            recv(CR.at[n], k + n)
            T[n] = T[n] + CR[n].astype(F32)

    def cy_third(YB, YC, YHL, YHR, YFL, YFR, k):
        recv(YHL, k + 4)
        YB[0:256, :] = (T[1, 0:256, :] + YHL[...].astype(F32)).astype(BF16)
        YB[256:512, :] = T[1, 256:512, :].astype(BF16)
        send(YB, YFL, k + 6, y_up)
        recv(YHR, k + 5)
        YC[256:512, :] = (T[2, 256:512, :] + YHR[...].astype(F32)).astype(BF16)
        YC[0:256, :] = T[2, 0:256, :].astype(BF16)
        send(YC, YFR, k + 7, y_dn)

    def cy_last(YFL, YFR, k):
        recv(YFL, k + 6)
        recv(YFR, k + 7)
        return T[3] + YFL[...].astype(F32) + YFR[...].astype(F32)

    k3 = take(8)
    cy_first(lambda: MG[...].reshape(512, 256), WMP, CS4, CR4, k3)
    cy_second(CR4, YA4, YHL4, YHR4, k3)
    cy_third(YB4, YC4, YHL4, YHR4, YFL4, YFR4, k3)
    z_fwd(5)
    z_own(7)
    branch = cy_last(YFL4, YFR4, k3)
    hidden = (XG[me].reshape(512, 128).astype(F32) + branch).astype(BF16)
    HG[me] = hidden.reshape(4, 128, 128)

    kh = take(9)
    y_start(HG, kh)
    y_mid(HG, kh)
    y_end(HG, kh)
    z_fin(3)
    z_fin(4)
    y_last(HG, kh)
    scaled(HG, 1)

    def project(W, p):
        def cut(cols, n):
            w = W[:, :, cols].reshape(1024, n)
            prod = jnp.dot(XS[...], w, preferred_element_type=F32)
            p[:, :, cols] = prod.reshape(4, 128, n)

        def step(i, _):
            cut(pl.ds(pl.multiple_of(i * 256, 256), 256), 256)
            return 0

        lax.fori_loop(0, inner // 256, step, 0)
        if inner % 256:
            cut(pl.ds(inner - inner % 256, inner % 256), inner % 256)

    project(WGU, P2)
    edge = 128 - (inner - dn.shape[0])
    last = P2[:, :, inner - 128 : inner]
    lane = lax.broadcasted_iota(jnp.int32, (4, 128, 128), 2)
    P2[:, :, inner - 128 : inner] = jnp.where(lane < edge, last, SQ[...])
    k4, k5 = take(4), take(4)
    rs_first(P2, A2, HL2, HR2, k4, edge)
    z_fwd(6)
    z_own(8)
    z_fin(5)
    z_fin(6)
    project(WVU, P3)
    rs_second(P2, B2, C2, HL2, HR2, FL2, FR2, k4, edge)
    rs_first(P3, A3, HL3, HR3, k5, None)
    z_fwd(7)
    rs_wait(FL2, FR2, k4)
    rs_second(P3, B3, C3, HL3, HR3, FL3, FR3, k5, None)
    z_fwd(8)
    rs_wait(FL3, FR3, k5)

    at_end = slice(inner - 128, inner)
    sq = P2[x, :, at_end] + dec(FL2[:, at_end], edge) + dec(FR2[:, at_end], edge)
    rs2 = lax.rsqrt(sq[:, 127:128] / depth + EPS)
    row = lax.broadcasted_iota(jnp.int32, (128, 128), 0)

    def conv_tile(i, _):
        cols = pl.ds(pl.multiple_of(i * 128, 128), 128)

        def one(p, FL, FR, w):
            v = p[x, :, cols] + FL[:, cols].astype(F32) + FR[:, cols].astype(F32)
            v = (rs2 * v).astype(BF16).astype(F32)
            prev = jnp.where(row == 0, 0.0, pltpu.roll(v, 1, axis=0))
            after = jnp.where(row == 127, 0.0, pltpu.roll(v, 127, axis=0))
            k = cv[w, :, cols]
            return k[3:4] + prev * k[0:1] + v * k[1:2] + after * k[2:3]

        active = gelu(one(P2, FL2, FR2, 0)) * one(P3, FL3, FR3, 1)
        ACT[x, :, cols] = active.astype(BF16)
        return 0

    lax.fori_loop(0, inner // 128, conv_tile, 0)

    k6 = take(4)
    x_start(ACT, k6)
    x_mid(ACT, k6)
    z_fin(7)
    z_fin(8)
    x_last(ACT, k6)

    k7 = take(8)
    cy_first(lambda: ACT[...].reshape(512, inner), WDN, CS5, CR5, k7)
    cy_second(CR5, YA5, YHL5, YHR5, k7)
    cy_third(YB5, YC5, YHL5, YHR5, YFL5, YFR5, k7)
    change = cy_last(YFL5, YFR5, k7)
    result = (HG[me].reshape(512, 128).astype(F32) + change).astype(BF16)
    OP[...] = result.reshape(4, 128, 128)

    ko = take(4)
    place = lax.rem(x, 2)
    to_cols = pl.ds(pl.multiple_of(place * 256 + c * 128, 128), 128)
    for j in range(4):
        mine = jnp.logical_and(x == j, to_me)
        copy = remote(
            OP.at[j], out.at[:, to_cols], ko + j, ko + 2 * place + c,
            at(x_=jnp.int32(j), c_=x // 2),
        )
        swaps.append((mine, copy))

        @pl.when(jnp.logical_not(mine))
        def _():
            copy.start()

        @pl.when(mine)
        def _():
            out[:, to_cols] = OP[j]

    for j in range(2):
        for h in range(2):

            @pl.when(jnp.logical_not(jnp.logical_and(2 * c + j == x, c == h)))
            def _():
                recv(out.at[:, pl.ds(j * 256 + h * 128, 128)], ko + 2 * j + h)

    for copy in started:
        copy.wait_send()
    for mine, copy in swaps:

        @pl.when(jnp.logical_not(mine))
        def _():
            copy.wait_send()


def body(
    tokens, mixer_gain, gate_proj, value_proj, value_gain, spatial_mix, spatial_bias,
    head_gain, merge_proj, ffn_gain, gate_up, value_up, gate_kernel, value_kernel,
    gate_offset, value_offset, down_proj,
):
    inner = gate_up.shape[1]
    wide = -(-inner // 128) * 128
    extra = ((0, 0), (0, wide - inner))
    gains = jnp.stack([mixer_gain, ffn_gain]).reshape(2, 16, 256)
    conv = jnp.stack([
        jnp.concatenate([gate_kernel, gate_offset[None]]),
        jnp.concatenate([value_kernel, value_offset[None]]),
    ])
    conv = jnp.pad(conv, ((0, 0), *extra))
    gate_up, value_up = jnp.pad(gate_up, extra), jnp.pad(value_up, extra)
    vm = lambda shape, dtype=BF16: pltpu.VMEM(shape, dtype)

    def rs_x(n):
        return [
            vm((4, 128, n), F32), *[vm((128, n))] * 3, *[vm((64, n))] * 2, *[vm((128, n))] * 2,
        ]

    def rs_y():
        return [
            *[vm((4, 512, 128))] * 2, *[vm((512, 128))] * 3, *[vm((256, 128))] * 2,
            *[vm((512, 128))] * 2,
        ]

    in_vmem = pl.BlockSpec(memory_space=pltpu.VMEM)
    left = pl.BlockSpec(memory_space=pl.ANY)
    call = pl.pallas_call(
        kernel,
        out_shape=jax.ShapeDtypeStruct(tokens.shape, tokens.dtype),
        in_specs=[
            in_vmem, in_vmem, left, left, in_vmem, in_vmem, in_vmem, in_vmem, left,
            left, left, in_vmem, left,
        ],
        out_specs=in_vmem,
        scratch_shapes=[
            vm((8, 4, 128, 128)), vm((8, 4, 128, 128)), vm((512, 1024)),
            vm((4, 256, 256)), vm((4, 256, 256)), vm((4, 256, 256)),
            vm((4, 256, wide)), vm((4, 256, wide)), vm((4, wide, 256)),
            vm((16, 2, 8, 128)), vm((4, 128, 128), F32), vm((4, 128, 256)),
            vm((4, 128, wide)), vm((4, 128, 128)),
            *rs_x(640), *rs_x(wide), *rs_x(wide),
            vm((4, 512, 128), F32), *rs_y(), *rs_y(),
            pltpu.SemaphoreType.DMA((SEMS,)), pltpu.SemaphoreType.DMA((SEMS,)),
            pltpu.SemaphoreType.DMA((9,)),
        ],
        compiler_params=pltpu.CompilerParams(
            collective_id=0, has_side_effects=True, vmem_limit_bytes=58 << 20
        ),
        name="layer",
    )
    return call(
        tokens, gains, gate_proj, value_proj, value_gain, spatial_mix, spatial_bias,
        head_gain, merge_proj, gate_up, value_up, conv, down_proj,
    )


def solution(mesh):
    finer = Mesh(
        mesh.devices.reshape(mesh.shape["rep"], 4, 4, 4, 2), ("rep", "fs_0", "fs_1", "tp_0", "tp_1")
    )
    return jax.shard_map(
        body,
        mesh=finer,
        in_specs=(
            P(REP_FS, TP), P(), P(FS, TP), P(FS, TP), P(TP, None), P(TP, FS, None),
            P(TP, None), P(TP, None), P(TP, FS), P(), P(FS, TP), P(FS, TP), P(None, TP),
            P(None, TP), P(TP), P(TP), P(TP, FS),
        ),
        out_specs=P(REP_FS, TP),
        check_vma=False,
    )
```

time: 661 us -> 152 us (0.23)
  waiting for transfers between devices: 473 us -> 0 us
  Pallas kernels: 0 us -> 143 us
  blocking collectives: 126 us -> 0 us
  matrix products: 25.5 us -> 0 us
  between operations: 15.2 us -> 0.08 us
    all_gather x6 -> x0, waiting for transfers between devices: 394 us -> none  [the longest x2 227 us: folded(): lax.all_gather(part, axis, axis=dim, tiled=True)]
    pallas_call x0 -> x1, Pallas kernels: none -> 143 us  [body(): call(tokens, gains, gate_proj, value_proj, value_gain, spatial_mix, spati...]
    all_gather x13 -> x0, blocking collectives: 126 us -> none  [stacked_from(): blocks = lax.all_gather(blocks, axes[k], axis=0, tiled=True)]
    reduce_scatter x2 -> x0, waiting for transfers between devices: 77.9 us -> none  [the longest x1 45.8 us: body(): lax.psum_scatter(down_terms.astype(jnp.bfloat16), TP, scatter_dimension=1...]
    dot_general x7 -> x0, matrix products: 25.5 us -> none  [the longest x4 13.2 us: add_block(): return total + jnp.dot(columns, piece, preferred_element_type=jnp.float32)]
    transpose x6 -> x0, local copies, waits for them, and re-layouts: 9.44 us -> none  [the longest x5 6.58 us: stacked_from(): blocks.transpose(*turned, *range(len(sequence), blocks.ndim))]
  transfers between devices with their start and end apart: 8 -> 0, of which waited for: 6 -> 0; matrix products, arithmetic and copies ran while one was open for 4% -> 0% of each run, Pallas kernels for 0% -> 0%
where the time goes in v1:
time: 152 us
  Pallas kernels  143 us (94%)
  local copies, waits for them, and re-layouts  7.11 us (5%)
    pallas_call x1, Pallas kernels, body(): call(tokens, gains, gate_proj, value_proj, value_gain, spatial_mix, spati...  143 us
    unnamed x15, local copies, waits for them, and re-layouts  4.49 us

profile of v1, /device:TPU:57, one launch (start us, length us, event | category | flops | bytes accessed | tf_op | source)
XLA Modules:
  0.0 151.7 jit_solution(6779688977013605886)
XLA Ops:
  0.0 0.0 copy-start.3
  0.0 0.7 stack.19
  0.7 0.0 copy-done.3
  0.8 0.6 pad_maximum_fusion.gains
  1.4 1.4 copy.18
  2.8 0.0 copy-start
  2.8 0.9 pad.11.gu
  3.8 0.4 copy-done
  4.2 0.3 copy.19
  4.5 0.0 copy-start.4
  4.5 0.0 copy-start.5
  4.5 0.0 copy-start.2
  4.6 0.9 pad.12.vu
  5.5 0.0 copy-done.4
  5.5 0.0 copy-start.1
  5.5 0.0 copy-done.5
  5.5 0.0 copy-done.2
  5.5 0.7 copy-done.1
  6.2 0.6 select_maximum_fusion.cv
  6.9 143.2 %layer.1 = bf16[128,512]{1,0:T(8,128)(2,1)} custom-call(bf16[128,512]{1,0:T(8,128)(2,1)} %tok.1, f32[2,16,256]{2,1,0:T(8,128)} %pad_maximum_fusion.gains, bf16[256,256]{1,0:T(8,128)(2,1)} %gp.1, bf16[256,256]{1,0:T(8,128)(2,1)} %vp.1, f32[2,128]{1,0:T(2,128)} %vgain.1, bf16[2,8,128]{2,1,0:T(8,128)(2,1)} %smix.1, f32[2,128]{1,0:T(2,128)} %sbias.1, ...), custom_call_target="tpu_custom_call" | custom-call | tf_op jit(solution)/shard_map/layer/pallas_call | solution.py:549
  150.1 1.6 %copy.21 = bf16[128,512]{1,0:T(8,128)(2,1)} copy(bf16[128,512]{1,0:T(8,128)(2,1)} %layer.1) | data formatting | bytes 262144
  (4 shorter events, 0.0 us)
Async XLA Ops:
  0.0 0.7 copy-start.3
  2.8 1.4 copy-start
  4.5 1.0 copy-start.4
  4.5 1.0 copy-start.5
  4.5 1.0 copy-start.2
  5.5 0.7 copy-start.1

commit v2 on v1

--- a/solution.py
+++ b/solution.py
@@ -25,9 +25,9 @@
 
 
 def kernel(
-    tok, gains, gp, vp, vgain, smix, sbias, hgain, mp, gu, vu, cv, dn,
+    tok, mgain, fgain, gp, vp, vgain, smix, sbias, hgain, mp, gu, vu, gk, vk, go, vo, dn,
     out,
-    XG, HG, XS, WGP, WVP, WMP, WGU, WVU, WDN, SM, SQ, MG, ACT, OP,
+    cv, XG, HG, XS, WGP, WVP, WMP, WGU, WVU, WDN, SM, SQ, MG, ACT, OP,
     P1, A1, B1, C1, HL1, HR1, FL1, FR1,
     P2, A2, B2, C2, HL2, HR2, FL2, FR2,
     P3, A3, B3, C3, HL3, HR3, FL3, FR3,
@@ -38,8 +38,9 @@
     r, z, x, y, c = (lax.axis_index(a) for a in ("rep", "fs_0", "fs_1", "tp_0", "tp_1"))
     other = 1 - c
     f = 4 * z + x
-    inner = gu.shape[1]
-    depth = gains.shape[1] * gains.shape[2]
+    units = dn.shape[0]
+    inner = cv.shape[2]
+    depth = mgain.shape[0]
 
     def at(z_=None, x_=None, y_=None, c_=None, r_=None):
         pick = lambda new, old: old if new is None else new
@@ -90,11 +91,11 @@
     def recv(dst, k):
         remote(dst, dst, 0, k, mate).wait_recv()
 
-    half = dn.shape[0] // 2
+    half = units // 2
     chunks = [
         (gp, WGP, 0, 256, 128), (vp, WVP, 0, 256, 128), (mp, WMP, 0, 256, 128),
-        (gu, WGU, 0, 128, 64), (gu, WGU, 128, 128, 64),
-        (vu, WVU, 0, 128, 64), (vu, WVU, 128, 128, 64),
+        (gu, WGU, 0, half, 352), (gu, WGU, half, half, 352),
+        (vu, WVU, 0, half, 352), (vu, WVU, half, half, 352),
         (dn, WDN, 0, half, 352), (dn, WDN, half, half, 352),
     ]
     zk = [take(4) for _ in chunks]
@@ -123,8 +124,13 @@
         recv(buf.at[far(z), pl.ds(at0 + cut, n - cut)], zk[i] + 3)
         pltpu.make_async_copy(src.at[rows], buf.at[z, rows], lsem.at[i]).wait()
 
-    for k in range(4):
-        WDN[k, dn.shape[0] :, :] = jnp.zeros((inner - dn.shape[0], 256), BF16)
+    for W in (WGU, WVU, WDN):
+        for k in range(4):
+            W[k, units:, :] = jnp.zeros((inner - units, 256), BF16)
+    for w, kern, off in ((0, gk, go), (1, vk, vo)):
+        cv[w, :, inner - 128 :] = jnp.zeros((4, 128), F32)
+        cv[w, 0:3, 0:units] = kern[...]
+        cv[w, 3:4, 0:units] = off[...].reshape(1, units)
 
     swaps = []
     kx = take(4)
@@ -193,8 +199,9 @@
         recv(buf.at[2 * far(y) + other, a2], k + 7)
         recv(buf.at[2 * far(y) + other, b2], k + 8)
 
-    def scaled(buf, which):
-        gain = jnp.concatenate([gains[which, pl.ds(4 * k + x, 1), :] for k in range(4)], axis=1)
+    def scaled(buf, gains):
+        parts = [gains[pl.ds(pl.multiple_of((4 * k + x) * 256, 256), 256)] for k in range(4)]
+        gain = jnp.concatenate([part.reshape(1, 256) for part in parts], axis=1)
 
         def block(b, _):
             rows = jnp.concatenate([buf[i, b] for i in range(8)], axis=1).astype(F32)
@@ -215,7 +222,7 @@
     z_own(4)
     y_last(XG, ky)
 
-    scaled(XG, 0)
+    scaled(XG, mgain)
     z_fin(0)
     z_fin(1)
     for w, W in ((0, WGP), (1, WVP)):
@@ -384,12 +391,14 @@
     z_fin(3)
     z_fin(4)
     y_last(HG, kh)
-    scaled(HG, 1)
+    scaled(HG, fgain)
 
     def project(W, p):
         def cut(cols, n):
-            w = W[:, :, cols].reshape(1024, n)
-            prod = jnp.dot(XS[...], w, preferred_element_type=F32)
+            w = jnp.concatenate([W[k, cols, :] for k in range(4)], axis=1)
+            prod = lax.dot_general(
+                XS[...], w, (((1,), (1,)), ((), ())), preferred_element_type=F32
+            )
             p[:, :, cols] = prod.reshape(4, 128, n)
 
         def step(i, _):
@@ -401,7 +410,7 @@
             cut(pl.ds(inner - inner % 256, inner % 256), inner % 256)
 
     project(WGU, P2)
-    edge = 128 - (inner - dn.shape[0])
+    edge = 128 - (inner - units)
     last = P2[:, :, inner - 128 : inner]
     lane = lax.broadcasted_iota(jnp.int32, (4, 128, 128), 2)
     P2[:, :, inner - 128 : inner] = jnp.where(lane < edge, last, SQ[...])
@@ -497,16 +506,7 @@
     head_gain, merge_proj, ffn_gain, gate_up, value_up, gate_kernel, value_kernel,
     gate_offset, value_offset, down_proj,
 ):
-    inner = gate_up.shape[1]
-    wide = -(-inner // 128) * 128
-    extra = ((0, 0), (0, wide - inner))
-    gains = jnp.stack([mixer_gain, ffn_gain]).reshape(2, 16, 256)
-    conv = jnp.stack([
-        jnp.concatenate([gate_kernel, gate_offset[None]]),
-        jnp.concatenate([value_kernel, value_offset[None]]),
-    ])
-    conv = jnp.pad(conv, ((0, 0), *extra))
-    gate_up, value_up = jnp.pad(gate_up, extra), jnp.pad(value_up, extra)
+    wide = -(-gate_up.shape[1] // 128) * 128
     vm = lambda shape, dtype=BF16: pltpu.VMEM(shape, dtype)
 
     def rs_x(n):
@@ -526,14 +526,15 @@
         kernel,
         out_shape=jax.ShapeDtypeStruct(tokens.shape, tokens.dtype),
         in_specs=[
-            in_vmem, in_vmem, left, left, in_vmem, in_vmem, in_vmem, in_vmem, left,
-            left, left, in_vmem, left,
+            in_vmem, in_vmem, in_vmem, left, left, in_vmem, in_vmem, in_vmem, in_vmem, left,
+            left, left, in_vmem, in_vmem, in_vmem, in_vmem, left,
         ],
         out_specs=in_vmem,
         scratch_shapes=[
+            vm((2, 4, wide), F32),
             vm((8, 4, 128, 128)), vm((8, 4, 128, 128)), vm((512, 1024)),
             vm((4, 256, 256)), vm((4, 256, 256)), vm((4, 256, 256)),
-            vm((4, 256, wide)), vm((4, 256, wide)), vm((4, wide, 256)),
+            vm((4, wide, 256)), vm((4, wide, 256)), vm((4, wide, 256)),
             vm((16, 2, 8, 128)), vm((4, 128, 128), F32), vm((4, 128, 256)),
             vm((4, 128, wide)), vm((4, 128, 128)),
             *rs_x(640), *rs_x(wide), *rs_x(wide),
@@ -547,8 +548,9 @@
         name="layer",
     )
     return call(
-        tokens, gains, gate_proj, value_proj, value_gain, spatial_mix, spatial_bias,
-        head_gain, merge_proj, gate_up, value_up, conv, down_proj,
+        tokens, mixer_gain, ffn_gain, gate_proj, value_proj, value_gain, spatial_mix,
+        spatial_bias, head_gain, merge_proj, gate_up.T, value_up.T, gate_kernel, value_kernel,
+        gate_offset, value_offset, down_proj,
     )
 
 

time: 152 us -> 146 us (0.961)
  local copies, waits for them, and re-layouts: 7.11 us -> 1.57 us
    unnamed x15 -> x1, local copies, waits for them, and re-layouts: 4.49 us -> 1.57 us
    pad x2 -> x0, local copies, waits for them, and re-layouts: 1.87 us -> none  [body(): gate_up, value_up = (jnp.pad(gate_up, extra), jnp.pad(value_up, extra))]
where the time goes in v2:
time: 146 us; the launch traced here: 145 us
  Pallas kernels  144 us (99%)
  local copies, waits for them, and re-layouts  1.57 us (1%)
    pallas_call x1, Pallas kernels, body(): call(tokens, mixer_gain, ffn_gain, gate_proj, value_proj, value_gain, spa...  144 us

profile of v2, /device:TPU:57, one launch (start us, length us, event | category | flops | bytes accessed | tf_op | source)
XLA Modules:
  0.0 145.1 jit_solution(17736140436896926424)
XLA Ops:
  0.0 143.5 %layer.1 = bf16[128,512]{1,0:T(8,128)(2,1)} custom-call(bf16[128,512]{1,0:T(8,128)(2,1)} %tok.1, f32[4096]{0:T(1024)} %mgain.1, f32[4096]{0:T(1024)} %fgain.1, bf16[256,256]{1,0:T(8,128)(2,1)} %gp.1, bf16[256,256]{1,0:T(8,128)(2,1)} %vp.1, f32[2,128]{1,0:T(2,128)} %vgain.1, bf16[2,8,128]{2,1,0:T(8,128)(2,1)} %smix.1, f32[2,128]{1,0:T(2,128)} %sbias.1, ...), custom_call_target="tpu_custom_call" | custom-call | tf_op jit(solution)/shard_map/layer/pallas_call | solution.py:550
  143.6 1.6 %copy.19 = bf16[128,512]{1,0:T(8,128)(2,1)} copy(bf16[128,512]{1,0:T(8,128)(2,1)} %layer.1) | data formatting | bytes 262144

commit v3 on v2

v3 whole, which is shorter than its diff:
```python
import jax
import jax.numpy as jnp
from jax import lax
from jax.experimental import pallas as pl
from jax.experimental.pallas import tpu as pltpu
from jax.sharding import Mesh
from jax.sharding import PartitionSpec as P

TP = ("tp_0", "tp_1")
FS = ("fs_0", "fs_1")
REP_FS = ("rep", "fs_0", "fs_1")
MESH = pl.DeviceIdType.MESH
EPS = 1e-06
F32 = jnp.float32
BF16 = jnp.bfloat16
SEMS = 192


def gelu(v):
    return 0.5 * v * (1.0 + lax.erf(v * 0.7071067811865476))


def lanes_of(n):
    return lax.broadcasted_iota(jnp.int32, (n, 128), 1)


def kernel(
    tok, mgain, fgain, gp, vp, vgain, smix, sbias, hgain, mp, gu, vu, gk, vk, go, vo, dn,
    out,
    CV0, CV1, XG, HG, XS, SQ, RS, SM, MG, OP,
    WGP, WVP, WMP, WGU0, WVU0, WGU1, WVU1, WDN0, WDN1,
    ACT0, ACT1, T, ACC,
    P1, A1, B1, C1, HL1, HR1, FL1, FR1,
    P2, A2, B2, C2, HL2, HR2, FL2, FR2,
    P3, A3, B3, C3, HL3, HR3, FL3, FR3,
    CS4, CR4, YA4, YB4, YC4, YHL4, YHR4, YFL4, YFR4,
    CS5, CR5, YA5, YB5, YC5, YHL5, YHR5, YFL5, YFR5,
    ssem, rsem, lsem,
):
    r, z, x, y, c = (lax.axis_index(a) for a in ("rep", "fs_0", "fs_1", "tp_0", "tp_1"))
    other = 1 - c
    f = 4 * z + x
    units = dn.shape[0]
    n1 = CV1.shape[2]
    n0 = CV0.shape[2]
    real0 = units - n1
    edge = 128 - (n0 - real0)
    depth = mgain.shape[0]

    def at(z_=None, x_=None, y_=None, c_=None, r_=None):
        pick = lambda new, old: old if new is None else new
        return (pick(r_, r), pick(z_, z), pick(x_, x), pick(y_, y), pick(c_, c))

    up = lambda v: lax.rem(v + 1, 4)
    down = lambda v: lax.rem(v + 3, 4)
    far = lambda v: lax.rem(v + 2, 4)

    zr = 4 * r + z
    zu, zd = lax.rem(zr + 1, 8), lax.rem(zr + 7, 8)
    z_up = at(r_=zu // 4, z_=lax.rem(zu, 4))
    z_dn = at(r_=zd // 4, z_=lax.rem(zd, 4))
    x_up, x_dn = at(x_=up(x)), at(x_=down(x))
    y_up, y_dn = at(y_=up(y)), at(y_=down(y))
    mate = at(c_=other)
    fs_peers = []
    for i in range(1, 16):
        g = lax.rem(f + i, 16)
        fs_peers.append(at(z_=g // 4, x_=lax.rem(g, 4)))

    barrier = pltpu.get_barrier_semaphore()
    greet = fs_peers + [at(x_=jnp.int32(k), c_=other) for k in range(4)]
    greet += [y_up, y_dn, z_up, z_dn]
    for peer in greet:
        pl.semaphore_signal(barrier, inc=1, device_id=peer, device_id_type=MESH)
    pl.semaphore_wait(barrier, len(greet))

    started = []
    count = [0]

    def take(n=1):
        first = count[0]
        count[0] += n
        return first

    def remote(src, dst, s, k, peer):
        return pltpu.make_async_remote_copy(
            src_ref=src, dst_ref=dst, send_sem=ssem.at[s], recv_sem=rsem.at[k],
            device_id=peer, device_id_type=MESH,
        )

    def send(src, dst, k, peer):
        copy = remote(src, dst, k, k, peer)
        copy.start()
        started.append(copy)

    def push(ref, k, peer):
        send(ref, ref, k, peer)

    def recv(dst, k):
        remote(dst, dst, 0, k, mate).wait_recv()

    chunks = [
        (gp, WGP, 0, 256), (vp, WVP, 0, 256), (mp, WMP, 0, 256),
        (gu, WGU0, 0, real0), (vu, WVU0, 0, real0),
        (gu, WGU1, real0, n1), (vu, WVU1, real0, n1),
        (dn, WDN0, 0, real0), (dn, WDN1, real0, n1),
    ]
    zk = [take(6) for _ in chunks]

    def z_parts(i):
        _, _, at0, n = chunks[i]
        return (at0, pl.ds(0, n // 2)), (at0 + n // 2, pl.ds(n // 2, n // 2))

    def z_own(i):
        src, buf, at0, n = chunks[i]
        (sa, a), (sb, b) = z_parts(i)
        from_a, from_b = src.at[pl.ds(sa, n // 2)], src.at[pl.ds(sb, n // 2)]
        send(from_a, buf.at[z, a], zk[i], z_up)
        send(from_b, buf.at[z, b], zk[i] + 1, z_dn)
        send(from_b, buf.at[z, b], zk[i] + 2, z_up)
        send(from_a, buf.at[z, a], zk[i] + 3, z_dn)
        z_local(i).start()

    def z_local(i):
        src, buf, at0, n = chunks[i]
        return pltpu.make_async_copy(src.at[pl.ds(at0, n)], buf.at[z, pl.ds(0, n)], lsem.at[i])

    def z_fwd(i):
        buf = chunks[i][1]
        (_, a), (_, b) = z_parts(i)
        recv(buf.at[down(z), a], zk[i])
        push(buf.at[down(z), a], zk[i] + 4, z_up)
        recv(buf.at[up(z), b], zk[i] + 1)
        push(buf.at[up(z), b], zk[i] + 5, z_dn)

    def z_fin(i):
        buf = chunks[i][1]
        (_, a), (_, b) = z_parts(i)
        recv(buf.at[down(z), b], zk[i] + 2)
        recv(buf.at[up(z), a], zk[i] + 3)
        recv(buf.at[far(z), a], zk[i] + 4)
        recv(buf.at[far(z), b], zk[i] + 5)
        z_local(i).wait()

    swaps = []
    kx = take(4)
    me = 2 * y + c
    to_me = x // 2 == c
    for j in range(2):
        for h in range(2):
            xt = 2 * c + j
            mine = jnp.logical_and(xt == x, c == h)
            cols = slice(j * 256 + h * 128, j * 256 + h * 128 + 128)
            copy = remote(
                tok.at[:, cols], XG.at[2 * y + h, x], kx + 2 * j + h, kx + x,
                at(x_=xt, c_=jnp.int32(h)),
            )
            swaps.append((mine, copy))

            @pl.when(jnp.logical_not(mine))
            def _():
                copy.start()

            @pl.when(mine)
            def _():
                XG[2 * y + h, x] = tok[:, cols]

    z_own(0)
    z_own(1)
    z_own(2)

    for j in range(4):

        @pl.when(jnp.logical_not(jnp.logical_and(x == j, to_me)))
        def _():
            recv(XG.at[me, j], kx + j)

    lo_y, hi_y, far_y = 2 * down(y) + c, 2 * up(y) + c, 2 * far(y) + c
    a2, b2 = pl.ds(0, 2), pl.ds(2, 2)

    def y_start(buf, k):
        push(buf.at[me, a2], k, y_up)
        push(buf.at[me, b2], k + 1, y_dn)
        push(buf.at[me, b2], k + 2, y_up)
        push(buf.at[me, a2], k + 3, y_dn)
        push(buf.at[me], k + 6, mate)

    def y_mid(buf, k):
        recv(buf.at[lo_y, a2], k)
        push(buf.at[lo_y, a2], k + 4, y_up)
        push(buf.at[lo_y, a2], k + 7, mate)
        recv(buf.at[hi_y, b2], k + 1)
        push(buf.at[hi_y, b2], k + 5, y_dn)
        push(buf.at[hi_y, b2], k + 8, mate)

    def y_end(buf, k):
        recv(buf.at[lo_y, b2], k + 2)
        push(buf.at[lo_y, b2], k + 9, mate)
        recv(buf.at[hi_y, a2], k + 3)
        push(buf.at[hi_y, a2], k + 10, mate)
        recv(buf.at[far_y, a2], k + 4)
        push(buf.at[far_y, a2], k + 11, mate)
        recv(buf.at[far_y, b2], k + 5)
        push(buf.at[far_y, b2], k + 12, mate)

    def y_last(buf, k):
        recv(buf.at[2 * y + other], k + 6)
        recv(buf.at[2 * down(y) + other, a2], k + 7)
        recv(buf.at[2 * up(y) + other, b2], k + 8)
        recv(buf.at[2 * down(y) + other, b2], k + 9)
        recv(buf.at[2 * up(y) + other, a2], k + 10)
        recv(buf.at[2 * far(y) + other, a2], k + 11)
        recv(buf.at[2 * far(y) + other, b2], k + 12)

    def scaled(buf, gains):
        parts = [gains[pl.ds(pl.multiple_of((4 * k + x) * 256, 256), 256)] for k in range(4)]
        gain = jnp.concatenate([part.reshape(1, 256) for part in parts], axis=1)

        def block(b, _):
            rows = jnp.concatenate([buf[i, b] for i in range(8)], axis=1).astype(F32)
            SQ[b] = jnp.broadcast_to(jnp.sum(rows * rows, axis=-1, keepdims=True), (128, 128))
            XS[pl.ds(pl.multiple_of(b * 128, 128), 128), :] = (rows * gain).astype(BF16)
            return 0

        lax.fori_loop(0, 4, block, 0)

    ky = take(13)
    y_start(XG, ky)
    km = take(15)
    for i in range(15):
        send(smix, SM.at[f], km + i, fs_peers[i])
    SM[f] = smix[...]
    for W in (WGU0, WVU0, WDN0):
        for k in range(4):
            W[k, real0:, :] = jnp.zeros((n0 - real0, 256), BF16)
    for w, kern, off in ((0, gk, go), (1, vk, vo)):
        CV0[w, :, n0 - 128 :] = jnp.zeros((4, 128), F32)
        CV0[w, 0:3, 0:real0] = kern[:, 0:real0]
        CV1[w, 0:3, :] = kern[:, real0:]
        bias = off[...].reshape(1, units)
        CV0[w, 3:4, 0:real0] = bias[:, 0:real0]
        CV1[w, 3:4, :] = bias[:, real0:]
    y_mid(XG, ky)
    z_fwd(0)
    z_fwd(1)
    y_end(XG, ky)
    z_fwd(2)
    z_own(3)
    z_own(4)
    y_last(XG, ky)

    scaled(XG, mgain)
    z_fin(0)
    z_fin(1)
    for w, W in ((0, WGP), (1, WVP)):
        prod = jnp.dot(XS[...], W[...].reshape(1024, 256), preferred_element_type=F32)
        P1[:, :, w * 256 : w * 256 + 256] = prod.reshape(4, 128, 256)
    P1[:, :, 512:640] = SQ[...]

    def enc(v, edge):
        if edge is None:
            return v.astype(BF16)
        m = v.shape[1] - 128
        last = v[:, m:]
        low = last - last.astype(BF16).astype(F32)
        last = jnp.where(lanes_of(v.shape[0]) >= (edge + 128) // 2, low, last)
        return jnp.concatenate([v[:, :m].astype(BF16), last.astype(BF16)], axis=1)

    def dec(v, edge):
        v = v.astype(F32)
        if edge is None:
            return v
        m = v.shape[1] - 128
        last, lane = v[:, m:], lanes_of(v.shape[0])
        keep = jnp.logical_or(lane == edge, lane == (edge + 128) // 2)
        total = jnp.sum(jnp.where(keep, last, 0.0), axis=-1, keepdims=True)
        last = jnp.where(lane < edge, last, total)
        return jnp.concatenate([v[:, :m], last], axis=1) if m else last

    def row_loop(first, n, fn):
        def step(i, _):
            fn(pl.ds(pl.multiple_of(first + i * 16, 16), 16))
            return 0

        lax.fori_loop(0, n // 16, step, 0)

    ra, rb = pl.ds(0, 64), pl.ds(64, 64)

    def rs_first(p, A, B, C, HL, HR, FL, FR, k, edge):
        u, d = up(x), down(x)

        def far_rows(rows):
            A[rows, :] = enc(p[far(x), rows, :], edge)

        def up_rows(rows):
            B[rows, :] = enc(p[u, rows, :], edge)

        def down_rows(rows):
            C[rows, :] = enc(p[d, rows, :], edge)

        row_loop(0, 128, far_rows)
        send(A.at[ra], HL, k, x_up)
        send(A.at[rb], HR, k + 1, x_dn)
        row_loop(64, 64, up_rows)
        send(B.at[rb], FL.at[rb], k + 2, x_up)
        row_loop(0, 64, down_rows)
        send(C.at[ra], FR.at[ra], k + 3, x_dn)

    def rs_second(p, A, B, C, HL, HR, FL, FR, k, edge):
        u, d = up(x), down(x)

        def left(rows):
            B[rows, :] = enc(p[u, rows, :] + dec(HL[rows, :], edge), edge)

        def right(rows):
            low = pl.ds(pl.multiple_of(rows.start + 64, 16), 16)
            C[low, :] = enc(p[d, low, :] + dec(HR[rows, :], edge), edge)

        recv(HL, k)
        row_loop(0, 64, left)
        send(B.at[ra], FL.at[ra], k + 4, x_up)
        recv(HR, k + 1)
        row_loop(0, 64, right)
        send(C.at[rb], FR.at[rb], k + 5, x_dn)

    def rs_wait(FL, FR, k):
        recv(FL.at[rb], k + 2)
        recv(FR.at[ra], k + 3)
        recv(FL.at[ra], k + 4)
        recv(FR.at[rb], k + 5)

    k1 = take(6)
    set1 = (P1, A1, B1, C1, HL1, HR1, FL1, FR1, k1, 0)
    rs_first(*set1)
    rs_second(*set1)
    for i in range(15):
        recv(SM.at[lax.rem(f + 15 - i, 16)], km + i)
    rs_wait(FL1, FR1, k1)

    total = P1[x] + dec(FL1[...], 0) + dec(FR1[...], 0)
    rs = lax.rsqrt(total[:, 512:513] / depth + EPS)
    eye = lax.broadcasted_iota(jnp.int32, (128, 128), 0) == lanes_of(128)
    for h in range(2):
        cols = slice(h * 128, h * 128 + 128)
        gated = gelu((rs * total[:, cols]).astype(BF16).astype(F32))
        spread = gelu((rs * total[:, 256 + h * 128 : 384 + h * 128]).astype(BF16).astype(F32))
        spread = spread * lax.rsqrt(jnp.mean(spread * spread, axis=-1, keepdims=True) + EPS)
        spread = (spread * vgain[h : h + 1, :]).astype(BF16)
        matrix = SM[:, h].astype(F32).reshape(128, 128).astype(BF16)
        mixed = jnp.dot(matrix, spread, preferred_element_type=F32)
        bias = jnp.broadcast_to(sbias[h : h + 1, :], (128, 128))
        mixed = mixed + jnp.sum(jnp.where(eye, bias, 0.0), axis=-1, keepdims=True)
        joined = gated * mixed
        joined = joined * lax.rsqrt(jnp.mean(joined * joined, axis=-1, keepdims=True) + EPS)
        MG[x, :, cols] = (joined * hgain[h : h + 1, :]).astype(BF16)

    def x_start(buf, k):
        push(buf.at[x, ra], k, x_up)
        push(buf.at[x, rb], k + 1, x_dn)
        push(buf.at[x, rb], k + 2, x_up)
        push(buf.at[x, ra], k + 3, x_dn)

    def x_mid(buf, k):
        recv(buf.at[down(x), ra], k)
        push(buf.at[down(x), ra], k + 4, x_up)
        recv(buf.at[up(x), rb], k + 1)
        push(buf.at[up(x), rb], k + 5, x_dn)

    def x_last(buf, k):
        recv(buf.at[down(x), rb], k + 2)
        recv(buf.at[up(x), ra], k + 3)
        recv(buf.at[far(x), ra], k + 4)
        recv(buf.at[far(x), rb], k + 5)

    k2 = take(6)
    x_start(MG, k2)
    z_fwd(3)
    z_own(5)
    x_mid(MG, k2)
    z_fin(2)
    x_last(MG, k2)

    ya, yb = pl.ds(0, 256), pl.ds(256, 256)

    def cy_first(product, CS, CR, k):
        for n, yt in enumerate((far(y), up(y), down(y), y)):
            prod = product(yt)
            T[n] = jnp.where(c == 0, prod[:, :128], prod[:, 128:])
            CS[n] = jnp.where(c == 0, prod[:, 128:], prod[:, :128]).astype(BF16)
            send(CS.at[n], CR.at[n], k + n, mate)

    def cy_second(CR, YA, YB, YC, YHL, YHR, YFL, YFR, k):
        recv(CR.at[0], k)
        YA[...] = (T[0] + CR[0].astype(F32)).astype(BF16)
        send(YA.at[ya], YHL, k + 4, y_up)
        send(YA.at[yb], YHR, k + 5, y_dn)
        recv(CR.at[1], k + 1)
        YB[yb, :] = (T[1, yb, :] + CR[1, yb, :].astype(F32)).astype(BF16)
        send(YB.at[yb], YFL.at[yb], k + 6, y_up)
        recv(CR.at[2], k + 2)
        YC[ya, :] = (T[2, ya, :] + CR[2, ya, :].astype(F32)).astype(BF16)
        send(YC.at[ya], YFR.at[ya], k + 7, y_dn)

    def cy_third(CR, YB, YC, YHL, YHR, YFL, YFR, k):
        recv(YHL, k + 4)
        mixed = T[1, ya, :] + CR[1, ya, :].astype(F32) + YHL[...].astype(F32)
        YB[ya, :] = mixed.astype(BF16)
        send(YB.at[ya], YFL.at[ya], k + 8, y_up)
        recv(YHR, k + 5)
        mixed = T[2, yb, :] + CR[2, yb, :].astype(F32) + YHR[...].astype(F32)
        YC[yb, :] = mixed.astype(BF16)
        send(YC.at[yb], YFR.at[yb], k + 9, y_dn)
        recv(CR.at[3], k + 3)

    def cy_last(CR, YFL, YFR, k):
        recv(YFL.at[yb], k + 6)
        recv(YFR.at[ya], k + 7)
        recv(YFL.at[ya], k + 8)
        recv(YFR.at[yb], k + 9)
        both = YFL[...].astype(F32) + YFR[...].astype(F32)
        return T[3] + CR[3].astype(F32) + both

    def merge(yt):
        return jnp.dot(MG[...].reshape(512, 256), WMP[yt], preferred_element_type=F32)

    k3 = take(10)
    cy_first(merge, CS4, CR4, k3)
    cy_second(CR4, YA4, YB4, YC4, YHL4, YHR4, YFL4, YFR4, k3)
    cy_third(CR4, YB4, YC4, YHL4, YHR4, YFL4, YFR4, k3)
    z_fwd(4)
    z_own(6)
    branch = cy_last(CR4, YFL4, YFR4, k3)
    hidden = (XG[me].reshape(512, 128).astype(F32) + branch).astype(BF16)
    HG[me] = hidden.reshape(4, 128, 128)

    kh = take(13)
    y_start(HG, kh)
    y_mid(HG, kh)
    z_fwd(5)
    y_end(HG, kh)
    z_fin(3)
    z_fin(4)
    y_last(HG, kh)
    scaled(HG, fgain)

    def project(W, p, n, first):
        def cut(cols, to, size):
            w = jnp.concatenate([W[k, cols, :] for k in range(4)], axis=1)
            prod = lax.dot_general(
                XS[...], w, (((1,), (1,)), ((), ())), preferred_element_type=F32
            )
            p[:, :, to] = prod.reshape(4, 128, size)

        def step(i, _):
            cut(
                pl.ds(pl.multiple_of(i * 256, 256), 256),
                pl.ds(pl.multiple_of(first + i * 256, 128), 256), 256,
            )
            return 0

        lax.fori_loop(0, n // 256, step, 0)
        rest = n % 256
        if rest:
            cut(pl.ds(n - rest, rest), pl.ds(first + n - rest, rest), rest)

    project(WVU0, P2, n0, 0)
    project(WGU0, P2, n0, n0)
    ends = slice(2 * n0 - 128, 2 * n0)
    lane = lax.broadcasted_iota(jnp.int32, (4, 128, 128), 2)
    P2[:, :, ends] = jnp.where(lane < edge, P2[:, :, ends], SQ[...])
    k4, k5 = take(6), take(6)
    set2 = (P2, A2, B2, C2, HL2, HR2, FL2, FR2, k4, edge)
    set3 = (P3, A3, B3, C3, HL3, HR3, FL3, FR3, k5, None)
    rs_first(*set2)
    z_fwd(6)
    z_own(7)
    z_own(8)
    rs_second(*set2)
    z_fin(5)
    z_fin(6)
    project(WVU1, P3, n1, 0)
    project(WGU1, P3, n1, n1)
    rs_first(*set3)

    row = lax.broadcasted_iota(jnp.int32, (128, 128), 0)

    def activate(p, FL, FR, cv, act, n):
        def conv_tile(i, _):
            cols = pl.ds(pl.multiple_of(i * 128, 128), 128)

            def one(first, w):
                at_ = pl.ds(pl.multiple_of(first + i * 128, 128), 128)
                v = p[x, :, at_] + FL[:, at_].astype(F32) + FR[:, at_].astype(F32)
                v = (RS[...] * v).astype(BF16).astype(F32)
                prev = jnp.where(row == 0, 0.0, pltpu.roll(v, 1, axis=0))
                after = jnp.where(row == 127, 0.0, pltpu.roll(v, 127, axis=0))
                k = cv[w, :, cols]
                return k[3:4] + prev * k[0:1] + v * k[1:2] + after * k[2:3]

            act[x, :, cols] = (gelu(one(n, 0)) * one(0, 1)).astype(BF16)
            return 0

        lax.fori_loop(0, n // 128, conv_tile, 0)

    rs_wait(FL2, FR2, k4)
    sq = P2[x, :, ends] + dec(FL2[:, ends], edge) + dec(FR2[:, ends], edge)
    rs2 = lax.rsqrt(sq[:, 127:128] / depth + EPS)
    RS[...] = jnp.broadcast_to(rs2, (128, 128))
    rs_second(*set3)
    activate(P2, FL2, FR2, CV0, ACT0, n0)
    k6, k8 = take(6), take(6)
    x_start(ACT0, k6)
    z_fwd(7)
    rs_wait(FL3, FR3, k5)
    activate(P3, FL3, FR3, CV1, ACT1, n1)
    x_start(ACT1, k8)
    x_mid(ACT0, k6)
    z_fwd(8)
    x_last(ACT0, k6)
    z_fin(7)

    def early(n, _):
        ACC[n] = jnp.dot(ACT0[...].reshape(512, n0), WDN0[n], preferred_element_type=F32)
        return 0

    lax.fori_loop(0, 4, early, 0)
    x_mid(ACT1, k8)
    z_fin(8)
    x_last(ACT1, k8)

    def late(yt):
        prod = jnp.dot(ACT1[...].reshape(512, n1), WDN1[yt], preferred_element_type=F32)
        return prod + ACC[yt]

    k7 = take(10)
    cy_first(late, CS5, CR5, k7)
    cy_second(CR5, YA5, YB5, YC5, YHL5, YHR5, YFL5, YFR5, k7)
    cy_third(CR5, YB5, YC5, YHL5, YHR5, YFL5, YFR5, k7)
    change = cy_last(CR5, YFL5, YFR5, k7)
    result = (HG[me].reshape(512, 128).astype(F32) + change).astype(BF16)
    OP[...] = result.reshape(4, 128, 128)

    ko = take(8)
    place = lax.rem(x, 2)
    to_cols = pl.ds(pl.multiple_of(place * 256 + c * 128, 128), 128)
    for j in range(4):
        mine = jnp.logical_and(x == j, to_me)
        copy = remote(
            OP.at[j], out.at[:, to_cols], ko + 4 + j, ko + 2 * place + c,
            at(x_=jnp.int32(j), c_=x // 2),
        )
        swaps.append((mine, copy))

        @pl.when(jnp.logical_not(mine))
        def _():
            copy.start()

        @pl.when(mine)
        def _():
            out[:, to_cols] = OP[j]

    for j in range(2):
        for h in range(2):

            @pl.when(jnp.logical_not(jnp.logical_and(2 * c + j == x, c == h)))
            def _():
                recv(out.at[:, pl.ds(j * 256 + h * 128, 128)], ko + 2 * j + h)

    for copy in started:
        copy.wait_send()
    for mine, copy in swaps:

        @pl.when(jnp.logical_not(mine))
        def _():
            copy.wait_send()


def body(
    tokens, mixer_gain, gate_proj, value_proj, value_gain, spatial_mix, spatial_bias,
    head_gain, merge_proj, ffn_gain, gate_up, value_up, gate_kernel, value_kernel,
    gate_offset, value_offset, down_proj,
):
    units = gate_up.shape[1]
    n1 = units // 2 // 128 * 128 + 128
    n0 = -(-(units - n1) // 128) * 128
    vm = lambda shape, dtype=BF16: pltpu.VMEM(shape, dtype)

    def rs_x(n):
        return [
            vm((4, 128, n), F32), *[vm((128, n))] * 3, *[vm((64, n))] * 2, *[vm((128, n))] * 2,
        ]

    def rs_y():
        return [
            *[vm((4, 512, 128))] * 2, *[vm((512, 128))] * 3, *[vm((256, 128))] * 2,
            *[vm((512, 128))] * 2,
        ]

    in_vmem = pl.BlockSpec(memory_space=pltpu.VMEM)
    left = pl.BlockSpec(memory_space=pl.ANY)
    call = pl.pallas_call(
        kernel,
        out_shape=jax.ShapeDtypeStruct(tokens.shape, tokens.dtype),
        in_specs=[
            in_vmem, in_vmem, in_vmem, left, left, in_vmem, in_vmem, in_vmem, in_vmem, left,
            left, left, in_vmem, in_vmem, in_vmem, in_vmem, left,
        ],
        out_specs=in_vmem,
        scratch_shapes=[
            vm((2, 4, n0), F32), vm((2, 4, n1), F32),
            vm((8, 4, 128, 128)), vm((8, 4, 128, 128)), vm((512, 1024)),
            vm((4, 128, 128), F32), vm((128, 128), F32), vm((16, 2, 8, 128)),
            vm((4, 128, 256)), vm((4, 128, 128)),
            *[vm((4, 256, 256))] * 3, *[vm((4, n0, 256))] * 2, *[vm((4, n1, 256))] * 2,
            vm((4, n0, 256)), vm((4, n1, 256)),
            vm((4, 128, n0)), vm((4, 128, n1)), vm((4, 512, 128), F32), vm((4, 512, 256), F32),
            *rs_x(640), *rs_x(2 * n0), *rs_x(2 * n1),
            *rs_y(), *rs_y(),
            pltpu.SemaphoreType.DMA((SEMS,)), pltpu.SemaphoreType.DMA((SEMS,)),
            pltpu.SemaphoreType.DMA((9,)),
        ],
        compiler_params=pltpu.CompilerParams(
            collective_id=0, has_side_effects=True, vmem_limit_bytes=58 << 20
        ),
        name="layer",
    )
    return call(
        tokens, mixer_gain, ffn_gain, gate_proj, value_proj, value_gain, spatial_mix,
        spatial_bias, head_gain, merge_proj, gate_up.T, value_up.T, gate_kernel, value_kernel,
        gate_offset, value_offset, down_proj,
    )


def solution(mesh):
    finer = Mesh(
        mesh.devices.reshape(mesh.shape["rep"], 4, 4, 4, 2), ("rep", "fs_0", "fs_1", "tp_0", "tp_1")
    )
    return jax.shard_map(
        body,
        mesh=finer,
        in_specs=(
            P(REP_FS, TP), P(), P(FS, TP), P(FS, TP), P(TP, None), P(TP, FS, None),
            P(TP, None), P(TP, None), P(TP, FS), P(), P(FS, TP), P(FS, TP), P(None, TP),
            P(None, TP), P(TP), P(TP), P(TP, FS),
        ),
        out_specs=P(REP_FS, TP),
        check_vma=False,
    )
```

time: 146 us -> 125 us (0.86)
  Pallas kernels: 144 us -> 122 us
    pallas_call x1, Pallas kernels: 144 us -> 122 us  [body(): call(tokens, mixer_gain, ffn_gain, gate_proj, value_proj, value_gain, spa...]
where the time goes in v3:
time: 125 us; the launch traced here: 124 us
  Pallas kernels  122 us (98%)
  local copies, waits for them, and re-layouts  1.57 us (1%)
    pallas_call x1, Pallas kernels, body(): call(tokens, mixer_gain, ffn_gain, gate_proj, value_proj, value_gain, spa...  122 us

profile of v3, /device:TPU:57, one launch (start us, length us, event | category | flops | bytes accessed | tf_op | source)
XLA Modules:
  0.0 123.8 jit_solution(17018354626806184090)
XLA Ops:
  0.0 122.3 %layer.1 = bf16[128,512]{1,0:T(8,128)(2,1)} custom-call(bf16[128,512]{1,0:T(8,128)(2,1)} %tok.1, f32[4096]{0:T(1024)} %mgain.1, f32[4096]{0:T(1024)} %fgain.1, bf16[256,256]{1,0:T(8,128)(2,1)} %gp.1, bf16[256,256]{1,0:T(8,128)(2,1)} %vp.1, f32[2,128]{1,0:T(2,128)} %vgain.1, bf16[2,8,128]{2,1,0:T(8,128)(2,1)} %smix.1, f32[2,128]{1,0:T(2,128)} %sbias.1, ...), custom_call_target="tpu_custom_call" | custom-call | tf_op jit(solution)/shard_map/layer/pallas_call | solution.py:627
  122.3 1.6 %copy.19 = bf16[128,512]{1,0:T(8,128)(2,1)} copy(bf16[128,512]{1,0:T(8,128)(2,1)} %layer.1) | data formatting | bytes 262144

commit v4 on v3

--- a/solution.py
+++ b/solution.py
@@ -13,7 +13,7 @@
 EPS = 1e-06
 F32 = jnp.float32
 BF16 = jnp.bfloat16
-SEMS = 192
+SEMS = 224
 
 
 def gelu(v):
@@ -27,14 +27,14 @@
 def kernel(
     tok, mgain, fgain, gp, vp, vgain, smix, sbias, hgain, mp, gu, vu, gk, vk, go, vo, dn,
     out,
-    CV0, CV1, XG, HG, XS, SQ, RS, SM, MG, OP,
+    CV0, CV1, XG, HG, XS, SQ, RS, SM, MG, SSB, HRES, TB, TI,
     WGP, WVP, WMP, WGU0, WVU0, WGU1, WVU1, WDN0, WDN1,
     ACT0, ACT1, T, ACC,
     P1, A1, B1, C1, HL1, HR1, FL1, FR1,
     P2, A2, B2, C2, HL2, HR2, FL2, FR2,
     P3, A3, B3, C3, HL3, HR3, FL3, FR3,
     CS4, CR4, YA4, YB4, YC4, YHL4, YHR4, YFL4, YFR4,
-    CS5, CR5, YA5, YB5, YC5, YHL5, YHR5, YFL5, YFR5,
+    CS5, CR5,
     ssem, rsem, lsem,
 ):
     r, z, x, y, c = (lax.axis_index(a) for a in ("rep", "fs_0", "fs_1", "tp_0", "tp_1"))
@@ -68,8 +68,11 @@
         fs_peers.append(at(z_=g // 4, x_=lax.rem(g, 4)))
 
     barrier = pltpu.get_barrier_semaphore()
-    greet = fs_peers + [at(x_=jnp.int32(k), c_=other) for k in range(4)]
-    greet += [y_up, y_dn, z_up, z_dn]
+    near = []
+    for i in range(1, 16):
+        g = lax.rem(4 * y + x + i, 16)
+        near += [at(y_=g // 4, x_=lax.rem(g, 4), c_=jnp.int32(k)) for k in range(2)]
+    greet = [mate, z_up, z_dn] + near + [fs_peers[i - 1] for i in range(1, 16)]
     for peer in greet:
         pl.semaphore_signal(barrier, inc=1, device_id=peer, device_id_type=MESH)
     pl.semaphore_wait(barrier, len(greet))
@@ -168,6 +171,15 @@
     z_own(0)
     z_own(1)
     z_own(2)
+
+    me = 2 * y + c
+    square = tok[...].astype(F32)
+    square = jnp.sum(square * square, axis=-1, keepdims=True)
+    SSB[me] = jnp.broadcast_to(square, (128, 128)).T[0:8, :]
+    ks = take(7)
+    for i in range(1, 8):
+        t = lax.rem(me + i, 8)
+        send(SSB.at[me], SSB.at[me], ks + i - 1, at(y_=t // 2, c_=lax.rem(t, 2)))
 
     for j in range(4):
 
@@ -255,7 +267,6 @@
     for w, W in ((0, WGP), (1, WVP)):
         prod = jnp.dot(XS[...], W[...].reshape(1024, 256), preferred_element_type=F32)
         P1[:, :, w * 256 : w * 256 + 256] = prod.reshape(4, 128, 256)
-    P1[:, :, 512:640] = SQ[...]
 
     def enc(v, edge):
         if edge is None:
@@ -286,21 +297,23 @@
 
     ra, rb = pl.ds(0, 64), pl.ds(64, 64)
 
-    def rs_first(p, A, B, C, HL, HR, FL, FR, k, edge):
-        u, d = up(x), down(x)
-
+    def rs_far(p, A, B, C, HL, HR, FL, FR, k, edge):
         def far_rows(rows):
             A[rows, :] = enc(p[far(x), rows, :], edge)
-
-        def up_rows(rows):
-            B[rows, :] = enc(p[u, rows, :], edge)
-
-        def down_rows(rows):
-            C[rows, :] = enc(p[d, rows, :], edge)
 
         row_loop(0, 128, far_rows)
         send(A.at[ra], HL, k, x_up)
         send(A.at[rb], HR, k + 1, x_dn)
+
+    def rs_first(p, A, B, C, HL, HR, FL, FR, k, edge):
+        u, d = up(x), down(x)
+
+        def up_rows(rows):
+            B[rows, :] = enc(p[u, rows, :], edge)
+
+        def down_rows(rows):
+            C[rows, :] = enc(p[d, rows, :], edge)
+
         row_loop(64, 64, up_rows)
         send(B.at[rb], FL.at[rb], k + 2, x_up)
         row_loop(0, 64, down_rows)
@@ -330,15 +343,19 @@
         recv(FR.at[rb], k + 5)
 
     k1 = take(6)
-    set1 = (P1, A1, B1, C1, HL1, HR1, FL1, FR1, k1, 0)
+    set1 = (P1, A1, B1, C1, HL1, HR1, FL1, FR1, k1, None)
+    rs_far(*set1)
     rs_first(*set1)
     rs_second(*set1)
     for i in range(15):
         recv(SM.at[lax.rem(f + 15 - i, 16)], km + i)
     rs_wait(FL1, FR1, k1)
 
-    total = P1[x] + dec(FL1[...], 0) + dec(FR1[...], 0)
-    rs = lax.rsqrt(total[:, 512:513] / depth + EPS)
+    total = P1[x] + FL1[...].astype(F32) + FR1[...].astype(F32)
+    for i in range(1, 8):
+        recv(SSB.at[lax.rem(me + 8 - i, 8)], ks + i - 1)
+    square = jnp.sum(SSB[...], axis=0)[0:1, :]
+    rs = lax.rsqrt(jnp.broadcast_to(square, (128, 128)).T / depth + EPS)
     eye = lax.broadcasted_iota(jnp.int32, (128, 128), 0) == lanes_of(128)
     for h in range(2):
         cols = slice(h * 128, h * 128 + 128)
@@ -433,8 +450,24 @@
     hidden = (XG[me].reshape(512, 128).astype(F32) + branch).astype(BF16)
     HG[me] = hidden.reshape(4, 128, 128)
 
-    kh = take(13)
+    kh, ko = take(13), take(8)
     y_start(HG, kh)
+    spot = 2 * lax.rem(x, 2) + c
+    for j in range(4):
+        mine = jnp.logical_and(x == j, to_me)
+        copy = remote(
+            HG.at[me, j], HRES.at[spot], ko + 4 + j, ko + spot, at(x_=jnp.int32(j), c_=x // 2)
+        )
+        swaps.append((mine, copy))
+
+        @pl.when(jnp.logical_not(mine))
+        def _():
+            copy.start()
+
+        @pl.when(mine)
+        def _():
+            HRES[spot] = HG[me, j]
+
     y_mid(HG, kh)
     z_fwd(5)
     y_end(HG, kh)
@@ -443,13 +476,19 @@
     y_last(HG, kh)
     scaled(HG, fgain)
 
-    def project(W, p, n, first):
+    def project(W, p, n, first, block=None):
         def cut(cols, to, size):
             w = jnp.concatenate([W[k, cols, :] for k in range(4)], axis=1)
+            rows = XS[...]
+            if block is not None:
+                rows = XS[pl.ds(pl.multiple_of(block * 128, 128), 128), :]
             prod = lax.dot_general(
-                XS[...], w, (((1,), (1,)), ((), ())), preferred_element_type=F32
+                rows, w, (((1,), (1,)), ((), ())), preferred_element_type=F32
             )
-            p[:, :, to] = prod.reshape(4, 128, size)
+            if block is None:
+                p[:, :, to] = prod.reshape(4, 128, size)
+            else:
+                p[block, :, to] = prod
 
         def step(i, _):
             cut(
@@ -463,14 +502,18 @@
         if rest:
             cut(pl.ds(n - rest, rest), pl.ds(first + n - rest, rest), rest)
 
-    project(WVU0, P2, n0, 0)
-    project(WGU0, P2, n0, n0)
-    ends = slice(2 * n0 - 128, 2 * n0)
-    lane = lax.broadcasted_iota(jnp.int32, (4, 128, 128), 2)
-    P2[:, :, ends] = jnp.where(lane < edge, P2[:, :, ends], SQ[...])
     k4, k5 = take(6), take(6)
     set2 = (P2, A2, B2, C2, HL2, HR2, FL2, FR2, k4, edge)
     set3 = (P3, A3, B3, C3, HL3, HR3, FL3, FR3, k5, None)
+    ends = slice(2 * n0 - 128, 2 * n0)
+    lane = lax.broadcasted_iota(jnp.int32, (4, 128, 128), 2)
+    project(WVU0, P2, n0, 0, far(x))
+    project(WGU0, P2, n0, n0, far(x))
+    P2[far(x), :, ends] = jnp.where(lane[0] < edge, P2[far(x), :, ends], SQ[far(x)])
+    rs_far(*set2)
+    project(WVU0, P2, n0, 0)
+    project(WGU0, P2, n0, n0)
+    P2[:, :, ends] = jnp.where(lane < edge, P2[:, :, ends], SQ[...])
     rs_first(*set2)
     z_fwd(6)
     z_own(7)
@@ -480,6 +523,7 @@
     z_fin(6)
     project(WVU1, P3, n1, 0)
     project(WGU1, P3, n1, n1)
+    rs_far(*set3)
     rs_first(*set3)
 
     row = lax.broadcasted_iota(jnp.int32, (128, 128), 0)
@@ -516,6 +560,7 @@
     x_start(ACT1, k8)
     x_mid(ACT0, k6)
     z_fwd(8)
+    x_mid(ACT1, k8)
     x_last(ACT0, k6)
     z_fin(7)
 
@@ -524,7 +569,6 @@
         return 0
 
     lax.fori_loop(0, 4, early, 0)
-    x_mid(ACT1, k8)
     z_fin(8)
     x_last(ACT1, k8)
 
@@ -532,39 +576,52 @@
         prod = jnp.dot(ACT1[...].reshape(512, n1), WDN1[yt], preferred_element_type=F32)
         return prod + ACC[yt]
 
-    k7 = take(10)
+    k7 = take(4)
+    kt, kn = take(16), take(16)
     cy_first(late, CS5, CR5, k7)
-    cy_second(CR5, YA5, YB5, YC5, YHL5, YHR5, YFL5, YFR5, k7)
-    cy_third(CR5, YB5, YC5, YHL5, YHR5, YFL5, YFR5, k7)
-    change = cy_last(CR5, YFL5, YFR5, k7)
-    result = (HG[me].reshape(512, 128).astype(F32) + change).astype(BF16)
-    OP[...] = result.reshape(4, 128, 128)
-
-    ko = take(8)
-    place = lax.rem(x, 2)
-    to_cols = pl.ds(pl.multiple_of(place * 256 + c * 128, 128), 128)
-    for j in range(4):
-        mine = jnp.logical_and(x == j, to_me)
-        copy = remote(
-            OP.at[j], out.at[:, to_cols], ko + 4 + j, ko + 2 * place + c,
-            at(x_=jnp.int32(j), c_=x // 2),
-        )
-        swaps.append((mine, copy))
-
-        @pl.when(jnp.logical_not(mine))
-        def _():
-            copy.start()
-
-        @pl.when(mine)
-        def _():
-            out[:, to_cols] = OP[j]
+
+    for n, yt in enumerate((far(y), up(y), down(y), y)):
+        recv(CR5.at[n], k7 + n)
+        term = T[n] + CR5[n].astype(F32)
+        TB[n] = term.astype(BF16).reshape(4, 128, 128)
+        for j in range(4):
+            copy = remote(
+                TB.at[n, j], TI.at[y, spot], kn + 4 * n + j, kt + 4 * y + spot,
+                at(x_=jnp.int32(j), y_=yt, c_=x // 2),
+            )
+            if n < 3:
+                copy.start()
+                started.append(copy)
+                continue
+            mine = jnp.logical_and(x == j, to_me)
+            swaps.append((mine, copy))
+
+            @pl.when(jnp.logical_not(mine))
+            def _():
+                copy.start()
+
+            @pl.when(mine)
+            def _():
+                TI[y, spot] = TB[n, j]
 
     for j in range(2):
         for h in range(2):
-
-            @pl.when(jnp.logical_not(jnp.logical_and(2 * c + j == x, c == h)))
+            q = 2 * j + h
+            mine = jnp.logical_and(2 * c + j == x, c == h)
+
+            @pl.when(jnp.logical_not(mine))
             def _():
-                recv(out.at[:, pl.ds(j * 256 + h * 128, 128)], ko + 2 * j + h)
+                recv(HRES.at[q], ko + q)
+
+            for n in range(4):
+
+                @pl.when(jnp.logical_not(jnp.logical_and(mine, y == n)))
+                def _():
+                    recv(TI.at[n, q], kt + 4 * n + q)
+
+            change = jnp.sum(TI[:, q].astype(F32), axis=0)
+            result = (HRES[q].astype(F32) + change).astype(BF16)
+            out[:, q * 128 : q * 128 + 128] = result
 
     for copy in started:
         copy.wait_send()
@@ -610,12 +667,13 @@
             vm((2, 4, n0), F32), vm((2, 4, n1), F32),
             vm((8, 4, 128, 128)), vm((8, 4, 128, 128)), vm((512, 1024)),
             vm((4, 128, 128), F32), vm((128, 128), F32), vm((16, 2, 8, 128)),
-            vm((4, 128, 256)), vm((4, 128, 128)),
+            vm((4, 128, 256)), vm((8, 8, 128), F32), vm((4, 128, 128)),
+            vm((4, 4, 128, 128)), vm((4, 4, 128, 128)),
             *[vm((4, 256, 256))] * 3, *[vm((4, n0, 256))] * 2, *[vm((4, n1, 256))] * 2,
             vm((4, n0, 256)), vm((4, n1, 256)),
             vm((4, 128, n0)), vm((4, 128, n1)), vm((4, 512, 128), F32), vm((4, 512, 256), F32),
-            *rs_x(640), *rs_x(2 * n0), *rs_x(2 * n1),
-            *rs_y(), *rs_y(),
+            *rs_x(512), *rs_x(2 * n0), *rs_x(2 * n1),
+            *rs_y(), vm((4, 512, 128)), vm((4, 512, 128)),
             pltpu.SemaphoreType.DMA((SEMS,)), pltpu.SemaphoreType.DMA((SEMS,)),
             pltpu.SemaphoreType.DMA((9,)),
         ],

time: 125 us -> 119 us (0.952)
  the two profiles are of different devices: /device:TPU:57 before, /device:TPU:1 now
where the time goes in v4:
time: 119 us
  Pallas kernels  118 us (99%)
  local copies, waits for them, and re-layouts  1.57 us (1%)
    pallas_call x1, Pallas kernels, body(): call(tokens, mixer_gain, ffn_gain, gate_proj, value_proj, value_gain, spa...  118 us

profile of v4, /device:TPU:1, one launch (start us, length us, event | category | flops | bytes accessed | tf_op | source)
XLA Modules:
  0.0 119.4 jit_solution(10163852943222643988)
XLA Ops:
  0.0 117.8 %layer.1 = bf16[128,512]{1,0:T(8,128)(2,1)} custom-call(bf16[128,512]{1,0:T(8,128)(2,1)} %tok.1, f32[4096]{0:T(1024)} %mgain.1, f32[4096]{0:T(1024)} %fgain.1, bf16[256,256]{1,0:T(8,128)(2,1)} %gp.1, bf16[256,256]{1,0:T(8,128)(2,1)} %vp.1, f32[2,128]{1,0:T(2,128)} %vgain.1, bf16[2,8,128]{2,1,0:T(8,128)(2,1)} %smix.1, f32[2,128]{1,0:T(2,128)} %sbias.1, ...), custom_call_target="tpu_custom_call" | custom-call | tf_op jit(solution)/shard_map/layer/pallas_call | solution.py:685
  117.8 1.6 %copy.19 = bf16[128,512]{1,0:T(8,128)(2,1)} copy(bf16[128,512]{1,0:T(8,128)(2,1)} %layer.1) | data formatting | bytes 262144

commit v5 on v0

v5 whole, which is shorter than its diff:
```python
import functools

import jax
import jax.numpy as jnp
from jax import lax
from jax.experimental import pallas as pl
from jax.experimental.pallas import tpu as pltpu
from jax.sharding import Mesh
from jax.sharding import PartitionSpec as P

TP = ("tp_0", "tp_1")
FS = ("fs_0", "fs_1")
REP_FS = ("rep", "fs_0", "fs_1")
MESH = pl.DeviceIdType.MESH
EPS = 1e-06
SENDS, RECVS = 33, 96
CHUNK = 512
F32 = jnp.float32
BF16 = jnp.bfloat16


def gelu(v):
    return 0.5 * v * (1.0 + lax.erf(v * 0.7071067811865476))


def lanes_of(n):
    return lax.broadcasted_iota(jnp.int32, (n, 128), 1)


def kernel(layout, tok, mgain, fgain, gp, vp, vgain, smix, sbias, hgain, mp, gu, vu, gk, vk, go, vo,
           dn, out, tokv, gkv, vkv, CV, XG, HG, XS, SQR, RS, SM, MG, SSB, SSF, HRES, TB, TI,
           WGP, WVP, WMP, T, ACC, P1, S1, H1, F1, CS4, CR4, YS4, YH4, YF4, CS5, CR5, *rest):
    chunks = len(layout)
    WGU, WVU, WDN, ACT, PC, SC, HC, FC = (rest[i * chunks : (i + 1) * chunks] for i in range(8))
    ssem, rsem, lsem = rest[8 * chunks :]
    r, z, x, y, c = (lax.axis_index(a) for a in ("rep", "fs_0", "fs_1", "tp_0", "tp_1"))
    other = 1 - c
    f = 4 * z + x
    units = dn.shape[0]
    depth = mgain.shape[0]

    def at(z_=None, x_=None, y_=None, c_=None, r_=None):
        pick = lambda new, old: old if new is None else new
        return (pick(r_, r), pick(z_, z), pick(x_, x), pick(y_, y), pick(c_, c))

    up = lambda v: lax.rem(v + 1, 4)
    down = lambda v: lax.rem(v + 3, 4)
    far = lambda v: lax.rem(v + 2, 4)

    zr = 4 * r + z
    zu, zd = lax.rem(zr + 1, 8), lax.rem(zr + 7, 8)
    z_up = at(r_=zu // 4, z_=lax.rem(zu, 4))
    z_dn = at(r_=zd // 4, z_=lax.rem(zd, 4))
    x_up, x_dn, x_far = at(x_=up(x)), at(x_=down(x)), at(x_=far(x))
    y_up, y_dn = at(y_=up(y)), at(y_=down(y))
    mate = at(c_=other)
    fs_peers = []
    for i in range(1, 16):
        g = lax.rem(f + i, 16)
        fs_peers.append(at(z_=g // 4, x_=lax.rem(g, 4)))
    near = []
    for i in range(1, 16):
        g = lax.rem(4 * y + x + i, 16)
        near += [at(y_=g // 4, x_=lax.rem(g, 4), c_=jnp.int32(k)) for k in range(2)]

    barrier = pltpu.get_barrier_semaphore()
    greet = [mate, z_up, z_dn] + near + fs_peers
    for peer in greet:
        pl.semaphore_signal(barrier, inc=1, device_id=peer, device_id_type=MESH)
    loads = [
        pltpu.make_async_copy(src, dst, lsem.at[i])
        for i, (src, dst) in enumerate(((tok, tokv), (gk, gkv), (vk, vkv)))
    ]
    for copy in loads:
        copy.start()
    pl.semaphore_wait(barrier, len(greet))

    sends, recvs, ends = [0], [0], []

    def new(counter, n=1):
        counter[0] += n
        return counter[0] - n

    def remote(src, dst, s, k, peer):
        return pltpu.make_async_remote_copy(
            src_ref=src, dst_ref=dst, send_sem=ssem.at[s], recv_sem=rsem.at[k],
            device_id=peer, device_id_type=MESH,
        )

    def send(src, dst, s, k, peer):
        remote(src, dst, s, k, peer).start()

    def recv(dst, k):
        remote(dst, dst, 0, k, mate).wait_recv()

    def sender(ref):
        s = new(sends)
        ends.append(lambda: remote(ref, ref, s, 0, mate).wait_send())
        return s

    pieces = [(gp, WGP, 0, 256), (vp, WVP, 0, 256), (mp, WMP, 0, 256)]
    for (at0, n, _), G, V in zip(layout, WGU, WVU):
        pieces += [(gu, G, at0, n), (vu, V, at0, n)]
    for (at0, n, _), W in zip(layout, WDN):
        pieces.append((dn, W, at0, n))
    zk = [new(recvs, 3) for _ in pieces]
    zs = [sender(buf.at[pl.ds(0, 3), pl.ds(0, n)]) for _, buf, _, n in pieces]

    def z_local(i):
        src, buf, at0, n = pieces[i]
        return pltpu.make_async_copy(src.at[pl.ds(at0, n)], buf.at[z, pl.ds(0, n)], lsem.at[3 + i])

    def z_own(i):
        src, buf, at0, n = pieces[i]
        a, b = pl.ds(0, n // 2), pl.ds(n // 2, n // 2)
        from_a, from_b = src.at[pl.ds(at0, n // 2)], src.at[pl.ds(at0 + n // 2, n // 2)]
        send(from_a, buf.at[z, a], zs[i], zk[i], z_up)
        send(from_b, buf.at[z, b], zs[i], zk[i] + 1, z_dn)
        send(from_b, buf.at[z, b], zs[i], zk[i] + 2, z_up)
        send(from_a, buf.at[z, a], zs[i], zk[i] + 2, z_dn)
        z_local(i).start()

    def z_fwd(i):
        _, buf, _, n = pieces[i]
        a, b = buf.at[down(z), pl.ds(0, n // 2)], buf.at[up(z), pl.ds(n // 2, n // 2)]
        recv(a, zk[i])
        send(a, a, zs[i], zk[i] + 2, z_up)
        recv(b, zk[i] + 1)
        send(b, b, zs[i], zk[i] + 2, z_dn)

    def z_fin(i):
        _, buf, _, n = pieces[i]
        recv(buf.at[pl.ds(0, 2), pl.ds(0, n)], zk[i] + 2)
        z_local(i).wait()

    def weight(kind, j):
        return {"g": 3 + 2 * j, "v": 4 + 2 * j, "d": 3 + 2 * chunks + j}[kind]

    me = 2 * y + c
    to_me = x // 2 == c
    loads[0].wait()
    kx = new(recvs, 2)
    sx = new(sends)
    for j in range(2):
        for h in range(2):
            xt = 2 * c + j
            ahead = lax.rem(x - xt + 4, 4)
            place = jnp.where(ahead >= 2, 5 - ahead, ahead)
            mine = jnp.logical_and(xt == x, c == h)
            block = tokv.at[:, j * 256 + h * 128 : j * 256 + h * 128 + 128]

            @pl.when(jnp.logical_not(mine))
            def _():
                dst = XG.at[2 * y + h, place]
                send(block, dst, sx, kx + place // 2, at(x_=xt, c_=jnp.int32(h)))

            @pl.when(mine)
            def _():
                XG[2 * y + h, 0] = block[...]

    def fewer(ref_of, n, wait):
        @pl.when(to_me)
        def _():
            wait(ref_of(n - 1))

        @pl.when(jnp.logical_not(to_me))
        def _():
            wait(ref_of(n))

    stay = lambda s: lambda ref: remote(ref, ref, s, 0, mate).wait_send()
    ends.append(lambda: fewer(lambda n: XG.at[0, pl.ds(0, n)], 4, stay(sx)))
    z_own(0)
    z_own(1)
    square = tokv[...].astype(F32)
    square = jnp.sum(square * square, axis=-1, keepdims=True)
    SSB[me] = jnp.broadcast_to(square, (128, 128)).T[0:8, :]
    kss = new(recvs)
    sss = sender(SSB.at[pl.ds(0, 7)])
    for i in range(1, 8):
        t = lax.rem(me + i, 8)
        send(SSB.at[me], SSB.at[me], sss, kss, at(y_=t // 2, c_=lax.rem(t, 2)))

    lo_y, hi_y, far_y = 2 * down(y) + c, 2 * up(y) + c, 2 * far(y) + c

    def y_start(buf, k, s, g):
        a, b = buf.at[me, 2 * g], buf.at[me, 2 * g + 1]
        send(a, a, s, k, y_up)
        send(b, b, s, k + 1, y_dn)
        send(b, b, s, k + 2, y_up)
        send(a, a, s, k + 3, y_dn)
        both = buf.at[me, pl.ds(2 * g, 2)]
        send(both, both, s, k + 6, mate)

    def y_mid(buf, k, s, g):
        a, b = buf.at[lo_y, 2 * g], buf.at[hi_y, 2 * g + 1]
        recv(a, k)
        send(a, a, s, k + 4, y_up)
        send(a, a, s, k + 6, mate)
        recv(b, k + 1)
        send(b, b, s, k + 5, y_dn)
        send(b, b, s, k + 6, mate)

    def y_end(buf, k, s, g):
        rows = (buf.at[lo_y, 2 * g + 1], buf.at[hi_y, 2 * g], buf.at[far_y, 2 * g], buf.at[far_y, 2 * g + 1])
        for i, ref in enumerate(rows):
            recv(ref, k + 2 + i)
            send(ref, ref, s, k + 6, mate)

    def y_last(buf, k):
        recv(buf.at[pl.ds(0, 4), pl.ds(0, 2)], k + 6)

    def scaled(buf, gains, squares):
        parts = [gains[pl.ds(pl.multiple_of((4 * k + x) * 256, 256), 256)] for k in range(4)]
        gain = jnp.concatenate([part.reshape(1, 256) for part in parts], axis=1)

        def block(b, _):
            rows = jnp.concatenate([buf[i, b] for i in range(8)], axis=1).astype(F32)
            if squares:
                total = jnp.sum(rows * rows, axis=-1, keepdims=True)
                SQR[b] = jnp.broadcast_to(total, (128, 128)).T[0:8, :]
            XS[pl.ds(pl.multiple_of(b * 128, 128), 128), :] = (rows * gain).astype(BF16)
            return 0

        lax.fori_loop(0, 4, block, 0)

    def scale_of(rows):
        return lax.rsqrt(jnp.broadcast_to(rows, (128, 128)).T / depth + EPS)

    ky = [new(recvs, 7) for _ in range(2)]
    sy = [sender(buf.at[pl.ds(0, 7), pl.ds(0, 2)]) for buf in (XG, XG)]
    fewer(lambda n: XG.at[me, pl.ds(0, n)], 2, lambda ref: recv(ref, kx))
    y_start(XG, ky[0], sy[0], 0)
    recv(XG.at[me, pl.ds(2, 2)], kx + 1)
    y_start(XG, ky[1], sy[1], 1)
    km = new(recvs)
    sm = sender(SM.at[pl.ds(0, 15)])
    for i in range(15):
        send(smix, SM.at[f], sm, km, fs_peers[i])
    SM[f] = smix[...]
    last0, lastn, wide = layout[-1]
    for W in (WGU[-1], WVU[-1], WDN[-1]):
        for k in range(4):
            W[k, lastn:, :] = jnp.zeros((wide - lastn, 256), BF16)
    z_fwd(0)
    z_fwd(1)
    z_own(2)
    z_own(3)
    y_mid(XG, ky[0], sy[0], 0)
    y_mid(XG, ky[1], sy[1], 1)
    loads[1].wait()
    loads[2].wait()
    for w, kern, off in ((0, gkv, go), (1, vkv, vo)):
        CV[w, :, last0:] = jnp.zeros((4, wide), F32)
        CV[w, 0:3, 0:units] = kern[...]
        CV[w, 3:4, 0:units] = off[...].reshape(1, units)
    y_end(XG, ky[0], sy[0], 0)
    y_end(XG, ky[1], sy[1], 1)
    y_last(XG, ky[0])
    y_last(XG, ky[1])
    scaled(XG, mgain, False)
    z_fin(0)
    z_fin(1)
    for w, W in ((0, WGP), (1, WVP)):
        prod = jnp.dot(XS[...], W[...].reshape(1024, 256), preferred_element_type=F32)
        P1[:, :, w * 256 : w * 256 + 256] = prod.reshape(4, 128, 256)

    def row_loop(first, n, fn):
        def step(i, _):
            fn(pl.ds(pl.multiple_of(first + i * 16, 16), 16))
            return 0

        lax.fori_loop(0, n // 16, step, 0)

    ra, rb = pl.ds(0, 64), pl.ds(64, 64)

    def rounded_rows(p, S, i, first, n):
        def fn(rows):
            S[i % 3, rows, :] = p[i, rows, :].astype(BF16)

        row_loop(first, n, fn)

    def rs_far(p, S, H, F, k, s):
        rounded_rows(p, S, 3, 0, 128)
        send(S.at[0, ra], H.at[0], s, k, x_up)
        send(S.at[0, rb], H.at[1], s, k + 1, x_dn)

    def rs_first(p, S, H, F, k, s):
        rounded_rows(p, S, 1, 64, 64)
        send(S.at[1, rb], F.at[0, rb], s, k + 2, x_up)
        rounded_rows(p, S, 2, 0, 64)
        send(S.at[2, ra], F.at[1, ra], s, k + 2, x_dn)

    def rs_second(p, S, H, F, k, s):
        def left(rows):
            S[1, rows, :] = (p[1, rows, :] + H[0, rows, :].astype(F32)).astype(BF16)

        def right(rows):
            low = pl.ds(pl.multiple_of(rows.start + 64, 16), 16)
            S[2, low, :] = (p[2, low, :] + H[1, rows, :].astype(F32)).astype(BF16)

        recv(H.at[0], k)
        row_loop(0, 64, left)
        send(S.at[1, ra], F.at[0, ra], s, k + 2, x_up)
        recv(H.at[1], k + 1)
        row_loop(0, 64, right)
        send(S.at[2, rb], F.at[1, rb], s, k + 2, x_dn)

    def rs_wait(F, k):
        recv(F, k + 2)

    kr = [new(recvs, 3) for _ in layout]
    set1 = (P1, S1, H1, F1, kr[0], sender(S1))
    rs_far(*set1)
    rs_first(*set1)
    z_fwd(2)
    z_own(4)
    rs_second(*set1)
    z_fwd(3)
    z_own(5)
    recv(SM.at[pl.ds(0, 15)], km)
    recv(SSB.at[pl.ds(0, 7)], kss)
    rs_wait(F1, kr[0])

    total = P1[0] + F1[0].astype(F32) + F1[1].astype(F32)
    rs = scale_of(jnp.sum(SSB[...], axis=0)[0:1, :])
    eye = lax.broadcasted_iota(jnp.int32, (128, 128), 0) == lanes_of(128)
    for h in range(2):
        cols = slice(h * 128, h * 128 + 128)
        gated = gelu((rs * total[:, cols]).astype(BF16).astype(F32))
        spread = gelu((rs * total[:, 256 + h * 128 : 384 + h * 128]).astype(BF16).astype(F32))
        spread = spread * lax.rsqrt(jnp.mean(spread * spread, axis=-1, keepdims=True) + EPS)
        spread = (spread * vgain[h : h + 1, :]).astype(BF16)
        matrix = SM[:, h].astype(F32).reshape(128, 128).astype(BF16)
        mixed = jnp.dot(matrix, spread, preferred_element_type=F32)
        bias = jnp.broadcast_to(sbias[h : h + 1, :], (128, 128))
        mixed = mixed + jnp.sum(jnp.where(eye, bias, 0.0), axis=-1, keepdims=True)
        joined = gated * mixed
        joined = joined * lax.rsqrt(jnp.mean(joined * joined, axis=-1, keepdims=True) + EPS)
        MG[0, :, cols] = (joined * hgain[h : h + 1, :]).astype(BF16)

    k2 = new(recvs, 3)
    s2 = sender(MG.at[pl.ds(0, 3)])
    send(MG.at[0], MG.at[2], s2, k2 + 2, x_up)
    send(MG.at[0], MG.at[1], s2, k2 + 1, x_dn)
    send(MG.at[0], MG.at[3], s2, k2, x_far)
    z_fin(2)

    y_order = (far(y), up(y), down(y), y)

    def cy_first(g, product, CS, CR, k, s):
        for n, yt in enumerate(y_order):
            prod = product(yt)
            size = prod.shape[0] // 128
            rows = pl.ds(2 * g, size)
            T[n, rows] = jnp.where(c == 0, prod[:, :128], prod[:, 128:]).reshape(size, 128, 128)
            give = jnp.where(c == 0, prod[:, 128:], prod[:, :128]).astype(BF16)
            CS[n, rows] = give.reshape(size, 128, 128)
            send(CS.at[n, rows], CR.at[n, rows], s, k + n, mate)

    def joined_at(n, b, CR):
        return T[n, b] + CR[n, b].astype(F32)

    def cy_second(g, CR, YS, YH, YF, k, kc, s):
        a, b = 2 * g, 2 * g + 1
        recv(CR.at[0, pl.ds(a, 2)], kc)
        YS[0, a] = joined_at(0, a, CR).astype(BF16)
        YS[0, b] = joined_at(0, b, CR).astype(BF16)
        send(YS.at[0, a], YH.at[a], s, k, y_up)
        send(YS.at[0, b], YH.at[b], s, k + 1, y_dn)
        recv(CR.at[1, pl.ds(a, 2)], kc + 1)
        YS[1, b] = joined_at(1, b, CR).astype(BF16)
        send(YS.at[1, b], YF.at[g, 0, 1], s, k + 2, y_up)
        recv(CR.at[2, pl.ds(a, 2)], kc + 2)
        YS[2, a] = joined_at(2, a, CR).astype(BF16)
        send(YS.at[2, a], YF.at[g, 1, 0], s, k + 2, y_dn)

    def cy_third(g, CR, YS, YH, YF, k, kc, s):
        a, b = 2 * g, 2 * g + 1
        recv(YH.at[a], k)
        YS[1, a] = (joined_at(1, a, CR) + YH[a].astype(F32)).astype(BF16)
        send(YS.at[1, a], YF.at[g, 0, 0], s, k + 2, y_up)
        recv(YH.at[b], k + 1)
        YS[2, b] = (joined_at(2, b, CR) + YH[b].astype(F32)).astype(BF16)
        send(YS.at[2, b], YF.at[g, 1, 1], s, k + 2, y_dn)
        recv(CR.at[3, pl.ds(a, 2)], kc + 3)

    def cy_last(g, CR, YF, k):
        recv(YF.at[g], k + 2)
        return [
            joined_at(3, 2 * g + i, CR) + YF[g, 0, i].astype(F32) + YF[g, 1, i].astype(F32)
            for i in range(2)
        ]

    def merge(g):
        rows = MG[2 * g : 2 * g + 2].reshape(256, 256)
        return lambda yt: jnp.dot(rows, WMP[yt], preferred_element_type=F32)

    kc = [new(recvs, 4) for _ in range(2)]
    k3 = [new(recvs, 3) for _ in range(2)]
    sc, s3 = sender(CS4), sender(YS4)
    recv(MG.at[1], k2 + 1)
    cy_first(0, merge(0), CS4, CR4, kc[0], sc)
    cy_second(0, CR4, YS4, YH4, YF4, k3[0], kc[0], s3)
    recv(MG.at[2], k2 + 2)
    recv(MG.at[3], k2)
    cy_first(1, merge(1), CS4, CR4, kc[1], sc)
    cy_second(1, CR4, YS4, YH4, YF4, k3[1], kc[1], s3)
    z_fwd(4)
    z_own(6)
    cy_third(0, CR4, YS4, YH4, YF4, k3[0], kc[0], s3)
    cy_third(1, CR4, YS4, YH4, YF4, k3[1], kc[1], s3)

    ko = new(recvs)
    so = new(sends)
    ends.append(lambda: fewer(lambda n: HG.at[0, pl.ds(0, n)], 4, stay(so)))
    spot = 2 * lax.rem(x, 2) + c
    blocks = (x, up(x), down(x), far(x))
    sh = [sender(buf.at[pl.ds(0, 7), pl.ds(0, 2)]) for buf in (HG, HG)]
    for g in range(2):
        branch = cy_last(g, CR4, YF4, k3[g])
        for i in range(2):
            b = 2 * g + i
            HG[me, b] = (XG[me, b].astype(F32) + branch[i]).astype(BF16)
        y_start(HG, ky[g], sh[g], g)
    for b in range(4):
        if b:
            dst = HRES.at[spot]
            send(HG.at[me, b], dst, so, ko, at(x_=blocks[b], c_=x // 2))
            continue

        @pl.when(to_me)
        def _():
            HRES[spot] = HG[me, 0]

        @pl.when(jnp.logical_not(to_me))
        def _():
            send(HG.at[me, 0], HRES.at[spot], so, ko, mate)

    z_fwd(5)
    z_own(7)
    y_mid(HG, ky[0], sh[0], 0)
    y_mid(HG, ky[1], sh[1], 1)
    y_end(HG, ky[0], sh[0], 0)
    y_end(HG, ky[1], sh[1], 1)
    z_fwd(6)
    z_own(8)
    z_fin(weight("g", 0))
    z_fin(weight("v", 0))
    y_last(HG, ky[0])
    y_last(HG, ky[1])
    scaled(HG, fgain, True)
    kf = new(recvs)
    sf = sender(SSF.at[pl.ds(0, 3)])
    SSF[0] = SQR[0]
    send(SQR.at[1], SSF.at[2], sf, kf, x_up)
    send(SQR.at[2], SSF.at[1], sf, kf, x_dn)
    send(SQR.at[3], SSF.at[3], sf, kf, x_far)

    def project(W, p, n, first, only_far=False):
        def cut(cols, to, size):
            w = jnp.concatenate([W[k, cols, :] for k in range(4)], axis=1)
            rows = XS[384:512, :] if only_far else XS[...]
            prod = lax.dot_general(
                rows, w, (((1,), (1,)), ((), ())), preferred_element_type=F32
            )
            if only_far:
                p[3, :, to] = prod
            else:
                p[:, :, to] = prod.reshape(4, 128, size)

        def step(i, _):
            cut(
                pl.ds(pl.multiple_of(i * 256, 256), 256),
                pl.ds(pl.multiple_of(first + i * 256, 128), 256), 256,
            )
            return 0

        lax.fori_loop(0, n // 256, step, 0)
        left = n % 256
        if left:
            cut(pl.ds(n - left, left), pl.ds(first + n - left, left), left)

    def both(j, only_far=False):
        n = layout[j][2]
        project(WGU[j], PC[j], n, 0, only_far)
        project(WVU[j], PC[j], n, n, only_far)

    row = lax.broadcasted_iota(jnp.int32, (128, 128), 0)

    def activate(j):
        p, F, act = PC[j], FC[j], ACT[j]
        at0, _, n = layout[j]

        def conv_tile(i, _):
            def one(first, w):
                at_ = pl.ds(pl.multiple_of(first + i * 128, 128), 128)
                v = p[0, :, at_] + F[0, :, at_].astype(F32) + F[1, :, at_].astype(F32)
                v = (RS[...] * v).astype(BF16).astype(F32)
                prev = jnp.where(row == 0, 0.0, pltpu.roll(v, 1, axis=0))
                after = jnp.where(row == 127, 0.0, pltpu.roll(v, 127, axis=0))
                k = CV[w, :, pl.ds(pl.multiple_of(at0 + i * 128, 128), 128)]
                return k[3:4] + prev * k[0:1] + v * k[1:2] + after * k[2:3]

            cols = pl.ds(pl.multiple_of(i * 128, 128), 128)
            act[0, :, cols] = (gelu(one(0, 0)) * one(n, 1)).astype(BF16)
            return 0

        lax.fori_loop(0, n // 128, conv_tile, 0)

    sets = [
        (PC[j], SC[j], HC[j], FC[j], kr[j], sender(SC[j])) for j in range(chunks)
    ]
    kg = [new(recvs, 3) for _ in layout]
    sg = [sender(ACT[j].at[pl.ds(0, 3)]) for j in range(chunks)]

    def x_start(j):
        buf, k, s = ACT[j], kg[j], sg[j]
        send(buf.at[0, ra], buf.at[2, ra], s, k, x_up)
        send(buf.at[0, rb], buf.at[1, rb], s, k + 1, x_dn)
        send(buf.at[0, rb], buf.at[2, rb], s, k + 2, x_up)
        send(buf.at[0, ra], buf.at[1, ra], s, k + 2, x_dn)

    def x_mid(j):
        buf, k, s = ACT[j], kg[j], sg[j]
        recv(buf.at[2, ra], k)
        send(buf.at[2, ra], buf.at[3, ra], s, k + 2, x_up)
        recv(buf.at[1, rb], k + 1)
        send(buf.at[1, rb], buf.at[3, rb], s, k + 2, x_dn)

    def x_last(j):
        recv(ACT[j].at[pl.ds(0, 2)], kg[j] + 2)

    def down_early(j):
        def step(n, _):
            rows = ACT[j][...].reshape(512, layout[j][2])
            prod = jnp.dot(rows, WDN[j][n], preferred_element_type=F32)
            ACC[n] = prod if j == 0 else ACC[n] + prod
            return 0

        lax.fori_loop(0, 4, step, 0)

    both(0, True)
    rs_far(*sets[0])
    both(0)
    rs_first(*sets[0])
    z_fwd(7)
    rs_second(*sets[0])
    z_fin(weight("g", 1))
    z_fin(weight("v", 1))
    both(1)
    rs_far(*sets[1])
    rs_first(*sets[1])
    z_fwd(8)
    z_own(9)
    z_own(10)
    z_own(11)
    rs_second(*sets[1])
    z_fin(weight("g", 2))
    z_fin(weight("v", 2))
    both(2)
    rs_far(*sets[2])
    rs_first(*sets[2])
    recv(SSF.at[pl.ds(0, 3)], kf)
    RS[...] = scale_of(jnp.sum(SSF[...], axis=0)[0:1, :])
    rs_wait(FC[0], kr[0])
    activate(0)
    x_start(0)
    rs_second(*sets[2])
    rs_wait(FC[1], kr[1])
    activate(1)
    x_start(1)
    x_mid(0)
    z_fwd(9)
    rs_wait(FC[2], kr[2])
    activate(2)
    x_start(2)
    x_mid(1)
    z_fwd(10)
    z_fwd(11)
    x_mid(2)
    x_last(0)
    z_fin(9)
    down_early(0)
    x_last(1)
    z_fin(10)
    down_early(1)
    z_fin(11)
    x_last(2)

    final = ACT[2][...].reshape(512, layout[2][2])
    k7 = new(recvs, 4)
    s7 = sender(CS5)
    cy_first(
        0, lambda yt: jnp.dot(final, WDN[2][yt], preferred_element_type=F32) + ACC[yt],
        CS5, CR5, k7, s7,
    )
    kt = new(recvs)
    st = new(sends)
    ends.append(lambda: fewer(lambda n: TB.at[pl.ds(0, n)], 16, stay(st)))
    for n, yt in enumerate(y_order):
        recv(CR5.at[n], k7 + n)
        for b in range(4):
            i = 4 * n + b
            TB[i] = (T[n, b] + CR5[n, b].astype(F32)).astype(BF16)
            if i != 12:
                peer = at(x_=blocks[b], y_=yt, c_=x // 2)
                send(TB.at[i], TI.at[4 * y + spot], st, kt, peer)
                continue

            @pl.when(to_me)
            def _():
                TI[4 * y + spot] = TB[12]

            @pl.when(jnp.logical_not(to_me))
            def _():
                send(TB.at[12], TI.at[4 * y + spot], st, kt, mate)

    fewer(lambda n: HRES.at[pl.ds(0, n)], 4, lambda ref: recv(ref, ko))
    fewer(lambda n: TI.at[pl.ds(0, n)], 16, lambda ref: recv(ref, kt))
    for q in range(4):
        change = sum(TI[4 * n + q].astype(F32) for n in range(4))
        out[:, q * 128 : q * 128 + 128] = (HRES[q].astype(F32) + change).astype(BF16)
    for wait in ends:
        wait()
    assert sends[0] <= ssem.shape[0] and recvs[0] <= rsem.shape[0], (sends[0], recvs[0])


def body(
    tokens, mixer_gain, gate_proj, value_proj, value_gain, spatial_mix, spatial_bias,
    head_gain, merge_proj, ffn_gain, gate_up, value_up, gate_kernel, value_kernel,
    gate_offset, value_offset, down_proj,
):
    units = gate_up.shape[1]
    layout = []
    for first in range(0, units, CHUNK):
        n = min(CHUNK, units - first)
        layout.append((first, n, -(-n // 128) * 128))
    wide = sum(n for _, _, n in layout)
    widths = [n for _, _, n in layout]
    vm = lambda shape, dtype=BF16: pltpu.VMEM(shape, dtype)
    in_vmem = pl.BlockSpec(memory_space=pltpu.VMEM)
    left = pl.BlockSpec(memory_space=pl.ANY)
    call = pl.pallas_call(
        functools.partial(kernel, layout),
        out_shape=jax.ShapeDtypeStruct(tokens.shape, tokens.dtype),
        in_specs=[
            left, in_vmem, in_vmem, left, left, in_vmem, in_vmem, in_vmem, in_vmem, left,
            left, left, left, left, in_vmem, in_vmem, left,
        ],
        out_specs=in_vmem,
        scratch_shapes=[
            vm(tokens.shape), vm(gate_kernel.shape, F32), vm(gate_kernel.shape, F32),
            vm((2, 4, wide), F32),
            vm((8, 4, 128, 128)), vm((8, 4, 128, 128)), vm((512, 1024)),
            vm((4, 8, 128), F32), vm((128, 128), F32), vm((16, 2, 8, 128)),
            vm((4, 128, 256)), vm((8, 8, 128), F32), vm((4, 8, 128), F32), vm((4, 128, 128)),
            vm((16, 128, 128)), vm((16, 128, 128)),
            *[vm((4, 256, 256))] * 3, vm((4, 4, 128, 128), F32), vm((4, 512, 256), F32),
            vm((4, 128, 512), F32), vm((3, 128, 512)), vm((2, 64, 512)), vm((2, 128, 512)),
            vm((4, 4, 128, 128)), vm((4, 4, 128, 128)), vm((3, 4, 128, 128)),
            vm((4, 128, 128)), vm((2, 2, 2, 128, 128)),
            vm((4, 4, 128, 128)), vm((4, 4, 128, 128)),
            *[vm((4, n, 256)) for _ in range(3) for n in widths],
            *[vm((4, 128, n)) for n in widths],
            *[vm((4, 128, 2 * n), F32) for n in widths],
            *[vm((3, 128, 2 * n)) for n in widths],
            *[vm((2, 64, 2 * n)) for n in widths],
            *[vm((2, 128, 2 * n)) for n in widths],
            pltpu.SemaphoreType.DMA((SENDS,)), pltpu.SemaphoreType.DMA((RECVS,)),
            pltpu.SemaphoreType.DMA((6 + 3 * len(layout),)),
        ],
        compiler_params=pltpu.CompilerParams(
            collective_id=0, has_side_effects=True, vmem_limit_bytes=58 << 20
        ),
        name="layer",
    )
    return call(
        tokens, mixer_gain, ffn_gain, gate_proj, value_proj, value_gain, spatial_mix,
        spatial_bias, head_gain, merge_proj, gate_up.T, value_up.T, gate_kernel, value_kernel,
        gate_offset, value_offset, down_proj,
    )


def solution(mesh):
    finer = Mesh(
        mesh.devices.reshape(mesh.shape["rep"], 4, 4, 4, 2), ("rep", "fs_0", "fs_1", "tp_0", "tp_1")
    )
    return jax.shard_map(
        body,
        mesh=finer,
        in_specs=(
            P(REP_FS, TP), P(), P(FS, TP), P(FS, TP), P(TP, None), P(TP, FS, None),
            P(TP, None), P(TP, None), P(TP, FS), P(), P(FS, TP), P(FS, TP), P(None, TP),
            P(None, TP), P(TP), P(TP), P(TP, FS),
        ),
        out_specs=P(REP_FS, TP),
        check_vma=False,
    )
```

time: 661 us -> 111 us (0.17)
  the two profiles are of different devices: /device:TPU:57 before, /device:TPU:1 now
where the time goes in v5:
time: 111 us; the launch traced here: 110 us
  Pallas kernels  109 us (98%)
  local copies, waits for them, and re-layouts  1.57 us (1%)
    pallas_call x1, Pallas kernels, body(): call(tokens, mixer_gain, ffn_gain, gate_proj, value_proj, value_gain, spa...  109 us

profile of v5, /device:TPU:1, one launch (start us, length us, event | category | flops | bytes accessed | tf_op | source)
XLA Modules:
  0.0 110.5 jit_solution(8102864426165165947)
XLA Ops:
  0.0 108.9 %layer.1 = bf16[128,512]{1,0:T(8,128)(2,1)} custom-call(bf16[128,512]{1,0:T(8,128)(2,1)} %tok.1, f32[4096]{0:T(1024)} %mgain.1, f32[4096]{0:T(1024)} %fgain.1, bf16[256,256]{1,0:T(8,128)(2,1)} %gp.1, bf16[256,256]{1,0:T(8,128)(2,1)} %vp.1, f32[2,128]{1,0:T(2,128)} %vgain.1, bf16[2,8,128]{2,1,0:T(8,128)(2,1)} %smix.1, f32[2,128]{1,0:T(2,128)} %sbias.1, ...), custom_call_target="tpu_custom_call" | custom-call | tf_op jit(solution)/shard_map/layer/pallas_call | solution.py:677
  108.9 1.6 %copy.19 = bf16[128,512]{1,0:T(8,128)(2,1)} copy(bf16[128,512]{1,0:T(8,128)(2,1)} %layer.1) | data formatting | bytes 262144

commit v6 on v5

--- a/solution.py
+++ b/solution.py
@@ -13,7 +13,7 @@
 REP_FS = ("rep", "fs_0", "fs_1")
 MESH = pl.DeviceIdType.MESH
 EPS = 1e-06
-SENDS, RECVS = 33, 96
+SENDS, RECVS = 33, 103
 CHUNK = 512
 F32 = jnp.float32
 BF16 = jnp.bfloat16
@@ -145,7 +145,7 @@
         for h in range(2):
             xt = 2 * c + j
             ahead = lax.rem(x - xt + 4, 4)
-            place = jnp.where(ahead >= 2, 5 - ahead, ahead)
+            place = jnp.where(ahead == 0, 3, jnp.where(ahead == 2, 2, ahead // 2))
             mine = jnp.logical_and(xt == x, c == h)
             block = tokv.at[:, j * 256 + h * 128 : j * 256 + h * 128 + 128]
 
@@ -156,7 +156,7 @@
 
             @pl.when(mine)
             def _():
-                XG[2 * y + h, 0] = block[...]
+                XG[2 * y + h, 3] = block[...]
 
     def fewer(ref_of, n, wait):
         @pl.when(to_me)
@@ -209,7 +209,7 @@
     def y_last(buf, k):
         recv(buf.at[pl.ds(0, 4), pl.ds(0, 2)], k + 6)
 
-    def scaled(buf, gains, squares):
+    def scaled(buf, gains, squares, first, n):
         parts = [gains[pl.ds(pl.multiple_of((4 * k + x) * 256, 256), 256)] for k in range(4)]
         gain = jnp.concatenate([part.reshape(1, 256) for part in parts], axis=1)
 
@@ -221,16 +221,16 @@
             XS[pl.ds(pl.multiple_of(b * 128, 128), 128), :] = (rows * gain).astype(BF16)
             return 0
 
-        lax.fori_loop(0, 4, block, 0)
+        lax.fori_loop(first, first + n, block, 0)
 
     def scale_of(rows):
         return lax.rsqrt(jnp.broadcast_to(rows, (128, 128)).T / depth + EPS)
 
     ky = [new(recvs, 7) for _ in range(2)]
     sy = [sender(buf.at[pl.ds(0, 7), pl.ds(0, 2)]) for buf in (XG, XG)]
-    fewer(lambda n: XG.at[me, pl.ds(0, n)], 2, lambda ref: recv(ref, kx))
+    recv(XG.at[me, pl.ds(0, 2)], kx)
     y_start(XG, ky[0], sy[0], 0)
-    recv(XG.at[me, pl.ds(2, 2)], kx + 1)
+    fewer(lambda n: XG.at[me, pl.ds(0, n)], 2, lambda ref: recv(ref, kx + 1))
     y_start(XG, ky[1], sy[1], 1)
     km = new(recvs)
     sm = sender(SM.at[pl.ds(0, 15)])
@@ -257,7 +257,7 @@
     y_end(XG, ky[1], sy[1], 1)
     y_last(XG, ky[0])
     y_last(XG, ky[1])
-    scaled(XG, mgain, False)
+    scaled(XG, mgain, False, 0, 4)
     z_fin(0)
     z_fin(1)
     for w, W in ((0, WGP), (1, WVP)):
@@ -273,30 +273,30 @@
 
     ra, rb = pl.ds(0, 64), pl.ds(64, 64)
 
-    def rounded_rows(p, S, i, first, n):
+    def rounded_rows(p, i, S, k, first, n):
         def fn(rows):
-            S[i % 3, rows, :] = p[i, rows, :].astype(BF16)
+            S[k, rows, :] = p[i, rows, :].astype(BF16)
 
         row_loop(first, n, fn)
 
     def rs_far(p, S, H, F, k, s):
-        rounded_rows(p, S, 3, 0, 128)
+        rounded_rows(p, 2, S, 0, 0, 128)
         send(S.at[0, ra], H.at[0], s, k, x_up)
         send(S.at[0, rb], H.at[1], s, k + 1, x_dn)
 
     def rs_first(p, S, H, F, k, s):
-        rounded_rows(p, S, 1, 64, 64)
+        rounded_rows(p, 0, S, 1, 64, 64)
         send(S.at[1, rb], F.at[0, rb], s, k + 2, x_up)
-        rounded_rows(p, S, 2, 0, 64)
+        rounded_rows(p, 1, S, 2, 0, 64)
         send(S.at[2, ra], F.at[1, ra], s, k + 2, x_dn)
 
     def rs_second(p, S, H, F, k, s):
         def left(rows):
-            S[1, rows, :] = (p[1, rows, :] + H[0, rows, :].astype(F32)).astype(BF16)
+            S[1, rows, :] = (p[0, rows, :] + H[0, rows, :].astype(F32)).astype(BF16)
 
         def right(rows):
             low = pl.ds(pl.multiple_of(rows.start + 64, 16), 16)
-            S[2, low, :] = (p[2, low, :] + H[1, rows, :].astype(F32)).astype(BF16)
+            S[2, low, :] = (p[1, low, :] + H[1, rows, :].astype(F32)).astype(BF16)
 
         recv(H.at[0], k)
         row_loop(0, 64, left)
@@ -321,7 +321,7 @@
     recv(SSB.at[pl.ds(0, 7)], kss)
     rs_wait(F1, kr[0])
 
-    total = P1[0] + F1[0].astype(F32) + F1[1].astype(F32)
+    total = P1[3] + F1[0].astype(F32) + F1[1].astype(F32)
     rs = scale_of(jnp.sum(SSB[...], axis=0)[0:1, :])
     eye = lax.broadcasted_iota(jnp.int32, (128, 128), 0) == lanes_of(128)
     for h in range(2):
@@ -336,13 +336,13 @@
         mixed = mixed + jnp.sum(jnp.where(eye, bias, 0.0), axis=-1, keepdims=True)
         joined = gated * mixed
         joined = joined * lax.rsqrt(jnp.mean(joined * joined, axis=-1, keepdims=True) + EPS)
-        MG[0, :, cols] = (joined * hgain[h : h + 1, :]).astype(BF16)
+        MG[3, :, cols] = (joined * hgain[h : h + 1, :]).astype(BF16)
 
     k2 = new(recvs, 3)
     s2 = sender(MG.at[pl.ds(0, 3)])
-    send(MG.at[0], MG.at[2], s2, k2 + 2, x_up)
-    send(MG.at[0], MG.at[1], s2, k2 + 1, x_dn)
-    send(MG.at[0], MG.at[3], s2, k2, x_far)
+    send(MG.at[3], MG.at[1], s2, k2 + 1, x_up)
+    send(MG.at[3], MG.at[0], s2, k2 + 2, x_dn)
+    send(MG.at[3], MG.at[2], s2, k2, x_far)
     z_fin(2)
 
     y_order = (far(y), up(y), down(y), y)
@@ -398,11 +398,11 @@
     kc = [new(recvs, 4) for _ in range(2)]
     k3 = [new(recvs, 3) for _ in range(2)]
     sc, s3 = sender(CS4), sender(YS4)
+    recv(MG.at[0], k2 + 2)
     recv(MG.at[1], k2 + 1)
     cy_first(0, merge(0), CS4, CR4, kc[0], sc)
     cy_second(0, CR4, YS4, YH4, YF4, k3[0], kc[0], s3)
-    recv(MG.at[2], k2 + 2)
-    recv(MG.at[3], k2)
+    recv(MG.at[2], k2)
     cy_first(1, merge(1), CS4, CR4, kc[1], sc)
     cy_second(1, CR4, YS4, YH4, YF4, k3[1], kc[1], s3)
     z_fwd(4)
@@ -414,7 +414,7 @@
     so = new(sends)
     ends.append(lambda: fewer(lambda n: HG.at[0, pl.ds(0, n)], 4, stay(so)))
     spot = 2 * lax.rem(x, 2) + c
-    blocks = (x, up(x), down(x), far(x))
+    blocks = (up(x), down(x), far(x), x)
     sh = [sender(buf.at[pl.ds(0, 7), pl.ds(0, 2)]) for buf in (HG, HG)]
     for g in range(2):
         branch = cy_last(g, CR4, YF4, k3[g])
@@ -423,50 +423,40 @@
             HG[me, b] = (XG[me, b].astype(F32) + branch[i]).astype(BF16)
         y_start(HG, ky[g], sh[g], g)
     for b in range(4):
-        if b:
+        if b < 3:
             dst = HRES.at[spot]
             send(HG.at[me, b], dst, so, ko, at(x_=blocks[b], c_=x // 2))
             continue
 
         @pl.when(to_me)
         def _():
-            HRES[spot] = HG[me, 0]
+            HRES[spot] = HG[me, 3]
 
         @pl.when(jnp.logical_not(to_me))
         def _():
-            send(HG.at[me, 0], HRES.at[spot], so, ko, mate)
+            send(HG.at[me, 3], HRES.at[spot], so, ko, mate)
 
     z_fwd(5)
-    z_own(7)
     y_mid(HG, ky[0], sh[0], 0)
     y_mid(HG, ky[1], sh[1], 1)
     y_end(HG, ky[0], sh[0], 0)
+    z_fwd(6)
+    z_own(7)
+    z_own(8)
     y_end(HG, ky[1], sh[1], 1)
-    z_fwd(6)
-    z_own(8)
     z_fin(weight("g", 0))
     z_fin(weight("v", 0))
     y_last(HG, ky[0])
-    y_last(HG, ky[1])
-    scaled(HG, fgain, True)
-    kf = new(recvs)
-    sf = sender(SSF.at[pl.ds(0, 3)])
-    SSF[0] = SQR[0]
-    send(SQR.at[1], SSF.at[2], sf, kf, x_up)
-    send(SQR.at[2], SSF.at[1], sf, kf, x_dn)
-    send(SQR.at[3], SSF.at[3], sf, kf, x_far)
-
-    def project(W, p, n, first, only_far=False):
+    scaled(HG, fgain, True, 0, 2)
+
+    def project(W, p, n, first, b0, b1):
         def cut(cols, to, size):
             w = jnp.concatenate([W[k, cols, :] for k in range(4)], axis=1)
-            rows = XS[384:512, :] if only_far else XS[...]
             prod = lax.dot_general(
-                rows, w, (((1,), (1,)), ((), ())), preferred_element_type=F32
+                XS[b0 * 128 : b1 * 128, :], w, (((1,), (1,)), ((), ())),
+                preferred_element_type=F32,
             )
-            if only_far:
-                p[3, :, to] = prod
-            else:
-                p[:, :, to] = prod.reshape(4, 128, size)
+            p[b0:b1, :, to] = prod.reshape(b1 - b0, 128, size)
 
         def step(i, _):
             cut(
@@ -480,10 +470,10 @@
         if left:
             cut(pl.ds(n - left, left), pl.ds(first + n - left, left), left)
 
-    def both(j, only_far=False):
+    def both(j, b0=0, b1=4):
         n = layout[j][2]
-        project(WGU[j], PC[j], n, 0, only_far)
-        project(WVU[j], PC[j], n, n, only_far)
+        project(WGU[j], PC[j], n, 0, b0, b1)
+        project(WVU[j], PC[j], n, n, b0, b1)
 
     row = lax.broadcasted_iota(jnp.int32, (128, 128), 0)
 
@@ -494,7 +484,7 @@
         def conv_tile(i, _):
             def one(first, w):
                 at_ = pl.ds(pl.multiple_of(first + i * 128, 128), 128)
-                v = p[0, :, at_] + F[0, :, at_].astype(F32) + F[1, :, at_].astype(F32)
+                v = p[3, :, at_] + F[0, :, at_].astype(F32) + F[1, :, at_].astype(F32)
                 v = (RS[...] * v).astype(BF16).astype(F32)
                 prev = jnp.where(row == 0, 0.0, pltpu.roll(v, 1, axis=0))
                 after = jnp.where(row == 127, 0.0, pltpu.roll(v, 127, axis=0))
@@ -502,7 +492,7 @@
                 return k[3:4] + prev * k[0:1] + v * k[1:2] + after * k[2:3]
 
             cols = pl.ds(pl.multiple_of(i * 128, 128), 128)
-            act[0, :, cols] = (gelu(one(0, 0)) * one(n, 1)).astype(BF16)
+            act[3, :, cols] = (gelu(one(0, 0)) * one(n, 1)).astype(BF16)
             return 0
 
         lax.fori_loop(0, n // 128, conv_tile, 0)
@@ -510,110 +500,135 @@
     sets = [
         (PC[j], SC[j], HC[j], FC[j], kr[j], sender(SC[j])) for j in range(chunks)
     ]
-    kg = [new(recvs, 3) for _ in layout]
+    kg = [new(recvs, 4) for _ in layout]
     sg = [sender(ACT[j].at[pl.ds(0, 3)]) for j in range(chunks)]
 
     def x_start(j):
         buf, k, s = ACT[j], kg[j], sg[j]
-        send(buf.at[0, ra], buf.at[2, ra], s, k, x_up)
-        send(buf.at[0, rb], buf.at[1, rb], s, k + 1, x_dn)
-        send(buf.at[0, rb], buf.at[2, rb], s, k + 2, x_up)
-        send(buf.at[0, ra], buf.at[1, ra], s, k + 2, x_dn)
+        send(buf.at[3, ra], buf.at[1, ra], s, k, x_up)
+        send(buf.at[3, rb], buf.at[0, rb], s, k + 1, x_dn)
+        send(buf.at[3, rb], buf.at[1, rb], s, k + 2, x_up)
+        send(buf.at[3, ra], buf.at[0, ra], s, k + 2, x_dn)
 
     def x_mid(j):
         buf, k, s = ACT[j], kg[j], sg[j]
-        recv(buf.at[2, ra], k)
-        send(buf.at[2, ra], buf.at[3, ra], s, k + 2, x_up)
-        recv(buf.at[1, rb], k + 1)
-        send(buf.at[1, rb], buf.at[3, rb], s, k + 2, x_dn)
+        recv(buf.at[1, ra], k)
+        send(buf.at[1, ra], buf.at[2, ra], s, k + 3, x_up)
+        recv(buf.at[0, rb], k + 1)
+        send(buf.at[0, rb], buf.at[2, rb], s, k + 3, x_dn)
+
+    def x_near(j):
+        recv(ACT[j].at[0], kg[j] + 2)
 
     def x_last(j):
-        recv(ACT[j].at[pl.ds(0, 2)], kg[j] + 2)
-
-    def down_early(j):
-        def step(n, _):
-            rows = ACT[j][...].reshape(512, layout[j][2])
-            prod = jnp.dot(rows, WDN[j][n], preferred_element_type=F32)
-            ACC[n] = prod if j == 0 else ACC[n] + prod
+        recv(ACT[j].at[2], kg[j] + 3)
+
+    def down_rows(j, g):
+        n = layout[j][2]
+        rows = ACT[j][2 * g : 2 * g + 2].reshape(256, n)
+        return lambda k: jnp.dot(rows, WDN[j][k], preferred_element_type=F32)
+
+    def down_early(j, g):
+        product = down_rows(j, g)
+
+        def step(k, _):
+            prod = product(k)
+            ACC[k, g] = prod if j == 0 else ACC[k, g] + prod
             return 0
 
         lax.fori_loop(0, 4, step, 0)
 
-    both(0, True)
+    both(0, 0, 2)
+    rs_first(*sets[0])
+    y_last(HG, ky[1])
+    scaled(HG, fgain, True, 2, 2)
+    both(0, 2, 4)
     rs_far(*sets[0])
-    both(0)
-    rs_first(*sets[0])
-    z_fwd(7)
-    rs_second(*sets[0])
+    kf = new(recvs)
+    sf = sender(SSF.at[pl.ds(0, 3)])
+    SSF[3] = SQR[3]
+    send(SQR.at[0], SSF.at[1], sf, kf, x_up)
+    send(SQR.at[1], SSF.at[0], sf, kf, x_dn)
+    send(SQR.at[2], SSF.at[2], sf, kf, x_far)
     z_fin(weight("g", 1))
     z_fin(weight("v", 1))
     both(1)
+    rs_second(*sets[0])
     rs_far(*sets[1])
     rs_first(*sets[1])
+    z_fwd(7)
     z_fwd(8)
     z_own(9)
     z_own(10)
     z_own(11)
     rs_second(*sets[1])
+    recv(SSF.at[pl.ds(0, 3)], kf)
+    RS[...] = scale_of(jnp.sum(SSF[...], axis=0)[0:1, :])
+    rs_wait(FC[0], kr[0])
+    activate(0)
+    x_start(0)
     z_fin(weight("g", 2))
     z_fin(weight("v", 2))
     both(2)
     rs_far(*sets[2])
     rs_first(*sets[2])
-    recv(SSF.at[pl.ds(0, 3)], kf)
-    RS[...] = scale_of(jnp.sum(SSF[...], axis=0)[0:1, :])
-    rs_wait(FC[0], kr[0])
-    activate(0)
-    x_start(0)
-    rs_second(*sets[2])
     rs_wait(FC[1], kr[1])
     activate(1)
+    rs_second(*sets[2])
     x_start(1)
     x_mid(0)
     z_fwd(9)
+    x_near(0)
+    z_fin(9)
+    down_early(0, 0)
     rs_wait(FC[2], kr[2])
     activate(2)
     x_start(2)
     x_mid(1)
     z_fwd(10)
     z_fwd(11)
+    x_near(1)
+    z_fin(10)
+    down_early(1, 0)
     x_mid(2)
-    x_last(0)
-    z_fin(9)
-    down_early(0)
-    x_last(1)
-    z_fin(10)
-    down_early(1)
+    x_near(2)
     z_fin(11)
-    x_last(2)
-
-    final = ACT[2][...].reshape(512, layout[2][2])
-    k7 = new(recvs, 4)
+
+    k7 = [new(recvs, 4) for _ in range(2)]
     s7 = sender(CS5)
-    cy_first(
-        0, lambda yt: jnp.dot(final, WDN[2][yt], preferred_element_type=F32) + ACC[yt],
-        CS5, CR5, k7, s7,
-    )
     kt = new(recvs)
     st = new(sends)
     ends.append(lambda: fewer(lambda n: TB.at[pl.ds(0, n)], 16, stay(st)))
-    for n, yt in enumerate(y_order):
-        recv(CR5.at[n], k7 + n)
-        for b in range(4):
-            i = 4 * n + b
-            TB[i] = (T[n, b] + CR5[n, b].astype(F32)).astype(BF16)
-            if i != 12:
-                peer = at(x_=blocks[b], y_=yt, c_=x // 2)
-                send(TB.at[i], TI.at[4 * y + spot], st, kt, peer)
-                continue
-
-            @pl.when(to_me)
-            def _():
-                TI[4 * y + spot] = TB[12]
-
-            @pl.when(jnp.logical_not(to_me))
-            def _():
-                send(TB.at[12], TI.at[4 * y + spot], st, kt, mate)
+
+    def give(n, yt, b):
+        i = 4 * n + b
+        TB[i] = (T[n, b] + CR5[n, b].astype(F32)).astype(BF16)
+        dst = TI.at[4 * y + spot]
+        if i != 15:
+            send(TB.at[i], dst, st, kt, at(x_=blocks[b], y_=yt, c_=x // 2))
+            return
+
+        @pl.when(to_me)
+        def _():
+            TI[4 * y + spot] = TB[15]
+
+        @pl.when(jnp.logical_not(to_me))
+        def _():
+            send(TB.at[15], dst, st, kt, mate)
+
+    for g in range(2):
+        if g:
+            x_last(0)
+            down_early(0, 1)
+            x_last(1)
+            down_early(1, 1)
+            x_last(2)
+        product = down_rows(2, g)
+        cy_first(g, lambda yt: product(yt) + ACC[yt, g], CS5, CR5, k7[g], s7)
+        for n, yt in enumerate(y_order):
+            recv(CR5.at[n, pl.ds(2 * g, 2)], k7[g] + n)
+            for b in (2 * g, 2 * g + 1):
+                give(n, yt, b)
 
     fewer(lambda n: HRES.at[pl.ds(0, n)], 4, lambda ref: recv(ref, ko))
     fewer(lambda n: TI.at[pl.ds(0, n)], 16, lambda ref: recv(ref, kt))
@@ -655,7 +670,7 @@
             vm((4, 8, 128), F32), vm((128, 128), F32), vm((16, 2, 8, 128)),
             vm((4, 128, 256)), vm((8, 8, 128), F32), vm((4, 8, 128), F32), vm((4, 128, 128)),
             vm((16, 128, 128)), vm((16, 128, 128)),
-            *[vm((4, 256, 256))] * 3, vm((4, 4, 128, 128), F32), vm((4, 512, 256), F32),
+            *[vm((4, 256, 256))] * 3, vm((4, 4, 128, 128), F32), vm((4, 2, 256, 256), F32),
             vm((4, 128, 512), F32), vm((3, 128, 512)), vm((2, 64, 512)), vm((2, 128, 512)),
             vm((4, 4, 128, 128)), vm((4, 4, 128, 128)), vm((3, 4, 128, 128)),
             vm((4, 128, 128)), vm((2, 2, 2, 128, 128)),

time: 111 us -> 113 us (1.018)
  Pallas kernels: 109 us -> 111 us
    pallas_call x1, Pallas kernels: 109 us -> 111 us  [body(): call(tokens, mixer_gain, ffn_gain, gate_proj, value_proj, value_gain, spa...]
where the time goes in v6:
time: 113 us
  Pallas kernels  111 us (98%)
  local copies, waits for them, and re-layouts  1.57 us (1%)
    pallas_call x1, Pallas kernels, body(): call(tokens, mixer_gain, ffn_gain, gate_proj, value_proj, value_gain, spa...  111 us

profile of v6, /device:TPU:1, one launch (start us, length us, event | category | flops | bytes accessed | tf_op | source)
XLA Modules:
  0.0 112.8 jit_solution(13187403303249402859)
XLA Ops:
  0.0 111.3 %layer.1 = bf16[128,512]{1,0:T(8,128)(2,1)} custom-call(bf16[128,512]{1,0:T(8,128)(2,1)} %tok.1, f32[4096]{0:T(1024)} %mgain.1, f32[4096]{0:T(1024)} %fgain.1, bf16[256,256]{1,0:T(8,128)(2,1)} %gp.1, bf16[256,256]{1,0:T(8,128)(2,1)} %vp.1, f32[2,128]{1,0:T(2,128)} %vgain.1, bf16[2,8,128]{2,1,0:T(8,128)(2,1)} %smix.1, f32[2,128]{1,0:T(2,128)} %sbias.1, ...), custom_call_target="tpu_custom_call" | custom-call | tf_op jit(solution)/shard_map/layer/pallas_call | solution.py:692
  111.3 1.6 %copy.19 = bf16[128,512]{1,0:T(8,128)(2,1)} copy(bf16[128,512]{1,0:T(8,128)(2,1)} %layer.1) | data formatting | bytes 262144

commit v7 on v6

--- a/solution.py
+++ b/solution.py
@@ -560,7 +560,6 @@
     z_fwd(8)
     z_own(9)
     z_own(10)
-    z_own(11)
     rs_second(*sets[1])
     recv(SSF.at[pl.ds(0, 3)], kf)
     RS[...] = scale_of(jnp.sum(SSF[...], axis=0)[0:1, :])
@@ -572,25 +571,26 @@
     both(2)
     rs_far(*sets[2])
     rs_first(*sets[2])
+    z_fwd(9)
+    z_own(11)
     rs_wait(FC[1], kr[1])
     activate(1)
     rs_second(*sets[2])
     x_start(1)
     x_mid(0)
-    z_fwd(9)
-    x_near(0)
-    z_fin(9)
-    down_early(0, 0)
+    z_fwd(10)
     rs_wait(FC[2], kr[2])
     activate(2)
     x_start(2)
     x_mid(1)
-    z_fwd(10)
+    z_fin(9)
+    x_near(0)
+    down_early(0, 0)
     z_fwd(11)
+    x_mid(2)
+    z_fin(10)
     x_near(1)
-    z_fin(10)
     down_early(1, 0)
-    x_mid(2)
     x_near(2)
     z_fin(11)
 

time: 113 us -> 110 us (0.973)
  Pallas kernels: 111 us -> 109 us
    pallas_call x1, Pallas kernels: 111 us -> 109 us  [body(): call(tokens, mixer_gain, ffn_gain, gate_proj, value_proj, value_gain, spa...]
where the time goes in v7:
time: 110 us
  Pallas kernels  109 us (99%)
  local copies, waits for them, and re-layouts  1.57 us (1%)
    pallas_call x1, Pallas kernels, body(): call(tokens, mixer_gain, ffn_gain, gate_proj, value_proj, value_gain, spa...  109 us

profile of v7, /device:TPU:1, one launch (start us, length us, event | category | flops | bytes accessed | tf_op | source)
XLA Modules:
  0.0 110.2 jit_solution(8460833386457120443)
XLA Ops:
  0.0 108.6 %layer.1 = bf16[128,512]{1,0:T(8,128)(2,1)} custom-call(bf16[128,512]{1,0:T(8,128)(2,1)} %tok.1, f32[4096]{0:T(1024)} %mgain.1, f32[4096]{0:T(1024)} %fgain.1, bf16[256,256]{1,0:T(8,128)(2,1)} %gp.1, bf16[256,256]{1,0:T(8,128)(2,1)} %vp.1, f32[2,128]{1,0:T(2,128)} %vgain.1, bf16[2,8,128]{2,1,0:T(8,128)(2,1)} %smix.1, f32[2,128]{1,0:T(2,128)} %sbias.1, ...), custom_call_target="tpu_custom_call" | custom-call | tf_op jit(solution)/shard_map/layer/pallas_call | solution.py:692
  108.6 1.6 %copy.19 = bf16[128,512]{1,0:T(8,128)(2,1)} copy(bf16[128,512]{1,0:T(8,128)(2,1)} %layer.1) | data formatting | bytes 262144

commit v8 on v6

--- a/solution.py
+++ b/solution.py
@@ -29,7 +29,7 @@
 
 def kernel(layout, tok, mgain, fgain, gp, vp, vgain, smix, sbias, hgain, mp, gu, vu, gk, vk, go, vo,
            dn, out, tokv, gkv, vkv, CV, XG, HG, XS, SQR, RS, SM, MG, SSB, SSF, HRES, TB, TI,
-           WGP, WVP, WMP, T, ACC, P1, S1, H1, F1, CS4, CR4, YS4, YH4, YF4, CS5, CR5, *rest):
+           WGP, WVP, WMP, T, ACC, P1, S1, H1, F1, CS4, CR4, YS4, YH4, YF4, CS5, CR5, T5, *rest):
     chunks = len(layout)
     WGU, WVU, WDN, ACT, PC, SC, HC, FC = (rest[i * chunks : (i + 1) * chunks] for i in range(8))
     ssem, rsem, lsem = rest[8 * chunks :]
@@ -59,12 +59,21 @@
         g = lax.rem(f + i, 16)
         fs_peers.append(at(z_=g // 4, x_=lax.rem(g, 4)))
     near = []
-    for i in range(1, 16):
-        g = lax.rem(4 * y + x + i, 16)
-        near += [at(y_=g // 4, x_=lax.rem(g, 4), c_=jnp.int32(k)) for k in range(2)]
+    for i in range(1, 4):
+        near += [at(x_=lax.rem(x + i, 4), c_=k) for k in (c, other)]
+        near += [at(y_=lax.rem(y + i, 4), c_=other)]
+
+    def along(d, y_=None):
+        there = lax.rem(zr + 8 + d, 8)
+        return at(r_=there // 4, z_=lax.rem(there, 4), y_=y_)
+
+    for i in range(4):
+        for d in (-2, -1, 0, 1, 2):
+            if i or d:
+                near.append(along(d, lax.rem(y + i, 4)))
 
     barrier = pltpu.get_barrier_semaphore()
-    greet = [mate, z_up, z_dn] + near + fs_peers
+    greet = [mate] + near + fs_peers
     for peer in greet:
         pl.semaphore_signal(barrier, inc=1, device_id=peer, device_id_type=MESH)
     loads = [
@@ -108,25 +117,31 @@
 
     def z_local(i):
         src, buf, at0, n = pieces[i]
-        return pltpu.make_async_copy(src.at[pl.ds(at0, n)], buf.at[z, pl.ds(0, n)], lsem.at[3 + i])
+        own = buf.at[ring(i)[0], pl.ds(0, n)]
+        return pltpu.make_async_copy(src.at[pl.ds(at0, n)], own, lsem.at[3 + i])
+
+    def ring(i):
+        return (x, x_up, x_dn) if pieces[i][0] is dn else (z, z_up, z_dn)
 
     def z_own(i):
         src, buf, at0, n = pieces[i]
         a, b = pl.ds(0, n // 2), pl.ds(n // 2, n // 2)
         from_a, from_b = src.at[pl.ds(at0, n // 2)], src.at[pl.ds(at0 + n // 2, n // 2)]
-        send(from_a, buf.at[z, a], zs[i], zk[i], z_up)
-        send(from_b, buf.at[z, b], zs[i], zk[i] + 1, z_dn)
-        send(from_b, buf.at[z, b], zs[i], zk[i] + 2, z_up)
-        send(from_a, buf.at[z, a], zs[i], zk[i] + 2, z_dn)
+        place, above, below = ring(i)
+        send(from_a, buf.at[place, a], zs[i], zk[i], above)
+        send(from_b, buf.at[place, b], zs[i], zk[i] + 1, below)
+        send(from_b, buf.at[place, b], zs[i], zk[i] + 2, above)
+        send(from_a, buf.at[place, a], zs[i], zk[i] + 2, below)
         z_local(i).start()
 
     def z_fwd(i):
         _, buf, _, n = pieces[i]
-        a, b = buf.at[down(z), pl.ds(0, n // 2)], buf.at[up(z), pl.ds(n // 2, n // 2)]
+        place, above, below = ring(i)
+        a, b = buf.at[down(place), pl.ds(0, n // 2)], buf.at[up(place), pl.ds(n // 2, n // 2)]
         recv(a, zk[i])
-        send(a, a, zs[i], zk[i] + 2, z_up)
+        send(a, a, zs[i], zk[i] + 2, above)
         recv(b, zk[i] + 1)
-        send(b, b, zs[i], zk[i] + 2, z_dn)
+        send(b, b, zs[i], zk[i] + 2, below)
 
     def z_fin(i):
         _, buf, _, n = pieces[i]
@@ -158,12 +173,12 @@
             def _():
                 XG[2 * y + h, 3] = block[...]
 
-    def fewer(ref_of, n, wait):
-        @pl.when(to_me)
+    def fewer(ref_of, n, wait, stays=to_me):
+        @pl.when(stays)
         def _():
             wait(ref_of(n - 1))
 
-        @pl.when(jnp.logical_not(to_me))
+        @pl.when(jnp.logical_not(stays))
         def _():
             wait(ref_of(n))
 
@@ -241,6 +256,8 @@
     for W in (WGU[-1], WVU[-1], WDN[-1]):
         for k in range(4):
             W[k, lastn:, :] = jnp.zeros((wide - lastn, 256), BF16)
+    z_own(9)
+    z_own(11)
     z_fwd(0)
     z_fwd(1)
     z_own(2)
@@ -403,12 +420,17 @@
     cy_first(0, merge(0), CS4, CR4, kc[0], sc)
     cy_second(0, CR4, YS4, YH4, YF4, k3[0], kc[0], s3)
     recv(MG.at[2], k2)
+    z_own(10)
+    z_fwd(9)
+    z_fwd(11)
     cy_first(1, merge(1), CS4, CR4, kc[1], sc)
     cy_second(1, CR4, YS4, YH4, YF4, k3[1], kc[1], s3)
     z_fwd(4)
     z_own(6)
     cy_third(0, CR4, YS4, YH4, YF4, k3[0], kc[0], s3)
     cy_third(1, CR4, YS4, YH4, YF4, k3[1], kc[1], s3)
+
+    z_fwd(10)
 
     ko = new(recvs)
     so = new(sends)
@@ -505,17 +527,17 @@
 
     def x_start(j):
         buf, k, s = ACT[j], kg[j], sg[j]
-        send(buf.at[3, ra], buf.at[1, ra], s, k, x_up)
-        send(buf.at[3, rb], buf.at[0, rb], s, k + 1, x_dn)
-        send(buf.at[3, rb], buf.at[1, rb], s, k + 2, x_up)
-        send(buf.at[3, ra], buf.at[0, ra], s, k + 2, x_dn)
+        send(buf.at[3, ra], buf.at[1, ra], s, k, z_up)
+        send(buf.at[3, rb], buf.at[0, rb], s, k + 1, z_dn)
+        send(buf.at[3, rb], buf.at[1, rb], s, k + 2, z_up)
+        send(buf.at[3, ra], buf.at[0, ra], s, k + 2, z_dn)
 
     def x_mid(j):
         buf, k, s = ACT[j], kg[j], sg[j]
         recv(buf.at[1, ra], k)
-        send(buf.at[1, ra], buf.at[2, ra], s, k + 3, x_up)
+        send(buf.at[1, ra], buf.at[2, ra], s, k + 3, z_up)
         recv(buf.at[0, rb], k + 1)
-        send(buf.at[0, rb], buf.at[2, rb], s, k + 3, x_dn)
+        send(buf.at[0, rb], buf.at[2, rb], s, k + 3, z_dn)
 
     def x_near(j):
         recv(ACT[j].at[0], kg[j] + 2)
@@ -523,17 +545,17 @@
     def x_last(j):
         recv(ACT[j].at[2], kg[j] + 3)
 
-    def down_rows(j, g):
+    def down_rows(j, b0, b1):
         n = layout[j][2]
-        rows = ACT[j][2 * g : 2 * g + 2].reshape(256, n)
+        rows = ACT[j][b0:b1].reshape((b1 - b0) * 128, n)
         return lambda k: jnp.dot(rows, WDN[j][k], preferred_element_type=F32)
 
-    def down_early(j, g):
-        product = down_rows(j, g)
+    def down_early(j):
+        product = down_rows(j, 0, 4)
 
         def step(k, _):
-            prod = product(k)
-            ACC[k, g] = prod if j == 0 else ACC[k, g] + prod
+            prod = product(k).reshape(4, 128, 256)
+            ACC[k] = prod if j == 0 else ACC[k] + prod
             return 0
 
         lax.fori_loop(0, 4, step, 0)
@@ -558,9 +580,6 @@
     rs_first(*sets[1])
     z_fwd(7)
     z_fwd(8)
-    z_own(9)
-    z_own(10)
-    z_own(11)
     rs_second(*sets[1])
     recv(SSF.at[pl.ds(0, 3)], kf)
     RS[...] = scale_of(jnp.sum(SSF[...], axis=0)[0:1, :])
@@ -574,67 +593,75 @@
     rs_first(*sets[2])
     rs_wait(FC[1], kr[1])
     activate(1)
-    rs_second(*sets[2])
     x_start(1)
     x_mid(0)
-    z_fwd(9)
+    rs_second(*sets[2])
+    x_mid(1)
     x_near(0)
+    x_last(0)
     z_fin(9)
-    down_early(0, 0)
+    down_early(0)
     rs_wait(FC[2], kr[2])
     activate(2)
     x_start(2)
-    x_mid(1)
-    z_fwd(10)
-    z_fwd(11)
     x_near(1)
+    x_last(1)
     z_fin(10)
-    down_early(1, 0)
+    z_fin(11)
+    down_early(1)
     x_mid(2)
     x_near(2)
-    z_fin(11)
-
-    k7 = [new(recvs, 4) for _ in range(2)]
+
+    k7 = [new(recvs, 2) for _ in range(2)]
     s7 = sender(CS5)
     kt = new(recvs)
     st = new(sends)
-    ends.append(lambda: fewer(lambda n: TB.at[pl.ds(0, n)], 16, stay(st)))
-
-    def give(n, yt, b):
-        i = 4 * n + b
-        TB[i] = (T[n, b] + CR5[n, b].astype(F32)).astype(BF16)
-        dst = TI.at[4 * y + spot]
-        if i != 15:
-            send(TB.at[i], dst, st, kt, at(x_=blocks[b], y_=yt, c_=x // 2))
-            return
-
-        @pl.when(to_me)
-        def _():
-            TI[4 * y + spot] = TB[15]
-
-        @pl.when(jnp.logical_not(to_me))
-        def _():
-            send(TB.at[15], dst, st, kt, mate)
+    stays = y == z
+    ends.append(lambda: fewer(lambda n: TB.at[pl.ds(0, n)], 4, stay(st), stays))
+
+    def give(b):
+        for i in range(2):
+            TB[b, :, i * 256 : i * 256 + 256] = (T5[i, b] + CR5[i, b].astype(F32)).astype(BF16)
+        if b < 2:
+            send(TB.at[b], TI.at[y], st, kt, along(1 - 2 * b, z))
+        elif b == 2:
+            send(TB.at[b, ra], TI.at[y, ra], st, kt, along(-2, z))
+            send(TB.at[b, rb], TI.at[y, rb], st, kt, along(2, z))
+        else:
+
+            @pl.when(stays)
+            def _():
+                TI[y] = TB[b]
+
+            @pl.when(jnp.logical_not(stays))
+            def _():
+                send(TB.at[b], TI.at[y], st, kt, at(y_=z))
 
     for g in range(2):
         if g:
-            x_last(0)
-            down_early(0, 1)
-            x_last(1)
-            down_early(1, 1)
             x_last(2)
-        product = down_rows(2, g)
-        cy_first(g, lambda yt: product(yt) + ACC[yt, g], CS5, CR5, k7[g], s7)
-        for n, yt in enumerate(y_order):
-            recv(CR5.at[n, pl.ds(2 * g, 2)], k7[g] + n)
-            for b in (2 * g, 2 * g + 1):
-                give(n, yt, b)
+        rows = pl.ds(2 * g, 2)
+        product = down_rows(2, 2 * g, 2 * g + 2)
+
+        def final(k):
+            return product(k).reshape(2, 128, 256) + ACC[k, rows]
+
+        for i in range(2):
+            CS5[i, rows] = final(2 * other + i).astype(BF16)
+            send(CS5.at[i, rows], CR5.at[i, rows], s7, k7[g] + i, mate)
+        for i in range(2):
+            T5[i, rows] = final(2 * c + i)
+        for i in range(2):
+            recv(CR5.at[i, rows], k7[g] + i)
+        give(2 * g)
+        give(2 * g + 1)
 
     fewer(lambda n: HRES.at[pl.ds(0, n)], 4, lambda ref: recv(ref, ko))
-    fewer(lambda n: TI.at[pl.ds(0, n)], 16, lambda ref: recv(ref, kt))
+    fewer(lambda n: TI.at[pl.ds(0, n)], 4, lambda ref: recv(ref, kt), stays)
     for q in range(4):
-        change = sum(TI[4 * n + q].astype(F32) for n in range(4))
-        out[:, q * 128 : q * 128 + 128] = (HRES[q].astype(F32) + change).astype(BF16)
+        cols = slice(q * 128, q * 128 + 128)
+        change = sum(TI[n, :, cols].astype(F32) for n in range(4))
+        out[:, cols] = (HRES[q].astype(F32) + change).astype(BF16)
     for wait in ends:
         wait()
     assert sends[0] <= ssem.shape[0] and recvs[0] <= rsem.shape[0], (sends[0], recvs[0])
@@ -669,12 +696,12 @@
             vm((8, 4, 128, 128)), vm((8, 4, 128, 128)), vm((512, 1024)),
             vm((4, 8, 128), F32), vm((128, 128), F32), vm((16, 2, 8, 128)),
             vm((4, 128, 256)), vm((8, 8, 128), F32), vm((4, 8, 128), F32), vm((4, 128, 128)),
-            vm((16, 128, 128)), vm((16, 128, 128)),
-            *[vm((4, 256, 256))] * 3, vm((4, 4, 128, 128), F32), vm((4, 2, 256, 256), F32),
+            vm((4, 128, 512)), vm((4, 128, 512)),
+            *[vm((4, 256, 256))] * 3, vm((4, 4, 128, 128), F32), vm((4, 4, 128, 256), F32),
             vm((4, 128, 512), F32), vm((3, 128, 512)), vm((2, 64, 512)), vm((2, 128, 512)),
             vm((4, 4, 128, 128)), vm((4, 4, 128, 128)), vm((3, 4, 128, 128)),
             vm((4, 128, 128)), vm((2, 2, 2, 128, 128)),
-            vm((4, 4, 128, 128)), vm((4, 4, 128, 128)),
+            vm((2, 4, 128, 256)), vm((2, 4, 128, 256)), vm((2, 4, 128, 256), F32),
             *[vm((4, n, 256)) for _ in range(3) for n in widths],
             *[vm((4, 128, n)) for n in widths],
             *[vm((4, 128, 2 * n), F32) for n in widths],

time: 113 us -> 107 us (0.947)
  the two profiles are of different devices: /device:TPU:1 before, /device:TPU:57 now
where the time goes in v8:
time: 107 us; the launch traced here: 105 us
  Pallas kernels  103 us (96%)
  local copies, waits for them, and re-layouts  1.57 us (1%)
    pallas_call x1, Pallas kernels, body(): call(tokens, mixer_gain, ffn_gain, gate_proj, value_proj, value_gain, spa...  103 us

profile of v8, /device:TPU:57, one launch (start us, length us, event | category | flops | bytes accessed | tf_op | source)
XLA Modules:
  0.0 105.0 jit_solution(11425801073044707144)
XLA Ops:
  0.0 103.4 %layer.1 = bf16[128,512]{1,0:T(8,128)(2,1)} custom-call(bf16[128,512]{1,0:T(8,128)(2,1)} %tok.1, f32[4096]{0:T(1024)} %mgain.1, f32[4096]{0:T(1024)} %fgain.1, bf16[256,256]{1,0:T(8,128)(2,1)} %gp.1, bf16[256,256]{1,0:T(8,128)(2,1)} %vp.1, f32[2,128]{1,0:T(2,128)} %vgain.1, bf16[2,8,128]{2,1,0:T(8,128)(2,1)} %smix.1, f32[2,128]{1,0:T(2,128)} %sbias.1, ...), custom_call_target="tpu_custom_call" | custom-call | tf_op jit(solution)/shard_map/layer/pallas_call | solution.py:719
  103.5 1.6 %copy.19 = bf16[128,512]{1,0:T(8,128)(2,1)} copy(bf16[128,512]{1,0:T(8,128)(2,1)} %layer.1) | data formatting | bytes 262144

commit v9 on v8

--- a/solution.py
+++ b/solution.py
@@ -160,7 +160,7 @@
         for h in range(2):
             xt = 2 * c + j
             ahead = lax.rem(x - xt + 4, 4)
-            place = jnp.where(ahead == 0, 3, jnp.where(ahead == 2, 2, ahead // 2))
+            place = jnp.where(ahead == 0, 2, jnp.where(ahead == 2, 3, ahead // 2))
             mine = jnp.logical_and(xt == x, c == h)
             block = tokv.at[:, j * 256 + h * 128 : j * 256 + h * 128 + 128]
 
@@ -171,7 +171,7 @@
 
             @pl.when(mine)
             def _():
-                XG[2 * y + h, 3] = block[...]
+                XG[2 * y + h, 2] = block[...]
 
     def fewer(ref_of, n, wait, stays=to_me):
         @pl.when(stays)
@@ -297,7 +297,7 @@
         row_loop(first, n, fn)
 
     def rs_far(p, S, H, F, k, s):
-        rounded_rows(p, 2, S, 0, 0, 128)
+        rounded_rows(p, 3, S, 0, 0, 128)
         send(S.at[0, ra], H.at[0], s, k, x_up)
         send(S.at[0, rb], H.at[1], s, k + 1, x_dn)
 
@@ -338,7 +338,7 @@
     recv(SSB.at[pl.ds(0, 7)], kss)
     rs_wait(F1, kr[0])
 
-    total = P1[3] + F1[0].astype(F32) + F1[1].astype(F32)
+    total = P1[2] + F1[0].astype(F32) + F1[1].astype(F32)
     rs = scale_of(jnp.sum(SSB[...], axis=0)[0:1, :])
     eye = lax.broadcasted_iota(jnp.int32, (128, 128), 0) == lanes_of(128)
     for h in range(2):
@@ -353,13 +353,13 @@
         mixed = mixed + jnp.sum(jnp.where(eye, bias, 0.0), axis=-1, keepdims=True)
         joined = gated * mixed
         joined = joined * lax.rsqrt(jnp.mean(joined * joined, axis=-1, keepdims=True) + EPS)
-        MG[3, :, cols] = (joined * hgain[h : h + 1, :]).astype(BF16)
+        MG[2, :, cols] = (joined * hgain[h : h + 1, :]).astype(BF16)
 
     k2 = new(recvs, 3)
     s2 = sender(MG.at[pl.ds(0, 3)])
-    send(MG.at[3], MG.at[1], s2, k2 + 1, x_up)
-    send(MG.at[3], MG.at[0], s2, k2 + 2, x_dn)
-    send(MG.at[3], MG.at[2], s2, k2, x_far)
+    send(MG.at[2], MG.at[1], s2, k2 + 1, x_up)
+    send(MG.at[2], MG.at[0], s2, k2 + 2, x_dn)
+    send(MG.at[2], MG.at[3], s2, k2, x_far)
     z_fin(2)
 
     y_order = (far(y), up(y), down(y), y)
@@ -419,7 +419,7 @@
     recv(MG.at[1], k2 + 1)
     cy_first(0, merge(0), CS4, CR4, kc[0], sc)
     cy_second(0, CR4, YS4, YH4, YF4, k3[0], kc[0], s3)
-    recv(MG.at[2], k2)
+    recv(MG.at[3], k2)
     z_own(10)
     z_fwd(9)
     z_fwd(11)
@@ -430,13 +430,12 @@
     cy_third(0, CR4, YS4, YH4, YF4, k3[0], kc[0], s3)
     cy_third(1, CR4, YS4, YH4, YF4, k3[1], kc[1], s3)
 
-    z_fwd(10)
 
     ko = new(recvs)
     so = new(sends)
     ends.append(lambda: fewer(lambda n: HG.at[0, pl.ds(0, n)], 4, stay(so)))
     spot = 2 * lax.rem(x, 2) + c
-    blocks = (up(x), down(x), far(x), x)
+    blocks = (up(x), down(x), x, far(x))
     sh = [sender(buf.at[pl.ds(0, 7), pl.ds(0, 2)]) for buf in (HG, HG)]
     for g in range(2):
         branch = cy_last(g, CR4, YF4, k3[g])
@@ -445,18 +444,18 @@
             HG[me, b] = (XG[me, b].astype(F32) + branch[i]).astype(BF16)
         y_start(HG, ky[g], sh[g], g)
     for b in range(4):
-        if b < 3:
+        if b != 2:
             dst = HRES.at[spot]
             send(HG.at[me, b], dst, so, ko, at(x_=blocks[b], c_=x // 2))
             continue
 
         @pl.when(to_me)
         def _():
-            HRES[spot] = HG[me, 3]
+            HRES[spot] = HG[me, 2]
 
         @pl.when(jnp.logical_not(to_me))
         def _():
-            send(HG.at[me, 3], HRES.at[spot], so, ko, mate)
+            send(HG.at[me, 2], HRES.at[spot], so, ko, mate)
 
     z_fwd(5)
     y_mid(HG, ky[0], sh[0], 0)
@@ -465,6 +464,7 @@
     z_fwd(6)
     z_own(7)
     z_own(8)
+    z_fwd(10)
     y_end(HG, ky[1], sh[1], 1)
     z_fin(weight("g", 0))
     z_fin(weight("v", 0))
@@ -506,7 +506,7 @@
         def conv_tile(i, _):
             def one(first, w):
                 at_ = pl.ds(pl.multiple_of(first + i * 128, 128), 128)
-                v = p[3, :, at_] + F[0, :, at_].astype(F32) + F[1, :, at_].astype(F32)
+                v = p[2, :, at_] + F[0, :, at_].astype(F32) + F[1, :, at_].astype(F32)
                 v = (RS[...] * v).astype(BF16).astype(F32)
                 prev = jnp.where(row == 0, 0.0, pltpu.roll(v, 1, axis=0))
                 after = jnp.where(row == 127, 0.0, pltpu.roll(v, 127, axis=0))
@@ -514,7 +514,7 @@
                 return k[3:4] + prev * k[0:1] + v * k[1:2] + after * k[2:3]
 
             cols = pl.ds(pl.multiple_of(i * 128, 128), 128)
-            act[3, :, cols] = (gelu(one(0, 0)) * one(n, 1)).astype(BF16)
+            act[2, :, cols] = (gelu(one(0, 0)) * one(n, 1)).astype(BF16)
             return 0
 
         lax.fori_loop(0, n // 128, conv_tile, 0)
@@ -527,23 +527,23 @@
 
     def x_start(j):
         buf, k, s = ACT[j], kg[j], sg[j]
-        send(buf.at[3, ra], buf.at[1, ra], s, k, z_up)
-        send(buf.at[3, rb], buf.at[0, rb], s, k + 1, z_dn)
-        send(buf.at[3, rb], buf.at[1, rb], s, k + 2, z_up)
-        send(buf.at[3, ra], buf.at[0, ra], s, k + 2, z_dn)
+        send(buf.at[2, ra], buf.at[1, ra], s, k, z_up)
+        send(buf.at[2, rb], buf.at[0, rb], s, k + 1, z_dn)
+        send(buf.at[2, rb], buf.at[1, rb], s, k + 2, z_up)
+        send(buf.at[2, ra], buf.at[0, ra], s, k + 2, z_dn)
 
     def x_mid(j):
         buf, k, s = ACT[j], kg[j], sg[j]
         recv(buf.at[1, ra], k)
-        send(buf.at[1, ra], buf.at[2, ra], s, k + 3, z_up)
+        send(buf.at[1, ra], buf.at[3, ra], s, k + 3, z_up)
         recv(buf.at[0, rb], k + 1)
-        send(buf.at[0, rb], buf.at[2, rb], s, k + 3, z_dn)
+        send(buf.at[0, rb], buf.at[3, rb], s, k + 3, z_dn)
 
     def x_near(j):
         recv(ACT[j].at[0], kg[j] + 2)
 
     def x_last(j):
-        recv(ACT[j].at[2], kg[j] + 3)
+        recv(ACT[j].at[3], kg[j] + 3)
 
     def down_rows(j, b0, b1):
         n = layout[j][2]
@@ -568,15 +568,15 @@
     rs_far(*sets[0])
     kf = new(recvs)
     sf = sender(SSF.at[pl.ds(0, 3)])
-    SSF[3] = SQR[3]
+    SSF[2] = SQR[2]
     send(SQR.at[0], SSF.at[1], sf, kf, x_up)
     send(SQR.at[1], SSF.at[0], sf, kf, x_dn)
-    send(SQR.at[2], SSF.at[2], sf, kf, x_far)
+    send(SQR.at[3], SSF.at[3], sf, kf, x_far)
     z_fin(weight("g", 1))
     z_fin(weight("v", 1))
     both(1)
+    rs_far(*sets[1])
     rs_second(*sets[0])
-    rs_far(*sets[1])
     rs_first(*sets[1])
     z_fwd(7)
     z_fwd(8)
@@ -624,7 +624,7 @@
             TB[b, :, i * 256 : i * 256 + 256] = (T5[i, b] + CR5[i, b].astype(F32)).astype(BF16)
         if b < 2:
             send(TB.at[b], TI.at[y], st, kt, along(1 - 2 * b, z))
-        elif b == 2:
+        elif b == 3:
             send(TB.at[b, ra], TI.at[y, ra], st, kt, along(-2, z))
             send(TB.at[b, rb], TI.at[y, rb], st, kt, along(2, z))
         else:
@@ -637,14 +637,14 @@
             def _():
                 send(TB.at[b], TI.at[y], st, kt, at(y_=z))
 
-    for g in range(2):
+    for g, (b0, b1) in enumerate(((0, 3), (3, 4))):
         if g:
             x_last(2)
-        rows = pl.ds(2 * g, 2)
-        product = down_rows(2, 2 * g, 2 * g + 2)
+        rows = pl.ds(b0, b1 - b0)
+        product = down_rows(2, b0, b1)
 
         def final(k):
-            return product(k).reshape(2, 128, 256) + ACC[k, rows]
+            return product(k).reshape(b1 - b0, 128, 256) + ACC[k, rows]
 
         for i in range(2):
             CS5[i, rows] = final(2 * other + i).astype(BF16)
@@ -653,8 +653,8 @@
             T5[i, rows] = final(2 * c + i)
         for i in range(2):
             recv(CR5.at[i, rows], k7[g] + i)
-        give(2 * g)
-        give(2 * g + 1)
+        for b in range(b0, b1):
+            give(b)
 
     fewer(lambda n: HRES.at[pl.ds(0, n)], 4, lambda ref: recv(ref, ko))
     fewer(lambda n: TI.at[pl.ds(0, n)], 4, lambda ref: recv(ref, kt), stays)

time: 107 us -> 105 us (0.981); the launches traced: 105 us -> 104 us
  no operation moved by 1% of the time
where the time goes in v9:
time: 105 us; the launch traced here: 104 us
  Pallas kernels  103 us (98%)
  local copies, waits for them, and re-layouts  1.57 us (1%)
    pallas_call x1, Pallas kernels, body(): call(tokens, mixer_gain, ffn_gain, gate_proj, value_proj, value_gain, spa...  103 us

profile of v9, /device:TPU:57, one launch (start us, length us, event | category | flops | bytes accessed | tf_op | source)
XLA Modules:
  0.0 104.2 jit_solution(7430832817387692111)
XLA Ops:
  0.0 102.6 %layer.1 = bf16[128,512]{1,0:T(8,128)(2,1)} custom-call(bf16[128,512]{1,0:T(8,128)(2,1)} %tok.1, f32[4096]{0:T(1024)} %mgain.1, f32[4096]{0:T(1024)} %fgain.1, bf16[256,256]{1,0:T(8,128)(2,1)} %gp.1, bf16[256,256]{1,0:T(8,128)(2,1)} %vp.1, f32[2,128]{1,0:T(2,128)} %vgain.1, bf16[2,8,128]{2,1,0:T(8,128)(2,1)} %smix.1, f32[2,128]{1,0:T(2,128)} %sbias.1, ...), custom_call_target="tpu_custom_call" | custom-call | tf_op jit(solution)/shard_map/layer/pallas_call | solution.py:719
  102.6 1.6 %copy.19 = bf16[128,512]{1,0:T(8,128)(2,1)} copy(bf16[128,512]{1,0:T(8,128)(2,1)} %layer.1) | data formatting | bytes 262144

commit v10 on v9

--- a/solution.py
+++ b/solution.py
@@ -13,7 +13,7 @@
 REP_FS = ("rep", "fs_0", "fs_1")
 MESH = pl.DeviceIdType.MESH
 EPS = 1e-06
-SENDS, RECVS = 33, 103
+SENDS, RECVS = 33, 105
 CHUNK = 512
 F32 = jnp.float32
 BF16 = jnp.bfloat16
@@ -290,22 +290,22 @@
 
     ra, rb = pl.ds(0, 64), pl.ds(64, 64)
 
-    def rounded_rows(p, i, S, k, first, n):
+    def rounded_rows(p, i, S, k, first, n, cols):
         def fn(rows):
-            S[k, rows, :] = p[i, rows, :].astype(BF16)
+            S[k, rows, cols] = p[i, rows, cols].astype(BF16)
 
         row_loop(first, n, fn)
 
-    def rs_far(p, S, H, F, k, s):
-        rounded_rows(p, 3, S, 0, 0, 128)
-        send(S.at[0, ra], H.at[0], s, k, x_up)
-        send(S.at[0, rb], H.at[1], s, k + 1, x_dn)
-
-    def rs_first(p, S, H, F, k, s):
-        rounded_rows(p, 0, S, 1, 64, 64)
-        send(S.at[1, rb], F.at[0, rb], s, k + 2, x_up)
-        rounded_rows(p, 1, S, 2, 0, 64)
-        send(S.at[2, ra], F.at[1, ra], s, k + 2, x_dn)
+    def rs_far(p, S, H, F, k, s, cols=slice(None)):
+        rounded_rows(p, 3, S, 0, 0, 128, cols)
+        send(S.at[0, ra, cols], H.at[0, :, cols], s, k, x_up)
+        send(S.at[0, rb, cols], H.at[1, :, cols], s, k + 1, x_dn)
+
+    def rs_first(p, S, H, F, k, s, cols=slice(None)):
+        rounded_rows(p, 0, S, 1, 64, 64, cols)
+        send(S.at[1, rb, cols], F.at[0, rb, cols], s, k + 2, x_up)
+        rounded_rows(p, 1, S, 2, 0, 64, cols)
+        send(S.at[2, ra, cols], F.at[1, ra, cols], s, k + 2, x_dn)
 
     def rs_second(p, S, H, F, k, s):
         def left(rows):
@@ -497,6 +497,18 @@
         project(WGU[j], PC[j], n, 0, b0, b1)
         project(WVU[j], PC[j], n, n, b0, b1)
 
+    def gates(j):
+        n = layout[j][2]
+        z_fin(weight("g", j))
+        project(WGU[j], PC[j], n, 0, 0, 4)
+        return slice(0, n)
+
+    def values(j):
+        n = layout[j][2]
+        z_fin(weight("v", j))
+        project(WVU[j], PC[j], n, n, 0, 4)
+        return slice(n, 2 * n)
+
     row = lax.broadcasted_iota(jnp.int32, (128, 128), 0)
 
     def activate(j):
@@ -572,12 +584,13 @@
     send(SQR.at[0], SSF.at[1], sf, kf, x_up)
     send(SQR.at[1], SSF.at[0], sf, kf, x_dn)
     send(SQR.at[3], SSF.at[3], sf, kf, x_far)
-    z_fin(weight("g", 1))
-    z_fin(weight("v", 1))
-    both(1)
-    rs_far(*sets[1])
+    one1 = gates(1)
+    rs_far(*sets[1], one1)
+    rs_first(*sets[1], one1)
+    two1 = values(1)
+    rs_far(*sets[1], two1)
     rs_second(*sets[0])
-    rs_first(*sets[1])
+    rs_first(*sets[1], two1)
     z_fwd(7)
     z_fwd(8)
     rs_second(*sets[1])
@@ -586,11 +599,12 @@
     rs_wait(FC[0], kr[0])
     activate(0)
     x_start(0)
-    z_fin(weight("g", 2))
-    z_fin(weight("v", 2))
-    both(2)
-    rs_far(*sets[2])
-    rs_first(*sets[2])
+    one2 = gates(2)
+    rs_far(*sets[2], one2)
+    rs_first(*sets[2], one2)
+    two2 = values(2)
+    rs_far(*sets[2], two2)
+    rs_first(*sets[2], two2)
     rs_wait(FC[1], kr[1])
     activate(1)
     x_start(1)
@@ -609,10 +623,8 @@
     z_fin(10)
     z_fin(11)
     down_early(1)
-    x_mid(2)
-    x_near(2)
-
-    k7 = [new(recvs, 2) for _ in range(2)]
+
+    k7 = [new(recvs, 2) for _ in range(3)]
     s7 = sender(CS5)
     kt = new(recvs)
     st = new(sends)
@@ -637,9 +649,10 @@
             def _():
                 send(TB.at[b], TI.at[y], st, kt, at(y_=z))
 
-    for g, (b0, b1) in enumerate(((0, 3), (3, 4))):
-        if g:
-            x_last(2)
+    parts = ((2, 3), (0, 2), (3, 4))
+
+    def finish(g):
+        b0, b1 = parts[g]
         rows = pl.ds(b0, b1 - b0)
         product = down_rows(2, b0, b1)
 
@@ -651,10 +664,23 @@
             send(CS5.at[i, rows], CR5.at[i, rows], s7, k7[g] + i, mate)
         for i in range(2):
             T5[i, rows] = final(2 * c + i)
+
+    def hand_over(g):
+        b0, b1 = parts[g]
         for i in range(2):
-            recv(CR5.at[i, rows], k7[g] + i)
+            recv(CR5.at[i, pl.ds(b0, b1 - b0)], k7[g] + i)
         for b in range(b0, b1):
             give(b)
+
+    finish(0)
+    x_mid(2)
+    x_near(2)
+    finish(1)
+    hand_over(0)
+    hand_over(1)
+    x_last(2)
+    finish(2)
+    hand_over(2)
 
     fewer(lambda n: HRES.at[pl.ds(0, n)], 4, lambda ref: recv(ref, ko))
     fewer(lambda n: TI.at[pl.ds(0, n)], 4, lambda ref: recv(ref, kt), stays)

time: 105 us -> 105 us (level)
  no operation moved by 1% of the time
where the time goes in v10:
time: 105 us; the launch traced here: 104 us
  Pallas kernels  103 us (98%)
  local copies, waits for them, and re-layouts  1.57 us (1%)
    pallas_call x1, Pallas kernels, body(): call(tokens, mixer_gain, ffn_gain, gate_proj, value_proj, value_gain, spa...  103 us

profile of v10, /device:TPU:57, one launch (start us, length us, event | category | flops | bytes accessed | tf_op | source)
XLA Modules:
  0.0 104.5 jit_solution(7289985367342537692)
XLA Ops:
  0.0 102.9 %layer.1 = bf16[128,512]{1,0:T(8,128)(2,1)} custom-call(bf16[128,512]{1,0:T(8,128)(2,1)} %tok.1, f32[4096]{0:T(1024)} %mgain.1, f32[4096]{0:T(1024)} %fgain.1, bf16[256,256]{1,0:T(8,128)(2,1)} %gp.1, bf16[256,256]{1,0:T(8,128)(2,1)} %vp.1, f32[2,128]{1,0:T(2,128)} %vgain.1, bf16[2,8,128]{2,1,0:T(8,128)(2,1)} %smix.1, f32[2,128]{1,0:T(2,128)} %sbias.1, ...), custom_call_target="tpu_custom_call" | custom-call | tf_op jit(solution)/shard_map/layer/pallas_call | solution.py:745
  102.9 1.6 %copy.19 = bf16[128,512]{1,0:T(8,128)(2,1)} copy(bf16[128,512]{1,0:T(8,128)(2,1)} %layer.1) | data formatting | bytes 262144

commit v11 on v10

--- a/solution.py
+++ b/solution.py
@@ -53,6 +53,7 @@
     z_dn = at(r_=zd // 4, z_=lax.rem(zd, 4))
     x_up, x_dn, x_far = at(x_=up(x)), at(x_=down(x)), at(x_=far(x))
     y_up, y_dn = at(y_=up(y)), at(y_=down(y))
+    y_up_mate, y_dn_mate = at(y_=up(y), c_=other), at(y_=down(y), c_=other)
     mate = at(c_=other)
     fs_peers = []
     for i in range(1, 16):
@@ -210,16 +211,19 @@
         a, b = buf.at[lo_y, 2 * g], buf.at[hi_y, 2 * g + 1]
         recv(a, k)
         send(a, a, s, k + 4, y_up)
+        send(a, a, s, k + 6, y_up_mate)
         send(a, a, s, k + 6, mate)
         recv(b, k + 1)
         send(b, b, s, k + 5, y_dn)
+        send(b, b, s, k + 6, y_dn_mate)
         send(b, b, s, k + 6, mate)
 
     def y_end(buf, k, s, g):
         rows = (buf.at[lo_y, 2 * g + 1], buf.at[hi_y, 2 * g], buf.at[far_y, 2 * g], buf.at[far_y, 2 * g + 1])
         for i, ref in enumerate(rows):
             recv(ref, k + 2 + i)
-            send(ref, ref, s, k + 6, mate)
+            if i < 2:
+                send(ref, ref, s, k + 6, mate)
 
     def y_last(buf, k):
         recv(buf.at[pl.ds(0, 4), pl.ds(0, 2)], k + 6)
@@ -492,11 +496,6 @@
         if left:
             cut(pl.ds(n - left, left), pl.ds(first + n - left, left), left)
 
-    def both(j, b0=0, b1=4):
-        n = layout[j][2]
-        project(WGU[j], PC[j], n, 0, b0, b1)
-        project(WVU[j], PC[j], n, n, b0, b1)
-
     def gates(j):
         n = layout[j][2]
         z_fin(weight("g", j))
@@ -572,12 +571,18 @@
 
         lax.fori_loop(0, 4, step, 0)
 
-    both(0, 0, 2)
-    rs_first(*sets[0])
+    n0 = layout[0][2]
+    one0, two0 = slice(0, n0), slice(n0, 2 * n0)
+    project(WGU[0], PC[0], n0, 0, 0, 2)
+    rs_first(*sets[0], one0)
+    project(WVU[0], PC[0], n0, n0, 0, 2)
+    rs_first(*sets[0], two0)
     y_last(HG, ky[1])
     scaled(HG, fgain, True, 2, 2)
-    both(0, 2, 4)
-    rs_far(*sets[0])
+    project(WGU[0], PC[0], n0, 0, 2, 4)
+    rs_far(*sets[0], one0)
+    project(WVU[0], PC[0], n0, n0, 2, 4)
+    rs_far(*sets[0], two0)
     kf = new(recvs)
     sf = sender(SSF.at[pl.ds(0, 3)])
     SSF[2] = SQR[2]
@@ -586,9 +591,9 @@
     send(SQR.at[3], SSF.at[3], sf, kf, x_far)
     one1 = gates(1)
     rs_far(*sets[1], one1)
-    rs_first(*sets[1], one1)
     two1 = values(1)
     rs_far(*sets[1], two1)
+    rs_first(*sets[1], one1)
     rs_second(*sets[0])
     rs_first(*sets[1], two1)
     z_fwd(7)
@@ -601,10 +606,9 @@
     x_start(0)
     one2 = gates(2)
     rs_far(*sets[2], one2)
-    rs_first(*sets[2], one2)
     two2 = values(2)
     rs_far(*sets[2], two2)
-    rs_first(*sets[2], two2)
+    rs_first(*sets[2])
     rs_wait(FC[1], kr[1])
     activate(1)
     x_start(1)
@@ -674,9 +678,9 @@
 
     finish(0)
     x_mid(2)
+    hand_over(0)
     x_near(2)
     finish(1)
-    hand_over(0)
     hand_over(1)
     x_last(2)
     finish(2)

time: 105 us -> 105 us (level)
  no operation moved by 1% of the time
where the time goes in v11:
time: 105 us
  Pallas kernels  103 us (98%)
  local copies, waits for them, and re-layouts  1.57 us (1%)
    pallas_call x1, Pallas kernels, body(): call(tokens, mixer_gain, ffn_gain, gate_proj, value_proj, value_gain, spa...  103 us

profile of v11, /device:TPU:57, one launch (start us, length us, event | category | flops | bytes accessed | tf_op | source)
XLA Modules:
  0.0 104.6 jit_solution(14282688375817973644)
XLA Ops:
  0.0 103.1 %layer.1 = bf16[128,512]{1,0:T(8,128)(2,1)} custom-call(bf16[128,512]{1,0:T(8,128)(2,1)} %tok.1, f32[4096]{0:T(1024)} %mgain.1, f32[4096]{0:T(1024)} %fgain.1, bf16[256,256]{1,0:T(8,128)(2,1)} %gp.1, bf16[256,256]{1,0:T(8,128)(2,1)} %vp.1, f32[2,128]{1,0:T(2,128)} %vgain.1, bf16[2,8,128]{2,1,0:T(8,128)(2,1)} %smix.1, f32[2,128]{1,0:T(2,128)} %sbias.1, ...), custom_call_target="tpu_custom_call" | custom-call | tf_op jit(solution)/shard_map/layer/pallas_call | solution.py:749
  103.1 1.6 %copy.19 = bf16[128,512]{1,0:T(8,128)(2,1)} copy(bf16[128,512]{1,0:T(8,128)(2,1)} %layer.1) | data formatting | bytes 262144

commit v12 on v11

--- a/solution.py
+++ b/solution.py
@@ -615,13 +615,13 @@
     x_mid(0)
     rs_second(*sets[2])
     x_mid(1)
+    rs_wait(FC[2], kr[2])
+    activate(2)
+    x_start(2)
     x_near(0)
     x_last(0)
     z_fin(9)
     down_early(0)
-    rs_wait(FC[2], kr[2])
-    activate(2)
-    x_start(2)
     x_near(1)
     x_last(1)
     z_fin(10)
@@ -676,11 +676,11 @@
         for b in range(b0, b1):
             give(b)
 
+    x_mid(2)
     finish(0)
-    x_mid(2)
-    hand_over(0)
     x_near(2)
     finish(1)
+    hand_over(0)
     hand_over(1)
     x_last(2)
     finish(2)

time: 105 us -> 103 us (0.981)
  Pallas kernels: 103 us -> 101 us
    pallas_call x1, Pallas kernels: 103 us -> 101 us  [body(): call(tokens, mixer_gain, ffn_gain, gate_proj, value_proj, value_gain, spa...]
where the time goes in v12:
time: 103 us; the launch traced here: 102 us
  Pallas kernels  101 us (98%)
  local copies, waits for them, and re-layouts  1.57 us (2%)
    pallas_call x1, Pallas kernels, body(): call(tokens, mixer_gain, ffn_gain, gate_proj, value_proj, value_gain, spa...  101 us

profile of v12, /device:TPU:57, one launch (start us, length us, event | category | flops | bytes accessed | tf_op | source)
XLA Modules:
  0.0 102.2 jit_solution(13219249304543509262)
XLA Ops:
  0.0 100.6 %layer.1 = bf16[128,512]{1,0:T(8,128)(2,1)} custom-call(bf16[128,512]{1,0:T(8,128)(2,1)} %tok.1, f32[4096]{0:T(1024)} %mgain.1, f32[4096]{0:T(1024)} %fgain.1, bf16[256,256]{1,0:T(8,128)(2,1)} %gp.1, bf16[256,256]{1,0:T(8,128)(2,1)} %vp.1, f32[2,128]{1,0:T(2,128)} %vgain.1, bf16[2,8,128]{2,1,0:T(8,128)(2,1)} %smix.1, f32[2,128]{1,0:T(2,128)} %sbias.1, ...), custom_call_target="tpu_custom_call" | custom-call | tf_op jit(solution)/shard_map/layer/pallas_call | solution.py:749
  100.6 1.6 %copy.19 = bf16[128,512]{1,0:T(8,128)(2,1)} copy(bf16[128,512]{1,0:T(8,128)(2,1)} %layer.1) | data formatting | bytes 262144

commit v13 on v12

--- a/solution.py
+++ b/solution.py
@@ -198,32 +198,37 @@
 
     lo_y, hi_y, far_y = 2 * down(y) + c, 2 * up(y) + c, 2 * far(y) + c
 
-    def y_start(buf, k, s, g):
+    def y_start(buf, k, s, g, direct=False):
         a, b = buf.at[me, 2 * g], buf.at[me, 2 * g + 1]
         send(a, a, s, k, y_up)
         send(b, b, s, k + 1, y_dn)
         send(b, b, s, k + 2, y_up)
         send(a, a, s, k + 3, y_dn)
         both = buf.at[me, pl.ds(2 * g, 2)]
+        if direct:
+            send(both, both, s, k + 4, at(y_=far(y)))
         send(both, both, s, k + 6, mate)
 
-    def y_mid(buf, k, s, g):
+    def y_mid(buf, k, s, g, direct=False):
         a, b = buf.at[lo_y, 2 * g], buf.at[hi_y, 2 * g + 1]
-        recv(a, k)
-        send(a, a, s, k + 4, y_up)
-        send(a, a, s, k + 6, y_up_mate)
-        send(a, a, s, k + 6, mate)
-        recv(b, k + 1)
-        send(b, b, s, k + 5, y_dn)
-        send(b, b, s, k + 6, y_dn_mate)
-        send(b, b, s, k + 6, mate)
-
-    def y_end(buf, k, s, g):
-        rows = (buf.at[lo_y, 2 * g + 1], buf.at[hi_y, 2 * g], buf.at[far_y, 2 * g], buf.at[far_y, 2 * g + 1])
-        for i, ref in enumerate(rows):
+        for ref, i, there, there_mate in ((a, 0, y_up, y_up_mate), (b, 1, y_dn, y_dn_mate)):
+            recv(ref, k + i)
+            if not direct:
+                send(ref, ref, s, k + 4 + i, there)
+                send(ref, ref, s, k + 6, there_mate)
+            send(ref, ref, s, k + 6, mate)
+
+    def y_end(buf, k, s, g, direct=False):
+        for i, ref in enumerate((buf.at[lo_y, 2 * g + 1], buf.at[hi_y, 2 * g])):
             recv(ref, k + 2 + i)
-            if i < 2:
-                send(ref, ref, s, k + 6, mate)
+            send(ref, ref, s, k + 6, mate)
+        if direct:
+            ref = buf.at[far_y, pl.ds(2 * g, 2)]
+            recv(ref, k + 4)
+            send(ref, ref, s, k + 6, mate)
+        else:
+            recv(buf.at[far_y, 2 * g], k + 4)
+            recv(buf.at[far_y, 2 * g + 1], k + 5)
 
     def y_last(buf, k):
         recv(buf.at[pl.ds(0, 4), pl.ds(0, 2)], k + 6)
@@ -446,7 +451,7 @@
         for i in range(2):
             b = 2 * g + i
             HG[me, b] = (XG[me, b].astype(F32) + branch[i]).astype(BF16)
-        y_start(HG, ky[g], sh[g], g)
+        y_start(HG, ky[g], sh[g], g, g == 0)
     for b in range(4):
         if b != 2:
             dst = HRES.at[spot]
@@ -462,9 +467,9 @@
             send(HG.at[me, 2], HRES.at[spot], so, ko, mate)
 
     z_fwd(5)
-    y_mid(HG, ky[0], sh[0], 0)
+    y_mid(HG, ky[0], sh[0], 0, True)
     y_mid(HG, ky[1], sh[1], 1)
-    y_end(HG, ky[0], sh[0], 0)
+    y_end(HG, ky[0], sh[0], 0, True)
     z_fwd(6)
     z_own(7)
     z_own(8)
@@ -536,19 +541,25 @@
     kg = [new(recvs, 4) for _ in layout]
     sg = [sender(ACT[j].at[pl.ds(0, 3)]) for j in range(chunks)]
 
-    def x_start(j):
+    def x_start(j, direct=False):
         buf, k, s = ACT[j], kg[j], sg[j]
         send(buf.at[2, ra], buf.at[1, ra], s, k, z_up)
         send(buf.at[2, rb], buf.at[0, rb], s, k + 1, z_dn)
         send(buf.at[2, rb], buf.at[1, rb], s, k + 2, z_up)
         send(buf.at[2, ra], buf.at[0, ra], s, k + 2, z_dn)
 
-    def x_mid(j):
+        if direct:
+            send(buf.at[2, ra], buf.at[3, ra], s, k + 3, along(2))
+            send(buf.at[2, rb], buf.at[3, rb], s, k + 3, along(-2))
+
+    def x_mid(j, direct=False):
         buf, k, s = ACT[j], kg[j], sg[j]
         recv(buf.at[1, ra], k)
-        send(buf.at[1, ra], buf.at[3, ra], s, k + 3, z_up)
+        if not direct:
+            send(buf.at[1, ra], buf.at[3, ra], s, k + 3, z_up)
         recv(buf.at[0, rb], k + 1)
-        send(buf.at[0, rb], buf.at[3, rb], s, k + 3, z_dn)
+        if not direct:
+            send(buf.at[0, rb], buf.at[3, rb], s, k + 3, z_dn)
 
     def x_near(j):
         recv(ACT[j].at[0], kg[j] + 2)
@@ -591,9 +602,9 @@
     send(SQR.at[3], SSF.at[3], sf, kf, x_far)
     one1 = gates(1)
     rs_far(*sets[1], one1)
+    rs_first(*sets[1], one1)
     two1 = values(1)
     rs_far(*sets[1], two1)
-    rs_first(*sets[1], one1)
     rs_second(*sets[0])
     rs_first(*sets[1], two1)
     z_fwd(7)
@@ -617,7 +628,7 @@
     x_mid(1)
     rs_wait(FC[2], kr[2])
     activate(2)
-    x_start(2)
+    x_start(2, True)
     x_near(0)
     x_last(0)
     z_fin(9)
@@ -676,8 +687,8 @@
         for b in range(b0, b1):
             give(b)
 
-    x_mid(2)
     finish(0)
+    x_mid(2, True)
     x_near(2)
     finish(1)
     hand_over(0)

time: 103 us -> 104 us (level)
    pallas_call x1, Pallas kernels: 101 us -> 102 us  [body(): call(tokens, mixer_gain, ffn_gain, gate_proj, value_proj, value_gain, spa...]
where the time goes in v13:
time: 104 us; the launch traced here: 103 us
  Pallas kernels  102 us (98%)
  local copies, waits for them, and re-layouts  1.57 us (2%)
    pallas_call x1, Pallas kernels, body(): call(tokens, mixer_gain, ffn_gain, gate_proj, value_proj, value_gain, spa...  102 us

profile of v13, /device:TPU:57, one launch (start us, length us, event | category | flops | bytes accessed | tf_op | source)
XLA Modules:
  0.0 103.4 jit_solution(13773054591310177382)
XLA Ops:
  0.0 101.8 %layer.1 = bf16[128,512]{1,0:T(8,128)(2,1)} custom-call(bf16[128,512]{1,0:T(8,128)(2,1)} %tok.1, f32[4096]{0:T(1024)} %mgain.1, f32[4096]{0:T(1024)} %fgain.1, bf16[256,256]{1,0:T(8,128)(2,1)} %gp.1, bf16[256,256]{1,0:T(8,128)(2,1)} %vp.1, f32[2,128]{1,0:T(2,128)} %vgain.1, bf16[2,8,128]{2,1,0:T(8,128)(2,1)} %smix.1, f32[2,128]{1,0:T(2,128)} %sbias.1, ...), custom_call_target="tpu_custom_call" | custom-call | tf_op jit(solution)/shard_map/layer/pallas_call | solution.py:760
  101.8 1.6 %copy.19 = bf16[128,512]{1,0:T(8,128)(2,1)} copy(bf16[128,512]{1,0:T(8,128)(2,1)} %layer.1) | data formatting | bytes 262144

commit v14 on v13

--- a/solution.py
+++ b/solution.py
@@ -470,11 +470,6 @@
     y_mid(HG, ky[0], sh[0], 0, True)
     y_mid(HG, ky[1], sh[1], 1)
     y_end(HG, ky[0], sh[0], 0, True)
-    z_fwd(6)
-    z_own(7)
-    z_own(8)
-    z_fwd(10)
-    y_end(HG, ky[1], sh[1], 1)
     z_fin(weight("g", 0))
     z_fin(weight("v", 0))
     y_last(HG, ky[0])
@@ -586,8 +581,13 @@
     one0, two0 = slice(0, n0), slice(n0, 2 * n0)
     project(WGU[0], PC[0], n0, 0, 0, 2)
     rs_first(*sets[0], one0)
+    z_fwd(6)
+    z_own(7)
+    z_own(8)
+    z_fwd(10)
     project(WVU[0], PC[0], n0, n0, 0, 2)
     rs_first(*sets[0], two0)
+    y_end(HG, ky[1], sh[1], 1)
     y_last(HG, ky[1])
     scaled(HG, fgain, True, 2, 2)
     project(WGU[0], PC[0], n0, 0, 2, 4)
@@ -612,11 +612,11 @@
     rs_second(*sets[1])
     recv(SSF.at[pl.ds(0, 3)], kf)
     RS[...] = scale_of(jnp.sum(SSF[...], axis=0)[0:1, :])
+    one2 = gates(2)
+    rs_far(*sets[2], one2)
     rs_wait(FC[0], kr[0])
     activate(0)
     x_start(0)
-    one2 = gates(2)
-    rs_far(*sets[2], one2)
     two2 = values(2)
     rs_far(*sets[2], two2)
     rs_first(*sets[2])
@@ -689,9 +689,9 @@
 
     finish(0)
     x_mid(2, True)
+    hand_over(0)
     x_near(2)
     finish(1)
-    hand_over(0)
     hand_over(1)
     x_last(2)
     finish(2)

time: 104 us -> 104 us (level)
  no operation moved by 1% of the time
where the time goes in v14:
time: 104 us
  Pallas kernels  102 us (98%)
  local copies, waits for them, and re-layouts  1.57 us (2%)
    pallas_call x1, Pallas kernels, body(): call(tokens, mixer_gain, ffn_gain, gate_proj, value_proj, value_gain, spa...  102 us

profile of v14, /device:TPU:57, one launch (start us, length us, event | category | flops | bytes accessed | tf_op | source)
XLA Modules:
  0.0 104.0 jit_solution(7215031786722923728)
XLA Ops:
  0.0 102.4 %layer.1 = bf16[128,512]{1,0:T(8,128)(2,1)} custom-call(bf16[128,512]{1,0:T(8,128)(2,1)} %tok.1, f32[4096]{0:T(1024)} %mgain.1, f32[4096]{0:T(1024)} %fgain.1, bf16[256,256]{1,0:T(8,128)(2,1)} %gp.1, bf16[256,256]{1,0:T(8,128)(2,1)} %vp.1, f32[2,128]{1,0:T(2,128)} %vgain.1, bf16[2,8,128]{2,1,0:T(8,128)(2,1)} %smix.1, f32[2,128]{1,0:T(2,128)} %sbias.1, ...), custom_call_target="tpu_custom_call" | custom-call | tf_op jit(solution)/shard_map/layer/pallas_call | solution.py:760
  102.4 1.6 %copy.19 = bf16[128,512]{1,0:T(8,128)(2,1)} copy(bf16[128,512]{1,0:T(8,128)(2,1)} %layer.1) | data formatting | bytes 262144

commit v15 on v12

--- a/solution.py
+++ b/solution.py
@@ -593,12 +593,11 @@
     rs_far(*sets[1], one1)
     two1 = values(1)
     rs_far(*sets[1], two1)
-    rs_first(*sets[1], one1)
     rs_second(*sets[0])
-    rs_first(*sets[1], two1)
+    rs_first(*sets[1])
     z_fwd(7)
+    rs_second(*sets[1])
     z_fwd(8)
-    rs_second(*sets[1])
     recv(SSF.at[pl.ds(0, 3)], kf)
     RS[...] = scale_of(jnp.sum(SSF[...], axis=0)[0:1, :])
     rs_wait(FC[0], kr[0])

time: 103 us -> 103 us (level)
  no operation moved by 1% of the time
where the time goes in v15:
time: 103 us; the launch traced here: 102 us
  Pallas kernels  101 us (98%)
  local copies, waits for them, and re-layouts  1.57 us (2%)
    pallas_call x1, Pallas kernels, body(): call(tokens, mixer_gain, ffn_gain, gate_proj, value_proj, value_gain, spa...  101 us

profile of v15, /device:TPU:57, one launch (start us, length us, event | category | flops | bytes accessed | tf_op | source)
XLA Modules:
  0.0 102.3 jit_solution(10341771247917779658)
XLA Ops:
  0.0 100.7 %layer.1 = bf16[128,512]{1,0:T(8,128)(2,1)} custom-call(bf16[128,512]{1,0:T(8,128)(2,1)} %tok.1, f32[4096]{0:T(1024)} %mgain.1, f32[4096]{0:T(1024)} %fgain.1, bf16[256,256]{1,0:T(8,128)(2,1)} %gp.1, bf16[256,256]{1,0:T(8,128)(2,1)} %vp.1, f32[2,128]{1,0:T(2,128)} %vgain.1, bf16[2,8,128]{2,1,0:T(8,128)(2,1)} %smix.1, f32[2,128]{1,0:T(2,128)} %sbias.1, ...), custom_call_target="tpu_custom_call" | custom-call | tf_op jit(solution)/shard_map/layer/pallas_call | solution.py:748
  100.8 1.6 %copy.19 = bf16[128,512]{1,0:T(8,128)(2,1)} copy(bf16[128,512]{1,0:T(8,128)(2,1)} %layer.1) | data formatting | bytes 262144

commit v16 on v15

--- a/solution.py
+++ b/solution.py
@@ -678,8 +678,8 @@
     x_mid(2)
     finish(0)
     x_near(2)
+    hand_over(0)
     finish(1)
-    hand_over(0)
     hand_over(1)
     x_last(2)
     finish(2)

time: 103 us -> 102 us (level)
  the two profiles are of different devices: /device:TPU:57 before, /device:TPU:71 now
where the time goes in v16:
time: 102 us
  Pallas kernels  101 us (99%)
  local copies, waits for them, and re-layouts  1.57 us (2%)
    pallas_call x1, Pallas kernels, body(): call(tokens, mixer_gain, ffn_gain, gate_proj, value_proj, value_gain, spa...  101 us

profile of v16, /device:TPU:71, one launch (start us, length us, event | category | flops | bytes accessed | tf_op | source)
XLA Modules:
  0.0 102.1 jit_solution(13560384350640729102)
XLA Ops:
  0.0 100.6 %layer.1 = bf16[128,512]{1,0:T(8,128)(2,1)} custom-call(bf16[128,512]{1,0:T(8,128)(2,1)} %tok.1, f32[4096]{0:T(1024)} %mgain.1, f32[4096]{0:T(1024)} %fgain.1, bf16[256,256]{1,0:T(8,128)(2,1)} %gp.1, bf16[256,256]{1,0:T(8,128)(2,1)} %vp.1, f32[2,128]{1,0:T(2,128)} %vgain.1, bf16[2,8,128]{2,1,0:T(8,128)(2,1)} %smix.1, f32[2,128]{1,0:T(2,128)} %sbias.1, ...), custom_call_target="tpu_custom_call" | custom-call | tf_op jit(solution)/shard_map/layer/pallas_call | solution.py:748
  100.6 1.6 %copy.19 = bf16[128,512]{1,0:T(8,128)(2,1)} copy(bf16[128,512]{1,0:T(8,128)(2,1)} %layer.1) | data formatting | bytes 262144
